TPU v7x, 256 devices: a whole 4x4x8 slice. The times are simulated.
256 devices in a mesh: ep: 64 (over z, y, core), tp: 4 (over x).
Axes of the slice: x: 4, y: 4, z: 8, core: 2. Of those that a mesh axis runs over, the one named last changes fastest.
Arguments:
- state_probe_logits: bfloat16 [65536, 1024], P('ep', 'tp'), may hold values from -6 to 6
- retention_logits: bfloat16 [65536, 1024], P('ep', 'tp'), may hold values from -12 to 12
- state_source_entries: bfloat16 [65536, 1024], P('ep', 'tp'), may hold values from -6 to 6
- state_result_switch_logits: bfloat16 [65536, 1024], P('ep', 'tp'), may hold values from -6 to 6
- retention_bound_margin: float32 [1024], P('tp'), may hold values from 0 to 0.07
- extra_fading_amount: float32 [65536, 8], P('ep', 'tp'), may hold values from -0.7 to 0
- state_result_scale: float32 [1024], P('tp'), may hold values from 0.1 to 1.9
- state_result_matrix: bfloat16 [1024, 2048], P(None, 'tp'), may hold values from -0.1875 to 0.1875
- second_slice_tokens: bfloat16 [32768, 2048], P('ep'), may hold values from -6 to 6
- specialist_assignment: int32 [32768, 2], P('ep'), may hold values from 0 to 63, all different within a row; in each aligned block of 128 rows (0 to 127, 128 to 255, ...) at most 8 rows name the same one
- selected_specialist_share: float32 [32768, 2], P('ep'), may hold values from 0.1 to 1
- leading_scale_vector: float32 [2048], replicated, may hold values from 0.1 to 1.9
- trailing_scale_vector: float32 [2048], replicated, may hold values from 0.1 to 1.9
- specialist_switch_matrix: bfloat16 [64, 2048, 2048], P('ep', None, 'tp'), may hold values from -0.3125 to 0.3125
- specialist_widen_matrix: bfloat16 [64, 2048, 2048], P('ep', None, 'tp'), may hold values from -0.3125 to 0.3125
- specialist_contract_matrix: bfloat16 [64, 2048, 2048], P('ep', 'tp'), may hold values from -0.125 to 0.125
Outputs:
- mixer_out: bfloat16 [65536, 2048], P('ep', 'tp')
- moe_out: bfloat16 [32768, 2048], P(('ep', 'tp'))
Inputs may be any that keep to these rules, and one draw needn't show every extreme that they name: `specialist_assignment`: each row names 2 different experts. In each aligned block of 128 rows no expert is named by more than 8 rows, a bound that some block reaches.
All inputs are finite; a program needn't handle non-finite values.
Results may differ from a plain program's by a relative error of at most 0.012.
Values may be sent and summed in bfloat16 or wider, within the bound.
No kernel may reach another device: no remote copies, remote signals or barrier semaphores. Data moves between devices by JAX's collectives and lax.ppermute only.
A program may use at most 128 MiB of HBM per device.

v0:
```python
import functools

import jax
import jax.numpy as jnp
from jax import lax
from jax.experimental import pallas as pl
from jax.experimental.pallas import tpu as pltpu
from jax.sharding import Mesh
from jax.sharding import PartitionSpec as P

HEAD = 128
SPAN = 128
TOK_DEV = 128
EP = ("ep_0", "ep_1", "ep_2")
EP_TP = ("ep_0", "ep_1", "ep_2", "tp")
GROUPS = 2
CHUNKS = 2


NORM_EPS = 1e-06
SWISH_ALPHA = 1.702
CLAMP_LIMIT = 7.0

F32 = jnp.float32
BF16 = jnp.bfloat16


def rms_scale(values, gain):
    return values * lax.rsqrt(jnp.mean(values * values, axis=-1, keepdims=True) + NORM_EPS) * gain


def log_one_minus(x):
    total = jnp.full_like(x, 1.0 / 9.0)
    for k in range(8, 0, -1):
        total = total * x + 1.0 / k
    return -(x * total)


def split3(x):
    hi = x.astype(BF16)
    rest = x - hi.astype(F32)
    mid = rest.astype(BF16)
    low = (rest - mid.astype(F32)).astype(BF16)
    return hi, mid, low


def local_kernel(q_ref, r_ref, v_ref, m_ref, fade_ref, raw_ref, qdec_ref, st_ref):
    rows, width = q_ref.shape
    heads = width // HEAD
    steps = rows // SPAN
    row = lax.broadcasted_iota(jnp.int32, (SPAN, SPAN), 0)
    col = lax.broadcasted_iota(jnp.int32, (SPAN, SPAN), 1)
    lower = row >= col
    tri = lower.astype(F32).astype(BF16)
    margin = m_ref[...]

    def step(n, carry):
        base, states = carry
        at = pl.ds(pl.multiple_of(n * SPAN, SPAN), SPAN)
        q = q_ref[at, :].astype(F32)
        q = q / (1.0 + jnp.exp(-q)) * HEAD ** (-0.5)
        key = margin / (1.0 + jnp.exp(r_ref[at, :].astype(F32)))
        value = v_ref[at, :]
        fade = fade_ref[at, :]
        fade = jnp.concatenate(
            [jnp.broadcast_to(fade[:, h : h + 1], (SPAN, HEAD)) for h in range(heads)], axis=1
        )
        decay = log_one_minus(key) + fade
        cumul = sum(
            jnp.dot(tri, piece, preferred_element_type=F32) for piece in reversed(split3(decay))
        )
        middle = cumul[SPAN // 2 - 1 : SPAN // 2, :]
        last = cumul[SPAN - 1 : SPAN, :]
        grow = jnp.exp(cumul - middle)
        q_mid = (q * grow).astype(BF16)
        k_mid = (key * jnp.exp(middle - cumul)).astype(BF16)
        q_start = (q * jnp.exp(cumul)).astype(BF16)
        k_end = (key * jnp.exp(last - cumul)).astype(BF16)
        qdec_ref[at, :] = (q * jnp.exp(cumul + base)).astype(BF16)
        block_decay = jnp.exp(last)
        after = []
        for h in range(heads):
            c = slice(h * HEAD, (h + 1) * HEAD)
            scores = lax.dot_general(
                q_mid[:, c], k_mid[:, c], (((1,), (1,)), ((), ())), preferred_element_type=F32
            )
            scores = jnp.where(lower, scores, 0.0).astype(BF16)
            inner = jnp.dot(scores, value[:, c], preferred_element_type=F32)
            outer = jnp.dot(q_start[:, c], states[h].astype(BF16), preferred_element_type=F32)
            raw_ref[at, c] = inner + outer
            update = lax.dot_general(
                k_end[:, c], value[:, c], (((0,), (0,)), ((), ())), preferred_element_type=F32
            )
            wide = jnp.transpose(jnp.broadcast_to(block_decay[:, c], (HEAD, HEAD)))
            after.append(wide * states[h] + update)
        return base + last, tuple(after)

    base, states = lax.fori_loop(
        0,
        steps,
        step,
        (jnp.zeros((1, width), F32), tuple(jnp.zeros((HEAD, HEAD), F32) for _ in range(heads))),
    )
    total = jnp.exp(base)
    for h in range(heads):
        c = slice(h * HEAD, (h + 1) * HEAD)
        st_ref[c, :HEAD] = states[h]
        st_ref[c, HEAD:] = jnp.transpose(jnp.broadcast_to(total[:, c], (HEAD, HEAD)))


def prefix_kernel(x_ref, out_ref):
    state = jnp.zeros(out_ref.shape[1:], F32)
    for i in range(x_ref.shape[0]):
        out_ref[i] = state
        state = x_ref[i, :, HEAD:] * state + x_ref[i, :, :HEAD]


def output_kernel(raw_ref, qdec_ref, e_ref, gate_ref, scale_ref, out_ref):
    rows, width = raw_ref.shape
    tile = 256

    def step(n, carry):
        at = pl.ds(pl.multiple_of(n * tile, tile), tile)
        for h in range(width // HEAD):
            c = slice(h * HEAD, (h + 1) * HEAD)
            raw = raw_ref[at, c] + jnp.dot(
                qdec_ref[at, c], e_ref[c, :], preferred_element_type=F32
            )
            normed = raw * lax.rsqrt(jnp.mean(raw * raw, axis=-1, keepdims=True) + NORM_EPS)
            gate = gate_ref[at, c].astype(F32)
            out_ref[at, c] = (
                normed * scale_ref[:, c] * (gate / (1.0 + jnp.exp(-gate)))
            ).astype(BF16)
        return carry

    lax.fori_loop(0, rows // tile, step, 0)


def vmem_call(kernel, outs, flops, bytes_accessed, transcendentals):
    return pl.pallas_call(
        kernel,
        out_shape=outs,
        cost_estimate=pl.CostEstimate(
            flops=flops, bytes_accessed=bytes_accessed, transcendentals=transcendentals
        ),
    )


def local_pass(q, r, v, margin, fade):
    rows, width = q.shape
    return vmem_call(
        local_kernel,
        (
            jax.ShapeDtypeStruct((rows, width), F32),
            jax.ShapeDtypeStruct((rows, width), BF16),
            jax.ShapeDtypeStruct((width, 2 * HEAD), F32),
        ),
        4_000_000_000,
        6 << 20,
        rows * width * 6,
    )(q, r, v, margin.reshape(1, width), fade)


def prefix_pass(x):
    return vmem_call(
        prefix_kernel,
        jax.ShapeDtypeStruct((x.shape[0], x.shape[1], HEAD), F32),
        100_000_000,
        1 << 19,
        0,
    )(x)


def output_pass(raw, qdec, entering, gate, scale):
    rows, width = raw.shape
    return vmem_call(
        output_kernel,
        jax.ShapeDtypeStruct((rows, width), BF16),
        2_000_000_000,
        4 << 20,
        rows * width * 2,
    )(raw, qdec, entering, gate, scale.reshape(1, width))


def shift(x, by):
    n = lax.axis_size("tp")
    return lax.ppermute(x, "tp", [(i, (i + by) % n) for i in range(n)])


def expert_kernel(
    own_ref,
    far_ref,
    gate_own,
    gate_right,
    gate_left,
    up_own,
    up_right,
    up_left,
    down_own,
    down_right,
    down_left,
    out_own_ref,
    out_far_ref,
    rows,
    gate_w,
    up_w,
    down_w,
    hidden,
    sems,
):
    n = own_ref.shape[0]
    half = gate_right.shape[1]
    units = gate_w.shape[1]
    tile = half
    places = (slice(0, 2 * half), slice(2 * half, 3 * half), slice(3 * half, 4 * half))
    loads = []
    for k, place in enumerate(places):
        gate_src = (gate_own, gate_right, gate_left)[k]
        up_src = (up_own, up_right, up_left)[k]
        loads.append(pltpu.make_async_copy(gate_src, gate_w.at[:, place], sems.at[2 * k]))
        loads.append(pltpu.make_async_copy(up_src, up_w.at[:, place], sems.at[2 * k + 1]))
    for k, place in enumerate(places):
        down_src = (down_own, down_right, down_left)[k]
        loads.append(pltpu.make_async_copy(down_src, down_w.at[place, :], sems.at[6 + k]))
    for load in loads:
        load.start()
    rows[:n, :] = own_ref[...]
    rows[n:, :] = far_ref[...]

    def hidden_tile(f, carry):
        for first, k in ((0, 0), (2, 1), (3, 2)):

            @pl.when(f == first)
            def _():
                loads[2 * k].wait()
                loads[2 * k + 1].wait()

        at = pl.ds(pl.multiple_of(f * tile, tile), tile)
        gate = jnp.dot(rows[...], gate_w[:, at], preferred_element_type=F32)
        upward = jnp.dot(rows[...], up_w[:, at], preferred_element_type=F32)
        glued = jnp.minimum(gate, CLAMP_LIMIT)
        linear = jnp.clip(upward, -CLAMP_LIMIT, CLAMP_LIMIT)
        act = glued / (1.0 + jnp.exp(-SWISH_ALPHA * glued)) * (linear + 1.0)
        hidden[:, at] = act.astype(BF16)
        return carry

    lax.fori_loop(0, units // tile, hidden_tile, 0)
    for load in loads[6:]:
        load.wait()

    def out_tile(t, carry):
        at = pl.ds(pl.multiple_of(t * 512, 512), 512)
        part = jnp.dot(hidden[...], down_w[:, at], preferred_element_type=F32).astype(BF16)
        out_own_ref[:, at] = part[:n]
        out_far_ref[:, at] = part[n:]
        return carry

    lax.fori_loop(0, down_w.shape[1] // 512, out_tile, 0)


def expert_block(own, far, gates, ups, downs):
    n, features = own.shape
    units = sum(w.shape[1] for w in gates)
    vmem = pl.BlockSpec(memory_space=pltpu.VMEM)
    return pl.pallas_call(
        expert_kernel,
        out_shape=[jax.ShapeDtypeStruct((n, features), BF16)] * 2,
        in_specs=[vmem] * 2 + [pl.BlockSpec(memory_space=pl.ANY)] * 9,
        out_specs=[vmem] * 2,
        scratch_shapes=[
            pltpu.VMEM((2 * n, features), BF16),
            pltpu.VMEM((features, units), BF16),
            pltpu.VMEM((features, units), BF16),
            pltpu.VMEM((units, features), BF16),
            pltpu.VMEM((2 * n, units), BF16),
            pltpu.SemaphoreType.DMA((9,)),
        ],
        cost_estimate=pl.CostEstimate(
            flops=12 * n * features * units,
            bytes_accessed=6 * features * units + 8 * n * features,
            transcendentals=2 * n * units,
        ),
        name="expert_block",
    )(own, far, *gates, *ups, *downs)


def halves(weight, dim):
    half = weight.shape[dim] // 2
    return (
        lax.slice_in_dim(weight, 0, half, axis=dim),
        lax.slice_in_dim(weight, half, 2 * half, axis=dim),
    )


def widened(weight, pieces):
    first, second = pieces
    return weight, shift(first, -1), shift(second, 1)


def exchange(x):
    return lax.all_to_all(x, EP, split_axis=0, concat_axis=0, tiled=True)


def shards(
    state_probe_logits,
    retention_logits,
    state_source_entries,
    state_result_switch_logits,
    retention_bound_margin,
    extra_fading_amount,
    state_result_scale,
    state_result_matrix,
    second_slice_tokens,
    specialist_assignment,
    selected_specialist_share,
    leading_scale_vector,
    trailing_scale_vector,
    specialist_switch_matrix,
    specialist_widen_matrix,
    specialist_contract_matrix,
):
    _, width = state_probe_logits.shape
    members = lax.axis_size(EP)
    place = lax.axis_index("tp")
    ring = lax.axis_size("tp")
    features = second_slice_tokens.shape[1]

    own_route = lax.dynamic_slice_in_dim(specialist_assignment, place * TOK_DEV, TOK_DEV, 0)
    own_share = lax.dynamic_slice_in_dim(selected_specialist_share, place * TOK_DEV, TOK_DEV, 0)
    own_rows = lax.dynamic_slice_in_dim(second_slice_tokens, place * TOK_DEV, TOK_DEV, 0)

    gate_halves = halves(specialist_switch_matrix[0], 1)
    gate_halves, own_rows = lax.optimization_barrier((gate_halves, own_rows))
    gates = widened(specialist_switch_matrix[0], gate_halves)
    ups = widened(specialist_widen_matrix[0], halves(specialist_widen_matrix[0], 1))
    down_halves = halves(specialist_contract_matrix[0], 0)
    down_halves, retention_logits = lax.optimization_barrier((down_halves, retention_logits))
    downs = widened(specialist_contract_matrix[0], down_halves)
    normed = rms_scale(own_rows.astype(F32), leading_scale_vector).astype(BF16)
    experts = specialist_switch_matrix.shape[0] * members
    capacity = 2 * TOK_DEV * own_route.shape[1] // experts
    expert_ids = jnp.arange(experts, dtype=jnp.int32)[:, None]
    named = [(own_route[:, k][None, :] == expert_ids) for k in range(own_route.shape[1])]
    member = functools.reduce(jnp.logical_or, named)
    weight = sum(jnp.where(named[k], own_share[:, k][None, :], 0.0) for k in range(len(named)))
    ahead = jnp.arange(TOK_DEV)[:, None] < jnp.arange(TOK_DEV)[None, :]
    rank = jnp.dot(
        member.astype(BF16), ahead.astype(BF16), preferred_element_type=F32
    ).astype(jnp.int32)

    def slots_of(first, count):
        ids = first + jnp.arange(count, dtype=jnp.int32)
        return member[:, None, :] & (rank[:, None, :] == ids[None, :, None])

    pick = slots_of(0, capacity).astype(BF16).reshape(experts * capacity, TOK_DEV)
    packed = jnp.dot(pick, normed, preferred_element_type=F32).astype(BF16)
    arrived = exchange(packed.reshape(experts, capacity, features))

    raw, qdec, ends = local_pass(
        state_probe_logits,
        retention_logits,
        state_source_entries,
        retention_bound_margin,
        extra_fading_amount,
    )
    ends, arrived = lax.optimization_barrier((ends, arrived))
    slices = exchange(ends.reshape(members, width // members, 2 * HEAD))
    entering = exchange(prefix_pass(slices).astype(BF16)).reshape(width, HEAD)
    rec = output_pass(raw, qdec, entering, state_result_switch_logits, state_result_scale)

    combined = jnp.zeros((TOK_DEV, features), F32)
    count = capacity // GROUPS
    n = members * count // CHUNKS
    done = None
    for k in range(GROUPS):
        first = k * count
        group = arrived[:, first : first + count].reshape(CHUNKS * n, features)
        if done is not None:
            group, done = lax.optimization_barrier((group, done))
        owns = [group[c * n : (c + 1) * n] for c in range(CHUNKS)]
        fars = [shift(own, 2) for own in owns]
        parts = [expert_block(own, far, gates, ups, downs) for own, far in zip(owns, fars)]
        done = parts[-1][1]
        finished = [
            (mine.astype(F32) + shift(other, 2).astype(F32)).astype(BF16) for mine, other in parts
        ]
        finished = jnp.concatenate(finished, axis=0)
        if k == GROUPS - 1:
            finished, rec = lax.optimization_barrier((finished, rec))
        returned = exchange(finished.reshape(members, count, features))
        share = jnp.where(slots_of(first, count), weight[:, None, :], 0.0)
        share = share.reshape(experts * count, TOK_DEV)
        coarse = share.astype(BF16)
        fine = (share - coarse.astype(F32)).astype(BF16)
        flat = returned.reshape(members * count, features)
        for piece in (coarse, fine):
            combined = combined + lax.dot_general(
                piece, flat, (((0,), (0,)), ((), ())), preferred_element_type=F32
            )
    moe_out = rms_scale(combined, trailing_scale_vector).astype(BF16)

    own, left, right, far = rec, shift(rec, 1), shift(rec, -1), shift(rec, 2)
    by_block = state_result_matrix.reshape(ring, width, -1)

    def columns(block, at):
        held = lax.dynamic_index_in_dim(by_block, lax.rem(place + at, ring), 0, keepdims=False)
        return jnp.dot(block, held, preferred_element_type=F32)

    mixed = columns(own, 0) + columns(left, ring - 1) + columns(right, 1) + columns(far, 2)
    mixer_out = mixed.astype(BF16)
    return (mixer_out, moe_out)


def solution(mesh):
    finer = Mesh(mesh.devices.reshape(8, 4, 2, mesh.shape["tp"]), ("ep_0", "ep_1", "ep_2", "tp"))
    placed = (
        P(EP, "tp"),
        P(EP, "tp"),
        P(EP, "tp"),
        P(EP, "tp"),
        P("tp"),
        P(EP, "tp"),
        P("tp"),
        P(None, "tp"),
        P(EP, None),
        P(EP, None),
        P(EP, None),
        P(),
        P(),
        P(EP, None, "tp"),
        P(EP, None, "tp"),
        P(EP, "tp", None),
    )

    return jax.shard_map(
        shards,
        mesh=finer,
        in_specs=placed,
        out_specs=(P(EP, "tp"), P(EP_TP, None)),
        check_vma=False,
    )
```

profile of v0, /device:TPU:8, one launch (start us, length us, event | category | flops | bytes accessed | tf_op | source)
XLA Modules:
  0.0 253.2 jit_solution(6960685272429485045)
XLA Ops:
  2.3 3.0 %fusion.69 = (bf16[2048,256]{1,0:T(8,128)(2,1)}, bf16[2048,256]{1,0:T(8,128)(2,1)}) fusion(bf16[2048,512]{1,0:T(8,128)(2,1)} %bitcast.63), kind=kLoop, calls=%fused_computation.102 | loop fusion | bytes 4194304 | tf_op jit(solution)/shard_map/slice | solution.py:291
  5.5 2.1 fusion
  7.6 12.4 %all-to-all-start = ((bf16[64,8,2048]{2,1,0:T(8,128)(2,1)}), bf16[64,8,2048]{2,1,0:T(8,128)(2,1)}, u32[]{:S(2)}, u32[]{:S(2)}) async-start(bf16[64,8,2048]{2,1,0:T(8,128)(2,1)} %fusion), calls=%async_computation | async-start | bytes 4194304 | tf_op jit(solution)/shard_map/all_to_all | solution.py:301
  20.1 2.8 %collective-permute-start.1 = (bf16[2048,256]{1,0:T(8,128)(2,1)}, bf16[2048,256]{1,0:T(8,128)(2,1)S(1)}, u32[]{:S(2)}, u32[]{:S(2)}) collective-permute-start(bf16[2048,256]{1,0:T(8,128)(2,1)} %get-tuple-element.28), channel_id=1, source_target_pairs={{0,3},{1,0},{2,1},{3,2},{4,7},{5,4},{6,5},{7,6},{8,11},{9,8},{10,9... | collective-permute-start | bytes 3145736 | tf_op jit(solution)/shard_map/ppermute | solution.py:187
  25.1 2.5 collective-permute-start.3
  29.0 2.0 collective-permute-start.5
  32.1 14.7 %collective-permute-done.1.gate_right = bf16[2048,256]{1,0:T(8,128)(2,1)S(1)} collective-permute-done((bf16[2048,256]{1,0:T(8,128)(2,1)}, bf16[2048,256]{1,0:T(8,128)(2,1)S(1)}, u32[]{:S(2)}, u32[]{:S(2)}) %collective-permute-start.1) | collective-permute-done | bytes 1048608 | tf_op jit(solution)/shard_map/ppermute | solution.py:187
  47.9 8.6 %shard_map.167 = (f32[1024,256]{1,0:T(8,128)}, bf16[1024,256]{1,0:T(8,128)(2,1)}, f32[256,256]{1,0:T(8,128)}) custom-call(bf16[1024,256]{1,0:T(8,128)(2,1)} %q_ref.1, bf16[1024,256]{1,0:T(8,128)(2,1)} %r_ref, bf16[1024,256]{1,0:T(8,128)(2,1)} %v_ref.1, f32[1,256]{1,0:T(1,128)} %bitcast.82, f32[1024,2]{1,0:T(8,128)} %copy.24.fade_ref), custom_call_target="tpu_custom_call" | custom-call | flops 4000000000 | bytes 6291456 | tf_op jit(solution)/shard_map/pallas_call | solution.py:151
  56.5 14.8 %all-to-all-done = bf16[64,8,2048]{2,1,0:T(8,128)(2,1)} async-done(((bf16[64,8,2048]{2,1,0:T(8,128)(2,1)}), bf16[64,8,2048]{2,1,0:T(8,128)(2,1)}, u32[]{:S(2)}, u32[]{:S(2)}) %all-to-all-start) | async-done | bytes 2097184 | tf_op jit(solution)/shard_map/all_to_all | solution.py:301
  72.9 5.4 %all-to-all-start.1 = ((f32[64,4,256]{2,1,0:T(4,128)}), f32[64,4,256]{2,1,0:T(4,128)S(1)}, u32[]{:S(2)}, u32[]{:S(2)}) async-start(f32[64,4,256]{2,1,0:T(4,128)} %reshape.208), calls=%async_computation.1 | async-start | bytes 524288 | tf_op jit(solution)/shard_map/all_to_all | solution.py:301
  78.4 2.1 fusion.67
  81.4 3.0 %collective-permute-start = (bf16[128,2048]{1,0:T(8,128)(2,1)}, bf16[128,2048]{1,0:T(8,128)(2,1)}, u32[]{:S(2)}, u32[]{:S(2)}) collective-permute-start(bf16[128,2048]{1,0:T(8,128)(2,1)} %slice.70.own_ref), channel_id=1, source_target_pairs={{0,2},{1,3},{2,0},{3,1},{4,6},{5,7},{6,4},{7,5},{8,10},{9,11},{10,... | collective-permute-start | bytes 1572872 | tf_op jit(solution)/shard_map/ppermute | solution.py:187
  85.9 3.2 %slice.68 = bf16[64,4,2048]{2,1,0:T(4,128)(2,1)} slice(bf16[64,8,2048]{2,1,0:T(8,128)(2,1)} %all-to-all-done), slice={[0:64], [4:8], [0:2048]} | slice | bytes 2097152 | tf_op jit(solution)/shard_map/slice | solution.py:377
  94.6 10.2 %all-to-all-start.2 = ((bf16[64,4,128]{2,1,0:T(4,128)(2,1)}), bf16[64,4,128]{2,1,0:T(4,128)(2,1)S(1)}, u32[]{:S(2)}, u32[]{:S(2)}) async-start(bf16[64,4,128]{2,1,0:T(4,128)(2,1)} %convert_element_type.96), calls=%async_computation.2 | async-start | bytes 131072 | tf_op jit(solution)/shard_map/all_to_all | solution.py:301
  104.8 8.6 %collective-permute-done.5.down_right = bf16[256,2048]{1,0:T(8,128)(2,1)} collective-permute-done((bf16[256,2048]{1,0:T(8,128)(2,1)}, bf16[256,2048]{1,0:T(8,128)(2,1)}, u32[]{:S(2)}, u32[]{:S(2)}) %collective-permute-start.5) | collective-permute-done | bytes 1048608 | tf_op jit(solution)/shard_map/ppermute | solution.py:187
  113.4 3.4 %collective-permute-done.6.down_left = bf16[256,2048]{1,0:T(8,128)(2,1)} collective-permute-done((bf16[256,2048]{1,0:T(8,128)(2,1)}, bf16[256,2048]{1,0:T(8,128)(2,1)}, u32[]{:S(2)}, u32[]{:S(2)}) %collective-permute-start.6) | collective-permute-done | bytes 1048608 | tf_op jit(solution)/shard_map/ppermute | solution.py:187
  116.7 9.4 %expert_block.4 = (bf16[128,2048]{1,0:T(8,128)(2,1)}, bf16[128,2048]{1,0:T(8,128)(2,1)}) custom-call(bf16[128,2048]{1,0:T(8,128)(2,1)} %slice.70.own_ref, bf16[128,2048]{1,0:T(8,128)(2,1)} %collective-permute-done.far_ref, bf16[2048,512]{1,0:T(8,128)(2,1)} %bitcast.64, bf16[2048,256]{1,0:T(8,128)(2,1)} %copy-done.4, ...), custom_call_target="tpu_custom_call" | custom-call | flops 3221225472 | bytes 14680064 | tf_op jit(solution)/shard_map/expert_block/pallas_call | solution.py:265
  126.2 9.4 %expert_block.7 = (bf16[128,2048]{1,0:T(8,128)(2,1)}, bf16[128,2048]{1,0:T(8,128)(2,1)}) custom-call(bf16[128,2048]{1,0:T(8,128)(2,1)} %slice.78.own_ref, bf16[128,2048]{1,0:T(8,128)(2,1)} %collective-permute-done.14.far_ref, bf16[2048,512]{1,0:T(8,128)(2,1)} %bitcast.65, bf16[2048,256]{1,0:T(8,128)(2,1)} %copy-done.4, ...), custom_call_target="tpu_custom_call" | custom-call | flops 3221225472 | bytes 14680064 | tf_op jit(solution)/shard_map/expert_block/pallas_call | solution.py:265
  135.7 3.6 %collective-permute-start.15 = (bf16[128,2048]{1,0:T(8,128)(2,1)}, bf16[128,2048]{1,0:T(8,128)(2,1)S(1)}, u32[]{:S(2)}, u32[]{:S(2)}) collective-permute-start(bf16[128,2048]{1,0:T(8,128)(2,1)} %get-tuple-element.43), channel_id=1, source_target_pairs={{0,2},{1,3},{2,0},{3,1},{4,6},{5,7},{6,4},{7,5},{8,10},{9,11},{10,... | collective-permute-start | bytes 1572872 | tf_op jit(solution)/shard_map/ppermute | solution.py:187
  140.4 3.5 %collective-permute-start.9 = (bf16[128,2048]{1,0:T(8,128)(2,1)}, bf16[128,2048]{1,0:T(8,128)(2,1)}, u32[]{:S(2)}, u32[]{:S(2)}) collective-permute-start(bf16[128,2048]{1,0:T(8,128)(2,1)} %get-tuple-element.55.own_ref), channel_id=1, source_target_pairs={{0,2},{1,3},{2,0},{3,1},{4,6},{5,7},{6,4},{7,5},{8,10},{9,11},{10,... | collective-permute-start | bytes 1572872 | tf_op jit(solution)/shard_map/ppermute | solution.py:187
  144.0 9.5 %collective-permute-done.15 = bf16[128,2048]{1,0:T(8,128)(2,1)S(1)} collective-permute-done((bf16[128,2048]{1,0:T(8,128)(2,1)}, bf16[128,2048]{1,0:T(8,128)(2,1)S(1)}, u32[]{:S(2)}, u32[]{:S(2)}) %collective-permute-start.15) | collective-permute-done | bytes 524320 | tf_op jit(solution)/shard_map/ppermute | solution.py:187
  155.0 10.3 %all-to-all-start.3 = ((bf16[64,4,2048]{2,1,0:T(4,128)(2,1)}), bf16[64,4,2048]{2,1,0:T(4,128)(2,1)S(1)}, u32[]{:S(2)}, u32[]{:S(2)}) async-start(bf16[64,4,2048]{2,1,0:T(4,128)(2,1)} %reshape.212), calls=%async_computation.3 | async-start | bytes 2097152 | tf_op jit(solution)/shard_map/all_to_all | solution.py:301
  165.4 9.4 %expert_block.5 = (bf16[128,2048]{1,0:T(8,128)(2,1)}, bf16[128,2048]{1,0:T(8,128)(2,1)}) custom-call(bf16[128,2048]{1,0:T(8,128)(2,1)} %get-tuple-element.54.own_ref, bf16[128,2048]{1,0:T(8,128)(2,1)} %collective-permute-done.7.far_ref, bf16[2048,512]{1,0:T(8,128)(2,1)} %bitcast.66, bf16[2048,256]{1,0:T(8,128)(2,1)} %copy-done.4, ...), custom_call_target="tpu_custom_call" | custom-call | flops 3221225472 | bytes 14680064 | tf_op jit(solution)/shard_map/expert_block/pallas_call | solution.py:265
  174.7 2.3 collective-permute-start.8
  177.1 9.4 %expert_block.6 = (bf16[128,2048]{1,0:T(8,128)(2,1)}, bf16[128,2048]{1,0:T(8,128)(2,1)}) custom-call(bf16[128,2048]{1,0:T(8,128)(2,1)} %get-tuple-element.55.own_ref, bf16[128,2048]{1,0:T(8,128)(2,1)} %collective-permute-done.9.far_ref, bf16[2048,512]{1,0:T(8,128)(2,1)} %bitcast.67, bf16[2048,256]{1,0:T(8,128)(2,1)} %copy-done.4, ...), custom_call_target="tpu_custom_call" | custom-call | flops 3221225472 | bytes 14680064 | tf_op jit(solution)/shard_map/expert_block/pallas_call | solution.py:265
  187.8 3.6 %shard_map.169 = bf16[1024,256]{1,0:T(8,128)(2,1)} custom-call(f32[1024,256]{1,0:T(8,128)} %get-tuple-element.38.raw_ref, bf16[1024,256]{1,0:T(8,128)(2,1)} %get-tuple-element.39.qdec_ref, bf16[256,128]{1,0:T(8,128)(2,1)} %bitcast.81, bf16[1024,256]{1,0:T(8,128)(2,1)} %gate_ref.1, f32[1,256]{1,0:T(1,128)} %bitcast.83), custom_call_target="tpu_custom_call" | custom-call | flops 2000000000 | bytes 4194304 | tf_op jit(solution)/shard_map/pallas_call | solution.py:176
  191.6 10.4 %collective-permute-done.10 = bf16[128,2048]{1,0:T(8,128)(2,1)} collective-permute-done((bf16[128,2048]{1,0:T(8,128)(2,1)}, bf16[128,2048]{1,0:T(8,128)(2,1)}, u32[]{:S(2)}, u32[]{:S(2)}) %collective-permute-start.10) | collective-permute-done | bytes 524320 | tf_op jit(solution)/shard_map/ppermute | solution.py:187
  204.5 10.4 %all-to-all-start.4 = ((bf16[64,4,2048]{2,1,0:T(4,128)(2,1)}), bf16[64,4,2048]{2,1,0:T(4,128)(2,1)S(1)}, u32[]{:S(2)}, u32[]{:S(2)}) async-start(bf16[64,4,2048]{2,1,0:T(4,128)(2,1)} %reshape.213), calls=%async_computation.4 | async-start | bytes 2097152 | tf_op jit(solution)/shard_map/all_to_all | solution.py:301
  215.7 2.4 collective-permute-start.13
  218.0 2.6 %collective-permute-start.12 = (bf16[1024,256]{1,0:T(8,128)(2,1)}, bf16[1024,256]{1,0:T(8,128)(2,1)S(1)}, u32[]{:S(2)}, u32[]{:S(2)}) collective-permute-start(bf16[1024,256]{1,0:T(8,128)(2,1)} %shard_map.169), channel_id=1, source_target_pairs={{0,3},{1,0},{2,1},{3,2},{4,7},{5,4},{6,5},{7,6},{8,11},{9,8},{10,9... | collective-permute-start | bytes 1572872 | tf_op jit(solution)/shard_map/ppermute | solution.py:187
  222.2 20.2 %collective-permute-done.11 = bf16[1024,256]{1,0:T(8,128)(2,1)} collective-permute-done((bf16[1024,256]{1,0:T(8,128)(2,1)}, bf16[1024,256]{1,0:T(8,128)(2,1)}, u32[]{:S(2)}, u32[]{:S(2)}) %collective-permute-start.11) | collective-permute-done | bytes 524320 | tf_op jit(solution)/shard_map/ppermute | solution.py:187
  245.7 2.3 convolution_bitcast_fusion.2
  (99 shorter events, 34.7 us)
Async XLA Ops:
  7.6 15.3 %copy-start.2 = (bf16[1,2048,512]{2,1,0:T(8,128)(2,1)S(1)}, bf16[1,2048,512]{2,1,0:T(8,128)(2,1)}, u32[]{:S(2)}) copy-start(bf16[1,2048,512]{2,1,0:T(8,128)(2,1)} %param.30) | copy-start | bytes 6291460
  7.6 63.6 %all-to-all-start = ((bf16[64,8,2048]{2,1,0:T(8,128)(2,1)}), bf16[64,8,2048]{2,1,0:T(8,128)(2,1)}, u32[]{:S(2)}, u32[]{:S(2)}) async-start(bf16[64,8,2048]{2,1,0:T(8,128)(2,1)} %fusion), calls=%async_computation | async-start | bytes 4194304 | tf_op jit(solution)/shard_map/all_to_all | solution.py:301
  20.1 26.7 %collective-permute-start.1 = (bf16[2048,256]{1,0:T(8,128)(2,1)}, bf16[2048,256]{1,0:T(8,128)(2,1)S(1)}, u32[]{:S(2)}, u32[]{:S(2)}) collective-permute-start(bf16[2048,256]{1,0:T(8,128)(2,1)} %get-tuple-element.28), channel_id=1, source_target_pairs={{0,3},{1,0},{2,1},{3,2},{4,7},{5,4},{6,5},{7,6},{8,11},{9,8},{10,9... | collective-permute-start | bytes 3145736 | tf_op jit(solution)/shard_map/ppermute | solution.py:187
  22.9 58.5 %collective-permute-start.2 = (bf16[2048,256]{1,0:T(8,128)(2,1)}, bf16[2048,256]{1,0:T(8,128)(2,1)}, u32[]{:S(2)}, u32[]{:S(2)}) collective-permute-start(bf16[2048,256]{1,0:T(8,128)(2,1)} %get-tuple-element.29), channel_id=1, source_target_pairs={{0,1},{1,2},{2,3},{3,0},{4,5},{5,6},{6,7},{7,4},{8,9},{9,10},{10,1... | collective-permute-start | bytes 3145736 | tf_op jit(solution)/shard_map/ppermute | solution.py:187
  24.3 61.0 %collective-permute-start.4 = (bf16[2048,256]{1,0:T(8,128)(2,1)}, bf16[2048,256]{1,0:T(8,128)(2,1)S(1)}, u32[]{:S(2)}, u32[]{:S(2)}) collective-permute-start(bf16[2048,256]{1,0:T(8,128)(2,1)} %get-tuple-element.48), channel_id=1, source_target_pairs={{0,1},{1,2},{2,3},{3,0},{4,5},{5,6},{6,7},{7,4},{8,9},{9,10},{10,1... | collective-permute-start | bytes 3145736 | tf_op jit(solution)/shard_map/ppermute | solution.py:187
  25.1 6.0 %copy-start.16 = (f32[1024,2]{0,1:T(2,128)S(1)}, f32[1024,2]{0,1:T(2,128)}, u32[]{:S(2)}) copy-start(f32[1024,2]{0,1:T(2,128)} %param.21) | copy-start | bytes 24580
  25.1 79.6 %collective-permute-start.3 = (bf16[2048,256]{1,0:T(8,128)(2,1)}, bf16[2048,256]{1,0:T(8,128)(2,1)S(1)}, u32[]{:S(2)}, u32[]{:S(2)}) collective-permute-start(bf16[2048,256]{1,0:T(8,128)(2,1)} %get-tuple-element.49), channel_id=1, source_target_pairs={{0,3},{1,0},{2,1},{3,2},{4,7},{5,4},{6,5},{7,6},{8,11},{9,8},{10,9... | collective-permute-start | bytes 3145736 | tf_op jit(solution)/shard_map/ppermute | solution.py:187
  29.0 84.3 %collective-permute-start.5 = (bf16[256,2048]{1,0:T(8,128)(2,1)}, bf16[256,2048]{1,0:T(8,128)(2,1)}, u32[]{:S(2)}, u32[]{:S(2)}) collective-permute-start(bf16[256,2048]{1,0:T(8,128)(2,1)} %get-tuple-element.30), channel_id=1, source_target_pairs={{0,3},{1,0},{2,1},{3,2},{4,7},{5,4},{6,5},{7,6},{8,11},{9,8},{10,9... | collective-permute-start | bytes 3145736 | tf_op jit(solution)/shard_map/ppermute | solution.py:187
  46.8 9.7 %copy-start.4 = (bf16[2048,256]{1,0:T(8,128)(2,1)}, bf16[2048,256]{1,0:T(8,128)(2,1)S(1)}, u32[]{:S(2)}) copy-start(bf16[2048,256]{1,0:T(8,128)(2,1)S(1)} %collective-permute-done.1.gate_right) | copy-start | bytes 3145732
  46.8 70.0 %collective-permute-start.6 = (bf16[256,2048]{1,0:T(8,128)(2,1)}, bf16[256,2048]{1,0:T(8,128)(2,1)}, u32[]{:S(2)}, u32[]{:S(2)}) collective-permute-start(bf16[256,2048]{1,0:T(8,128)(2,1)} %get-tuple-element.31), channel_id=1, source_target_pairs={{0,1},{1,2},{2,3},{3,0},{4,5},{5,6},{6,7},{7,4},{8,9},{9,10},{10,1... | collective-permute-start | bytes 3145736 | tf_op jit(solution)/shard_map/ppermute | solution.py:187
  72.9 17.6 %all-to-all-start.1 = ((f32[64,4,256]{2,1,0:T(4,128)}), f32[64,4,256]{2,1,0:T(4,128)S(1)}, u32[]{:S(2)}, u32[]{:S(2)}) async-start(f32[64,4,256]{2,1,0:T(4,128)} %reshape.208), calls=%async_computation.1 | async-start | bytes 524288 | tf_op jit(solution)/shard_map/all_to_all | solution.py:301
  81.4 35.3 %collective-permute-start = (bf16[128,2048]{1,0:T(8,128)(2,1)}, bf16[128,2048]{1,0:T(8,128)(2,1)}, u32[]{:S(2)}, u32[]{:S(2)}) collective-permute-start(bf16[128,2048]{1,0:T(8,128)(2,1)} %slice.70.own_ref), channel_id=1, source_target_pairs={{0,2},{1,3},{2,0},{3,1},{4,6},{5,7},{6,4},{7,5},{8,10},{9,11},{10,... | collective-permute-start | bytes 1572872 | tf_op jit(solution)/shard_map/ppermute | solution.py:187
  85.4 5.1 %copy-start.5 = (bf16[2048,256]{1,0:T(8,128)(2,1)}, bf16[2048,256]{1,0:T(8,128)(2,1)S(1)}, u32[]{:S(2)}) copy-start(bf16[2048,256]{1,0:T(8,128)(2,1)S(1)} %collective-permute-done.4.up_left) | copy-start | bytes 3145732
  85.4 40.8 %collective-permute-start.14 = (bf16[128,2048]{1,0:T(8,128)(2,1)}, bf16[128,2048]{1,0:T(8,128)(2,1)}, u32[]{:S(2)}, u32[]{:S(2)}) collective-permute-start(bf16[128,2048]{1,0:T(8,128)(2,1)} %slice.78.own_ref), channel_id=1, source_target_pairs={{0,2},{1,3},{2,0},{3,1},{4,6},{5,7},{6,4},{7,5},{8,10},{9,11},{10,... | collective-permute-start | bytes 1572872 | tf_op jit(solution)/shard_map/ppermute | solution.py:187
  94.6 60.5 %all-to-all-start.2 = ((bf16[64,4,128]{2,1,0:T(4,128)(2,1)}), bf16[64,4,128]{2,1,0:T(4,128)(2,1)S(1)}, u32[]{:S(2)}, u32[]{:S(2)}) async-start(bf16[64,4,128]{2,1,0:T(4,128)(2,1)} %convert_element_type.96), calls=%async_computation.2 | async-start | bytes 131072 | tf_op jit(solution)/shard_map/all_to_all | solution.py:301
  104.7 12.0 %copy-start.6 = (bf16[2048,256]{1,0:T(8,128)(2,1)}, bf16[2048,256]{1,0:T(8,128)(2,1)S(1)}, u32[]{:S(2)}) copy-start(bf16[2048,256]{1,0:T(8,128)(2,1)S(1)} %collective-permute-done.3.up_right) | copy-start | bytes 3145732
  126.1 17.8 %collective-permute-start.16 = (bf16[128,2048]{1,0:T(8,128)(2,1)}, bf16[128,2048]{1,0:T(8,128)(2,1)S(1)}, u32[]{:S(2)}, u32[]{:S(2)}) collective-permute-start(bf16[128,2048]{1,0:T(8,128)(2,1)} %get-tuple-element.32), channel_id=1, source_target_pairs={{0,2},{1,3},{2,0},{3,1},{4,6},{5,7},{6,4},{7,5},{8,10},{9,11},{10,... | collective-permute-start | bytes 1572872 | tf_op jit(solution)/shard_map/ppermute | solution.py:187
  135.6 8.3 %copy-start.10 = (bf16[128,2048]{1,0:T(8,128)(2,1)S(1)}, bf16[128,2048]{1,0:T(8,128)(2,1)}, u32[]{:S(2)}) copy-start(bf16[128,2048]{1,0:T(8,128)(2,1)} %get-tuple-element.44) | copy-start | bytes 1572868
  135.7 17.9 %copy-start.12 = (bf16[128,2048]{1,0:T(8,128)(2,1)S(1)}, bf16[128,2048]{1,0:T(8,128)(2,1)}, u32[]{:S(2)}) copy-start(bf16[128,2048]{1,0:T(8,128)(2,1)} %get-tuple-element.42) | copy-start | bytes 1572868
  135.7 17.9 %collective-permute-start.15 = (bf16[128,2048]{1,0:T(8,128)(2,1)}, bf16[128,2048]{1,0:T(8,128)(2,1)S(1)}, u32[]{:S(2)}, u32[]{:S(2)}) collective-permute-start(bf16[128,2048]{1,0:T(8,128)(2,1)} %get-tuple-element.43), channel_id=1, source_target_pairs={{0,2},{1,3},{2,0},{3,1},{4,6},{5,7},{6,4},{7,5},{8,10},{9,11},{10,... | collective-permute-start | bytes 1572872 | tf_op jit(solution)/shard_map/ppermute | solution.py:187
  140.4 25.0 %collective-permute-start.7 = (bf16[128,2048]{1,0:T(8,128)(2,1)}, bf16[128,2048]{1,0:T(8,128)(2,1)}, u32[]{:S(2)}, u32[]{:S(2)}) collective-permute-start(bf16[128,2048]{1,0:T(8,128)(2,1)} %get-tuple-element.54.own_ref), channel_id=1, source_target_pairs={{0,2},{1,3},{2,0},{3,1},{4,6},{5,7},{6,4},{7,5},{8,10},{9,11},{10,... | collective-permute-start | bytes 1572872 | tf_op jit(solution)/shard_map/ppermute | solution.py:187
  140.4 36.7 %collective-permute-start.9 = (bf16[128,2048]{1,0:T(8,128)(2,1)}, bf16[128,2048]{1,0:T(8,128)(2,1)}, u32[]{:S(2)}, u32[]{:S(2)}) collective-permute-start(bf16[128,2048]{1,0:T(8,128)(2,1)} %get-tuple-element.55.own_ref), channel_id=1, source_target_pairs={{0,2},{1,3},{2,0},{3,1},{4,6},{5,7},{6,4},{7,5},{8,10},{9,11},{10,... | collective-permute-start | bytes 1572872 | tf_op jit(solution)/shard_map/ppermute | solution.py:187
  155.0 19.7 %copy-start.14 = (bf16[64,4,128]{2,1,0:T(4,128)(2,1)}, bf16[64,4,128]{2,1,0:T(4,128)(2,1)S(1)}, u32[]{:S(2)}) copy-start(bf16[64,4,128]{2,1,0:T(4,128)(2,1)S(1)} %all-to-all-done.2) | copy-start | bytes 196612
  155.0 49.5 %all-to-all-start.3 = ((bf16[64,4,2048]{2,1,0:T(4,128)(2,1)}), bf16[64,4,2048]{2,1,0:T(4,128)(2,1)S(1)}, u32[]{:S(2)}, u32[]{:S(2)}) async-start(bf16[64,4,2048]{2,1,0:T(4,128)(2,1)} %reshape.212), calls=%async_computation.3 | async-start | bytes 2097152 | tf_op jit(solution)/shard_map/all_to_all | solution.py:301
  174.7 16.7 %collective-permute-start.8 = (bf16[128,2048]{1,0:T(8,128)(2,1)}, bf16[128,2048]{1,0:T(8,128)(2,1)S(1)}, u32[]{:S(2)}, u32[]{:S(2)}) collective-permute-start(bf16[128,2048]{1,0:T(8,128)(2,1)} %get-tuple-element.35), channel_id=1, source_target_pairs={{0,2},{1,3},{2,0},{3,1},{4,6},{5,7},{6,4},{7,5},{8,10},{9,11},{10,... | collective-permute-start | bytes 1572872 | tf_op jit(solution)/shard_map/ppermute | solution.py:187
  186.4 15.6 %collective-permute-start.10 = (bf16[128,2048]{1,0:T(8,128)(2,1)}, bf16[128,2048]{1,0:T(8,128)(2,1)}, u32[]{:S(2)}, u32[]{:S(2)}) collective-permute-start(bf16[128,2048]{1,0:T(8,128)(2,1)} %get-tuple-element.37), channel_id=1, source_target_pairs={{0,2},{1,3},{2,0},{3,1},{4,6},{5,7},{6,4},{7,5},{8,10},{9,11},{10,... | collective-permute-start | bytes 1572872 | tf_op jit(solution)/shard_map/ppermute | solution.py:187
  187.8 14.2 %copy-start.13 = (bf16[128,2048]{1,0:T(8,128)(2,1)S(1)}, bf16[128,2048]{1,0:T(8,128)(2,1)}, u32[]{:S(2)}) copy-start(bf16[128,2048]{1,0:T(8,128)(2,1)} %get-tuple-element.36) | copy-start | bytes 1572868
  204.5 16.2 %copy-start.8 = (bf16[1024,512]{1,0:T(8,128)(2,1)S(1)}, bf16[1024,512]{1,0:T(8,128)(2,1)}, u32[]{:S(2)}) copy-start(bf16[1024,512]{1,0:T(8,128)(2,1)} %param.23) | copy-start | bytes 3145732
  204.5 43.5 %all-to-all-start.4 = ((bf16[64,4,2048]{2,1,0:T(4,128)(2,1)}), bf16[64,4,2048]{2,1,0:T(4,128)(2,1)S(1)}, u32[]{:S(2)}, u32[]{:S(2)}) async-start(bf16[64,4,2048]{2,1,0:T(4,128)(2,1)} %reshape.213), calls=%async_computation.4 | async-start | bytes 2097152 | tf_op jit(solution)/shard_map/all_to_all | solution.py:301
  215.6 26.7 %collective-permute-start.11 = (bf16[1024,256]{1,0:T(8,128)(2,1)}, bf16[1024,256]{1,0:T(8,128)(2,1)}, u32[]{:S(2)}, u32[]{:S(2)}) collective-permute-start(bf16[1024,256]{1,0:T(8,128)(2,1)} %shard_map.169), channel_id=1, source_target_pairs={{0,1},{1,2},{2,3},{3,0},{4,5},{5,6},{6,7},{7,4},{8,9},{9,10},{10,1... | collective-permute-start | bytes 1572872 | tf_op jit(solution)/shard_map/ppermute | solution.py:187
  215.7 28.6 %collective-permute-start.13 = (bf16[1024,256]{1,0:T(8,128)(2,1)}, bf16[1024,256]{1,0:T(8,128)(2,1)S(1)}, u32[]{:S(2)}, u32[]{:S(2)}) collective-permute-start(bf16[1024,256]{1,0:T(8,128)(2,1)} %shard_map.169), channel_id=1, source_target_pairs={{0,2},{1,3},{2,0},{3,1},{4,6},{5,7},{6,4},{7,5},{8,10},{9,11},{10,... | collective-permute-start | bytes 1572872 | tf_op jit(solution)/shard_map/ppermute | solution.py:187
  218.0 25.8 %collective-permute-start.12 = (bf16[1024,256]{1,0:T(8,128)(2,1)}, bf16[1024,256]{1,0:T(8,128)(2,1)S(1)}, u32[]{:S(2)}, u32[]{:S(2)}) collective-permute-start(bf16[1024,256]{1,0:T(8,128)(2,1)} %shard_map.169), channel_id=1, source_target_pairs={{0,3},{1,0},{2,1},{3,2},{4,7},{5,4},{6,5},{7,6},{8,11},{9,8},{10,9... | collective-permute-start | bytes 1572872 | tf_op jit(solution)/shard_map/ppermute | solution.py:187
  (8 other events, 20.5 us)
where the time goes:
time: 254 us; the launch traced here: 253 us
  waiting for transfers between devices  81.7 us (32%)
  starting transfers between devices  77.4 us (30%)
  Pallas kernels  51.5 us (20%)
  local copies, waits for them, and re-layouts  23.6 us (9%)
  matrix products  13.6 us (5%)
  other arithmetic  4.49 us (2%)
    ppermute x17, waiting for transfers between devices, shift(): return lax.ppermute(x, 'tp', [(i, (i + by) % n) for i in range(n)])  66.8 us
    all_to_all x5, starting transfers between devices, exchange(): return lax.all_to_all(x, EP, split_axis=0, concat_axis=0, tiled=True)  48.8 us
    pallas_call x4, Pallas kernels, expert_block(): pl.pallas_call(expert_kernel, out_shape=[jax.ShapeDtypeStruct((n, feature...  37.5 us
    ppermute x17, starting transfers between devices, shift(): return lax.ppermute(x, 'tp', [(i, (i + by) % n) for i in range(n)])  28.6 us
    all_to_all x5, waiting for transfers between devices, exchange(): return lax.all_to_all(x, EP, split_axis=0, concat_axis=0, tiled=True)  14.9 us
    pallas_call x1, Pallas kernels, local_pass(): vmem_call(local_kernel, (jax.ShapeDtypeStruct((rows, width), F32), jax.Sh...  8.58 us
    dot_general x4, matrix products, shards(): lax.dot_general(piece, flat, (((0,), (0,)), ((), ())), preferred_element_...  6.46 us
    slice x3, local copies, waits for them, and re-layouts, halves(): lax.slice_in_dim(weight, half, 2 * half, axis=dim)  5.87 us
  transfers between devices with their start and end apart: 22, of which 8 were waited for; matrix products, arithmetic and copies ran while one was open for 11% of the time, Pallas kernels for 20%

commit v1 on v0

--- a/solution.py
+++ b/solution.py
@@ -14,6 +14,8 @@
 EP = ("ep_0", "ep_1", "ep_2")
 EP_TP = ("ep_0", "ep_1", "ep_2", "tp")
 GROUPS = 2
+EXPERT_VMEM = 24 << 20
+SMALL_VMEM = 12 << 20
 CHUNKS = 2
 
 
@@ -140,6 +142,7 @@
     return pl.pallas_call(
         kernel,
         out_shape=outs,
+        compiler_params=pltpu.CompilerParams(vmem_limit_bytes=SMALL_VMEM),
         cost_estimate=pl.CostEstimate(
             flops=flops, bytes_accessed=bytes_accessed, transcendentals=transcendentals
         ),
@@ -202,79 +205,82 @@
     out_own_ref,
     out_far_ref,
     rows,
-    gate_w,
-    up_w,
-    down_w,
     hidden,
+    gate_more,
+    up_more,
+    down_more,
     sems,
 ):
     n = own_ref.shape[0]
-    half = gate_right.shape[1]
-    units = gate_w.shape[1]
-    tile = half
-    places = (slice(0, 2 * half), slice(2 * half, 3 * half), slice(3 * half, 4 * half))
-    loads = []
-    for k, place in enumerate(places):
-        gate_src = (gate_own, gate_right, gate_left)[k]
-        up_src = (up_own, up_right, up_left)[k]
-        loads.append(pltpu.make_async_copy(gate_src, gate_w.at[:, place], sems.at[2 * k]))
-        loads.append(pltpu.make_async_copy(up_src, up_w.at[:, place], sems.at[2 * k + 1]))
-    for k, place in enumerate(places):
-        down_src = (down_own, down_right, down_left)[k]
-        loads.append(pltpu.make_async_copy(down_src, down_w.at[place, :], sems.at[6 + k]))
+    tile = gate_right.shape[1]
+    first, second = slice(0, tile), slice(tile, 2 * tile)
+    loads = [
+        pltpu.make_async_copy(gate_right, gate_more.at[:, first], sems.at[0]),
+        pltpu.make_async_copy(gate_left, gate_more.at[:, second], sems.at[1]),
+        pltpu.make_async_copy(up_right, up_more.at[:, first], sems.at[2]),
+        pltpu.make_async_copy(up_left, up_more.at[:, second], sems.at[3]),
+        pltpu.make_async_copy(down_right, down_more.at[first, :], sems.at[4]),
+        pltpu.make_async_copy(down_left, down_more.at[second, :], sems.at[5]),
+    ]
     for load in loads:
         load.start()
     rows[:n, :] = own_ref[...]
     rows[n:, :] = far_ref[...]
 
-    def hidden_tile(f, carry):
-        for first, k in ((0, 0), (2, 1), (3, 2)):
-
-            @pl.when(f == first)
-            def _():
-                loads[2 * k].wait()
-                loads[2 * k + 1].wait()
-
-        at = pl.ds(pl.multiple_of(f * tile, tile), tile)
-        gate = jnp.dot(rows[...], gate_w[:, at], preferred_element_type=F32)
-        upward = jnp.dot(rows[...], up_w[:, at], preferred_element_type=F32)
-        glued = jnp.minimum(gate, CLAMP_LIMIT)
-        linear = jnp.clip(upward, -CLAMP_LIMIT, CLAMP_LIMIT)
-        act = glued / (1.0 + jnp.exp(-SWISH_ALPHA * glued)) * (linear + 1.0)
-        hidden[:, at] = act.astype(BF16)
-        return carry
-
-    lax.fori_loop(0, units // tile, hidden_tile, 0)
-    for load in loads[6:]:
+    def hidden_tiles(gate_w, up_w, offset):
+        def step(f, carry):
+            at = pl.ds(pl.multiple_of(f * tile, tile), tile)
+            to = pl.ds(pl.multiple_of(f * tile + offset, tile), tile)
+            gate = jnp.dot(rows[...], gate_w[:, at], preferred_element_type=F32)
+            upward = jnp.dot(rows[...], up_w[:, at], preferred_element_type=F32)
+            glued = jnp.minimum(gate, CLAMP_LIMIT)
+            linear = jnp.clip(upward, -CLAMP_LIMIT, CLAMP_LIMIT)
+            act = glued / (1.0 + jnp.exp(-SWISH_ALPHA * glued)) * (linear + 1.0)
+            hidden[:, to] = act.astype(BF16)
+            return carry
+
+        lax.fori_loop(0, 2, step, 0)
+
+    hidden_tiles(gate_own, up_own, 0)
+    for load in loads[:4]:
         load.wait()
+    hidden_tiles(gate_more, up_more, 2 * tile)
+    for load in loads[4:]:
+        load.wait()
 
     def out_tile(t, carry):
-        at = pl.ds(pl.multiple_of(t * 512, 512), 512)
-        part = jnp.dot(hidden[...], down_w[:, at], preferred_element_type=F32).astype(BF16)
+        at = pl.ds(pl.multiple_of(t * 256, 256), 256)
+        part = (
+            jnp.dot(hidden[:, : 2 * tile], down_own[:, at], preferred_element_type=F32)
+            + jnp.dot(hidden[:, 2 * tile :], down_more[:, at], preferred_element_type=F32)
+        ).astype(BF16)
         out_own_ref[:, at] = part[:n]
         out_far_ref[:, at] = part[n:]
         return carry
 
-    lax.fori_loop(0, down_w.shape[1] // 512, out_tile, 0)
+    lax.fori_loop(0, down_own.shape[1] // 256, out_tile, 0)
 
 
 def expert_block(own, far, gates, ups, downs):
     n, features = own.shape
     units = sum(w.shape[1] for w in gates)
     vmem = pl.BlockSpec(memory_space=pltpu.VMEM)
+    hbm = pl.BlockSpec(memory_space=pltpu.HBM)
+    half = units // 2
     return pl.pallas_call(
         expert_kernel,
         out_shape=[jax.ShapeDtypeStruct((n, features), BF16)] * 2,
-        in_specs=[vmem] * 2 + [pl.BlockSpec(memory_space=pl.ANY)] * 9,
+        in_specs=[vmem] * 2 + [vmem, hbm, hbm] * 3,
         out_specs=[vmem] * 2,
         scratch_shapes=[
             pltpu.VMEM((2 * n, features), BF16),
-            pltpu.VMEM((features, units), BF16),
-            pltpu.VMEM((features, units), BF16),
-            pltpu.VMEM((units, features), BF16),
             pltpu.VMEM((2 * n, units), BF16),
-            pltpu.SemaphoreType.DMA((9,)),
+            pltpu.VMEM((features, half), BF16),
+            pltpu.VMEM((features, half), BF16),
+            pltpu.VMEM((half, features), BF16),
+            pltpu.SemaphoreType.DMA((6,)),
         ],
+        compiler_params=pltpu.CompilerParams(vmem_limit_bytes=EXPERT_VMEM),
         cost_estimate=pl.CostEstimate(
             flops=12 * n * features * units,
             bytes_accessed=6 * features * units + 8 * n * features,
@@ -363,30 +369,45 @@
         retention_bound_margin,
         extra_fading_amount,
     )
+    ends = ends.reshape(members, width // members, 2 * HEAD)
     ends, arrived = lax.optimization_barrier((ends, arrived))
-    slices = exchange(ends.reshape(members, width // members, 2 * HEAD))
-    entering = exchange(prefix_pass(slices).astype(BF16)).reshape(width, HEAD)
-    rec = output_pass(raw, qdec, entering, state_result_switch_logits, state_result_scale)
+    slices = exchange(ends)
 
     combined = jnp.zeros((TOK_DEV, features), F32)
     count = capacity // GROUPS
     n = members * count // CHUNKS
-    done = None
+    flat_in = arrived.reshape(CHUNKS, -1, features)
+    at = jnp.arange(n, dtype=jnp.int32)
+    where = at // count * capacity + at % count
+    owns = []
+    for k in range(GROUPS):
+        chosen = (where + k * count)[:, None] == jnp.arange(flat_in.shape[1])[None, :]
+        for c in range(CHUNKS):
+            owns.append(
+                jnp.dot(chosen.astype(BF16), flat_in[c], preferred_element_type=F32).astype(BF16)
+            )
+    parts = []
+    for k in range(GROUPS):
+        for c in range(CHUNKS):
+            i = k * CHUNKS + c
+            own = owns[i]
+            if i >= 3:
+                own, gate = lax.optimization_barrier((own, parts[i - 2][1]))
+                parts[i - 2] = (parts[i - 2][0], gate)
+            far = shift(own, 2)
+            parts.append(expert_block(own, far, gates, ups, downs))
+            if i == 1:
+                entering = exchange(prefix_pass(slices).astype(BF16)).reshape(width, HEAD)
+    rec = output_pass(raw, qdec, entering, state_result_switch_logits, state_result_scale)
+    parts[-1], rec = lax.optimization_barrier((parts[-1], rec))
     for k in range(GROUPS):
         first = k * count
-        group = arrived[:, first : first + count].reshape(CHUNKS * n, features)
-        if done is not None:
-            group, done = lax.optimization_barrier((group, done))
-        owns = [group[c * n : (c + 1) * n] for c in range(CHUNKS)]
-        fars = [shift(own, 2) for own in owns]
-        parts = [expert_block(own, far, gates, ups, downs) for own, far in zip(owns, fars)]
-        done = parts[-1][1]
-        finished = [
-            (mine.astype(F32) + shift(other, 2).astype(F32)).astype(BF16) for mine, other in parts
-        ]
+        finished = []
+        for c in range(CHUNKS):
+            mine, other = parts[k * CHUNKS + c]
+            back = shift(other, 2)
+            finished.append((mine.astype(F32) + back.astype(F32)).astype(BF16))
         finished = jnp.concatenate(finished, axis=0)
-        if k == GROUPS - 1:
-            finished, rec = lax.optimization_barrier((finished, rec))
         returned = exchange(finished.reshape(members, count, features))
         share = jnp.where(slots_of(first, count), weight[:, None, :], 0.0)
         share = share.reshape(experts * count, TOK_DEV)

time: 254 us -> 271 us (1.067)
  Pallas kernels: 51.5 us -> 35.7 us
  matrix products: 13.6 us -> 25.5 us
  waiting for transfers between devices: 81.7 us -> 93 us
  local copies, waits for them, and re-layouts: 23.6 us -> 29.8 us
    ppermute x17, waiting for transfers between devices: 66.8 us -> 82.5 us  [shift(): return lax.ppermute(x, 'tp', [(i, (i + by) % n) for i in range(n)])]
    unnamed x37 -> x61, local copies, waits for them, and re-layouts: 2.3 us -> 15.1 us
    pallas_call x4, Pallas kernels: 37.5 us -> 28.2 us  [expert_block(): pl.pallas_call(expert_kernel, out_shape=[jax.ShapeDtypeStruct((n, feature...]
    slice x5 -> x0, local copies, waits for them, and re-layouts: 8.26 us -> none  [the longest x4 5.06 us: shards(): owns = [group[c * n:(c + 1) * n] for c in range(CHUNKS)]]
    dot_general x0 -> x4, matrix products: none -> 8.08 us  [shards(): jnp.dot(chosen.astype(BF16), flat_in[c], preferred_element_type=F32)]
    all_to_all x5, waiting for transfers between devices: 14.9 us -> 10.5 us  [exchange(): return lax.all_to_all(x, EP, split_axis=0, concat_axis=0, tiled=True)]
    dot_general x4, matrix products: 6.46 us -> 10.4 us  [shards(): lax.dot_general(piece, flat, (((0,), (0,)), ((), ())), preferred_element_...]
  transfers between devices with their start and end apart: 22 -> 22, of which waited for: 8 -> 7; matrix products, arithmetic and copies ran while one was open for 11% -> 12% of each run, Pallas kernels for 20% -> 13%
where the time goes in v1:
time: 271 us; the launch traced here: 270 us
  waiting for transfers between devices  93 us (34%)
  starting transfers between devices  77.9 us (29%)
  Pallas kernels  35.7 us (13%)
  local copies, waits for them, and re-layouts  29.8 us (11%)
  matrix products  25.5 us (9%)
  other arithmetic  6.98 us (3%)
    ppermute x17, waiting for transfers between devices, shift(): return lax.ppermute(x, 'tp', [(i, (i + by) % n) for i in range(n)])  82.5 us
    all_to_all x5, starting transfers between devices, exchange(): return lax.all_to_all(x, EP, split_axis=0, concat_axis=0, tiled=True)  49 us
    ppermute x17, starting transfers between devices, shift(): return lax.ppermute(x, 'tp', [(i, (i + by) % n) for i in range(n)])  28.9 us
    pallas_call x4, Pallas kernels, expert_block(): pl.pallas_call(expert_kernel, out_shape=[jax.ShapeDtypeStruct((n, feature...  28.2 us
    unnamed x61, local copies, waits for them, and re-layouts  15.1 us
    all_to_all x5, waiting for transfers between devices, exchange(): return lax.all_to_all(x, EP, split_axis=0, concat_axis=0, tiled=True)  10.5 us
    dot_general x4, matrix products, shards(): lax.dot_general(piece, flat, (((0,), (0,)), ((), ())), preferred_element_...  10.4 us
    dot_general x4, matrix products, shards(): jnp.dot(chosen.astype(BF16), flat_in[c], preferred_element_type=F32)  8.08 us
  transfers between devices with their start and end apart: 22, of which 7 were waited for; matrix products, arithmetic and copies ran while one was open for 12% of the time, Pallas kernels for 13%

profile of v1, /device:TPU:8, one launch (start us, length us, event | category | flops | bytes accessed | tf_op | source)
XLA Modules:
  0.0 270.0 jit_solution(7319374693050017637)
XLA Ops:
  2.3 3.0 %fusion.82 = (bf16[2048,256]{1,0:T(8,128)(2,1)}, bf16[2048,256]{1,0:T(8,128)(2,1)}) fusion(bf16[2048,512]{1,0:T(8,128)(2,1)} %bitcast.73), kind=kLoop, calls=%fused_computation.127 | loop fusion | bytes 4194304 | tf_op jit(solution)/shard_map/slice | solution.py:297
  7.7 12.3 %all-to-all-start = ((bf16[64,8,2048]{2,1,0:T(8,128)(2,1)}), bf16[64,8,2048]{2,1,0:T(8,128)(2,1)}, u32[]{:S(2)}, u32[]{:S(2)}) async-start(bf16[64,8,2048]{2,1,0:T(8,128)(2,1)} %fusion), calls=%async_computation | async-start | bytes 4194304 | tf_op jit(solution)/shard_map/all_to_all | solution.py:307
  20.0 2.8 %collective-permute-start.1 = (bf16[2048,256]{1,0:T(8,128)(2,1)}, bf16[2048,256]{1,0:T(8,128)(2,1)S(1)}, u32[]{:S(2)}, u32[]{:S(2)}) collective-permute-start(bf16[2048,256]{1,0:T(8,128)(2,1)} %get-tuple-element.30), channel_id=1, source_target_pairs={{0,3},{1,0},{2,1},{3,2},{4,7},{5,4},{6,5},{7,6},{8,11},{9,8},{10,9... | collective-permute-start | bytes 3145736 | tf_op jit(solution)/shard_map/ppermute | solution.py:190
  22.8 3.2 %fusion.81 = (bf16[2048,256]{1,0:T(8,128)(2,1)}, bf16[2048,256]{1,0:T(8,128)(2,1)}) fusion(bf16[2048,512]{1,0:T(8,128)(2,1)} %bitcast.78), kind=kLoop, calls=%fused_computation.126 | loop fusion | bytes 4194304 | tf_op jit(solution)/shard_map/slice | solution.py:297
  26.8 2.6 collective-permute-start.3
  33.8 12.9 %collective-permute-done.1.gate_right = bf16[2048,256]{1,0:T(8,128)(2,1)S(1)} collective-permute-done((bf16[2048,256]{1,0:T(8,128)(2,1)}, bf16[2048,256]{1,0:T(8,128)(2,1)S(1)}, u32[]{:S(2)}, u32[]{:S(2)}) %collective-permute-start.1) | collective-permute-done | bytes 1048608 | tf_op jit(solution)/shard_map/ppermute | solution.py:190
  51.9 6.1 %shard_map.167 = (f32[1024,256]{1,0:T(8,128)S(1)}, bf16[1024,256]{1,0:T(8,128)(2,1)S(1)}, f32[256,256]{1,0:T(8,128)S(1)}) custom-call(bf16[1024,256]{1,0:T(8,128)(2,1)S(1)} %copy-done.16, bf16[1024,256]{1,0:T(8,128)(2,1)S(1)} %copy-done.17, bf16[1024,256]{1,0:T(8,128)(2,1)S(1)} %copy-done.18, f32[1,256]{1,0:T(1,128)S(1)} %bitcast.88, f32[1024,2]{1,0:T(8,128)S(1)} %copy-done.13), custom_call_target="tpu_custom_call" | custom-call | flops 4000000000 | bytes 6291456 | tf_op jit(solution)/shard_map/pallas_call | solution.py:154
  60.6 10.5 %all-to-all-done = bf16[64,8,2048]{2,1,0:T(8,128)(2,1)} async-done(((bf16[64,8,2048]{2,1,0:T(8,128)(2,1)}), bf16[64,8,2048]{2,1,0:T(8,128)(2,1)}, u32[]{:S(2)}, u32[]{:S(2)}) %all-to-all-start) | async-done | bytes 2097184 | tf_op jit(solution)/shard_map/all_to_all | solution.py:307
  71.1 5.4 %all-to-all-start.1 = ((f32[64,4,256]{2,1,0:T(4,128)}), f32[64,4,256]{2,1,0:T(4,128)S(1)}, u32[]{:S(2)}, u32[]{:S(2)}) async-start(f32[64,4,256]{2,1,0:T(4,128)} %reshape.230), calls=%async_computation.1 | async-start | bytes 524288 | tf_op jit(solution)/shard_map/all_to_all | solution.py:307
  78.3 3.1 %collective-permute-start.11 = (bf16[128,2048]{1,0:T(8,128)(2,1)S(1)}, bf16[128,2048]{1,0:T(8,128)(2,1)S(1)}, u32[]{:S(2)}, u32[]{:S(2)}) collective-permute-start(bf16[128,2048]{1,0:T(8,128)(2,1)S(1)} %convolution_convert_fusion.2.own_ref), channel_id=1, source_target_pairs={{0,2},{1,3},{2,0},{3,1},{4,6},{5,7},{6,4},{7,5},{8,10},{9,11},{10,... | collective-permute-start | bytes 1572872 | tf_op jit(solution)/shard_map/ppermute | solution.py:190
  83.8 2.4 convolution_convert_fusion.4.own_ref
  86.2 27.1 %collective-permute-done.5.down_right = bf16[256,2048]{1,0:T(8,128)(2,1)} collective-permute-done((bf16[256,2048]{1,0:T(8,128)(2,1)}, bf16[256,2048]{1,0:T(8,128)(2,1)}, u32[]{:S(2)}, u32[]{:S(2)}) %collective-permute-start.5) | collective-permute-done | bytes 1048608 | tf_op jit(solution)/shard_map/ppermute | solution.py:190
  113.3 9.0 %collective-permute-done.6.down_left = bf16[256,2048]{1,0:T(8,128)(2,1)} collective-permute-done((bf16[256,2048]{1,0:T(8,128)(2,1)}, bf16[256,2048]{1,0:T(8,128)(2,1)}, u32[]{:S(2)}, u32[]{:S(2)}) %collective-permute-start.6) | collective-permute-done | bytes 1048608 | tf_op jit(solution)/shard_map/ppermute | solution.py:190
  123.9 6.9 %expert_block.6 = (bf16[128,2048]{1,0:T(8,128)(2,1)S(1)}, bf16[128,2048]{1,0:T(8,128)(2,1)}) custom-call(bf16[128,2048]{1,0:T(8,128)(2,1)S(1)} %convolution_convert_fusion.2.own_ref, bf16[128,2048]{1,0:T(8,128)(2,1)S(1)} %collective-permute-done.11.far_ref, bf16[2048,512]{1,0:T(8,128)(2,1)S(1)} %bitcast.74, ...), custom_call_target="tpu_custom_call" | custom-call | flops 3221225472 | bytes 14680064 | tf_op jit(solution)/shard_map/expert_block/pallas_call | solution.py:270
  130.8 6.9 %expert_block.4 = (bf16[128,2048]{1,0:T(8,128)(2,1)S(1)}, bf16[128,2048]{1,0:T(8,128)(2,1)}) custom-call(bf16[128,2048]{1,0:T(8,128)(2,1)S(1)} %convolution_convert_fusion.3.own_ref, bf16[128,2048]{1,0:T(8,128)(2,1)S(1)} %collective-permute-done.far_ref, bf16[2048,512]{1,0:T(8,128)(2,1)S(1)} %bitcast.75, ...), custom_call_target="tpu_custom_call" | custom-call | flops 3221225472 | bytes 14680064 | tf_op jit(solution)/shard_map/expert_block/pallas_call | solution.py:270
  137.7 3.6 %collective-permute-start.13 = (bf16[128,2048]{1,0:T(8,128)(2,1)}, bf16[128,2048]{1,0:T(8,128)(2,1)}, u32[]{:S(2)}, u32[]{:S(2)}) collective-permute-start(bf16[128,2048]{1,0:T(8,128)(2,1)} %get-tuple-element.45), channel_id=1, source_target_pairs={{0,2},{1,3},{2,0},{3,1},{4,6},{5,7},{6,4},{7,5},{8,10},{9,11},{10,... | collective-permute-start | bytes 1572872 | tf_op jit(solution)/shard_map/ppermute | solution.py:190
  141.3 2.4 convolution_convert_fusion.1.own_ref
  144.6 10.3 %all-to-all-start.2 = ((bf16[64,4,128]{2,1,0:T(4,128)(2,1)}), bf16[64,4,128]{2,1,0:T(4,128)(2,1)S(1)}, u32[]{:S(2)}, u32[]{:S(2)}) async-start(bf16[64,4,128]{2,1,0:T(4,128)(2,1)} %convert_element_type.108), calls=%async_computation.2 | async-start | bytes 131072 | tf_op jit(solution)/shard_map/all_to_all | solution.py:307
  154.9 3.5 %collective-permute-start.7 = (bf16[128,2048]{1,0:T(8,128)(2,1)}, bf16[128,2048]{1,0:T(8,128)(2,1)}, u32[]{:S(2)}, u32[]{:S(2)}) collective-permute-start(bf16[128,2048]{1,0:T(8,128)(2,1)} %convolution_convert_fusion.4.own_ref), channel_id=1, source_target_pairs={{0,2},{1,3},{2,0},{3,1},{4,6},{5,7},{6,4},{7,5},{8,10},{9,11},{10,... | collective-permute-start | bytes 1572872 | tf_op jit(solution)/shard_map/ppermute | solution.py:190
  164.5 10.5 %all-to-all-start.3 = ((bf16[64,4,2048]{2,1,0:T(4,128)(2,1)}), bf16[64,4,2048]{2,1,0:T(4,128)(2,1)}, u32[]{:S(2)}, u32[]{:S(2)}) async-start(bf16[64,4,2048]{2,1,0:T(4,128)(2,1)} %reshape.235), calls=%async_computation.3 | async-start | bytes 2097152 | tf_op jit(solution)/shard_map/all_to_all | solution.py:307
  179.8 7.4 %expert_block.7 = (bf16[128,2048]{1,0:T(8,128)(2,1)S(1)}, bf16[128,2048]{1,0:T(8,128)(2,1)S(1)}) custom-call(bf16[128,2048]{1,0:T(8,128)(2,1)} %convolution_convert_fusion.1.own_ref, bf16[128,2048]{1,0:T(8,128)(2,1)} %collective-permute-done.14.far_ref, bf16[2048,512]{1,0:T(8,128)(2,1)S(1)} %bitcast.76, ...), custom_call_target="tpu_custom_call" | custom-call | flops 3221225472 | bytes 14680064 | tf_op jit(solution)/shard_map/expert_block/pallas_call | solution.py:270
  189.9 7.1 %expert_block.5 = (bf16[128,2048]{1,0:T(8,128)(2,1)S(1)}, bf16[128,2048]{1,0:T(8,128)(2,1)S(1)}) custom-call(bf16[128,2048]{1,0:T(8,128)(2,1)S(1)} %copy-done.10, bf16[128,2048]{1,0:T(8,128)(2,1)} %collective-permute-done.7.far_ref, bf16[2048,512]{1,0:T(8,128)(2,1)S(1)} %bitcast.77, bf16[2048,256]{1,0:T(8,128)(2,1)S(1)} %collective-permute-done.1.gate_right, ...), custom_call_target="tpu_custom_call" | custom-call | flops 3221225472 | bytes 14680064 | tf_op jit(solution)/shard_map/expert_block/pallas_call | solution.py:270
  197.0 3.7 %collective-permute-start.16 = (bf16[128,2048]{1,0:T(8,128)(2,1)S(1)}, bf16[128,2048]{1,0:T(8,128)(2,1)S(1)}, u32[]{:S(2)}, u32[]{:S(2)}) collective-permute-start(bf16[128,2048]{1,0:T(8,128)(2,1)S(1)} %get-tuple-element.49), channel_id=1, source_target_pairs={{0,2},{1,3},{2,0},{3,1},{4,6},{5,7},{6,4},{7,5},{8,10},{9,11},{10,... | collective-permute-start | bytes 1572872 | tf_op jit(solution)/shard_map/ppermute | solution.py:190
  200.8 2.9 %collective-permute-done.15 = bf16[128,2048]{1,0:T(8,128)(2,1)S(1)} collective-permute-done((bf16[128,2048]{1,0:T(8,128)(2,1)S(1)}, bf16[128,2048]{1,0:T(8,128)(2,1)S(1)}, u32[]{:S(2)}, u32[]{:S(2)}) %collective-permute-start.15) | collective-permute-done | bytes 524320 | tf_op jit(solution)/shard_map/ppermute | solution.py:190
  203.7 10.3 %collective-permute-done.16 = bf16[128,2048]{1,0:T(8,128)(2,1)S(1)} collective-permute-done((bf16[128,2048]{1,0:T(8,128)(2,1)S(1)}, bf16[128,2048]{1,0:T(8,128)(2,1)S(1)}, u32[]{:S(2)}, u32[]{:S(2)}) %collective-permute-start.16) | collective-permute-done | bytes 524320 | tf_op jit(solution)/shard_map/ppermute | solution.py:190
  217.5 10.5 %all-to-all-start.4 = ((bf16[64,4,2048]{2,1,0:T(4,128)(2,1)}), bf16[64,4,2048]{2,1,0:T(4,128)(2,1)}, u32[]{:S(2)}, u32[]{:S(2)}) async-start(bf16[64,4,2048]{2,1,0:T(4,128)(2,1)} %reshape.236), calls=%async_computation.4 | async-start | bytes 2097152 | tf_op jit(solution)/shard_map/all_to_all | solution.py:307
  230.8 2.6 collective-permute-start.9
  234.8 20.4 %collective-permute-done.8 = bf16[1024,256]{1,0:T(8,128)(2,1)} collective-permute-done((bf16[1024,256]{1,0:T(8,128)(2,1)S(1)}, bf16[1024,256]{1,0:T(8,128)(2,1)}, u32[]{:S(2)}, u32[]{:S(2)}) %collective-permute-start.8) | collective-permute-done | bytes 524320 | tf_op jit(solution)/shard_map/ppermute | solution.py:190
  258.6 2.5 convolution_bitcast_fusion.2
  261.2 2.6 convolution_bitcast_fusion
  263.7 2.6 convolution_bitcast_fusion.1
  266.3 2.7 %multiply_reduce_fusion = (f32[128]{0:T(128)S(1)}, f32[128,2048]{1,0:T(8,128)S(1)}) fusion(f32[128,2048]{1,0:T(8,128)S(1)} %convolution_bitcast_fusion, f32[128,2048]{1,0:T(8,128)S(1)} %convolution_bitcast_fusion.1, f32[128,2048]{1,0:T(8,128)S(1)} %convolution_bitcast_fusion.2, bf16[64,4,2048]{2,1,0:T(4,128)(2,1)} %all-to-all-done.3, ...), kind=kOutput, calls=%fused_computation.27 | convolution fusion | flops 135626624 | bytes 5317120 | tf_op jit(solution)/shard_map/dot_general | solution.py:418
  (123 shorter events, 49.3 us)
Async XLA Ops:
  7.7 63.5 %all-to-all-start = ((bf16[64,8,2048]{2,1,0:T(8,128)(2,1)}), bf16[64,8,2048]{2,1,0:T(8,128)(2,1)}, u32[]{:S(2)}, u32[]{:S(2)}) async-start(bf16[64,8,2048]{2,1,0:T(8,128)(2,1)} %fusion), calls=%async_computation | async-start | bytes 4194304 | tf_op jit(solution)/shard_map/all_to_all | solution.py:307
  20.0 26.7 %collective-permute-start.1 = (bf16[2048,256]{1,0:T(8,128)(2,1)}, bf16[2048,256]{1,0:T(8,128)(2,1)S(1)}, u32[]{:S(2)}, u32[]{:S(2)}) collective-permute-start(bf16[2048,256]{1,0:T(8,128)(2,1)} %get-tuple-element.30), channel_id=1, source_target_pairs={{0,3},{1,0},{2,1},{3,2},{4,7},{5,4},{6,5},{7,6},{8,11},{9,8},{10,9... | collective-permute-start | bytes 3145736 | tf_op jit(solution)/shard_map/ppermute | solution.py:190
  22.8 55.5 %collective-permute-start.2 = (bf16[2048,256]{1,0:T(8,128)(2,1)}, bf16[2048,256]{1,0:T(8,128)(2,1)}, u32[]{:S(2)}, u32[]{:S(2)}) collective-permute-start(bf16[2048,256]{1,0:T(8,128)(2,1)} %get-tuple-element.31), channel_id=1, source_target_pairs={{0,1},{1,2},{2,3},{3,0},{4,5},{5,6},{6,7},{7,4},{8,9},{9,10},{10,1... | collective-permute-start | bytes 3145736 | tf_op jit(solution)/shard_map/ppermute | solution.py:190
  26.0 57.0 %collective-permute-start.4 = (bf16[2048,256]{1,0:T(8,128)(2,1)}, bf16[2048,256]{1,0:T(8,128)(2,1)}, u32[]{:S(2)}, u32[]{:S(2)}) collective-permute-start(bf16[2048,256]{1,0:T(8,128)(2,1)} %get-tuple-element.50), channel_id=1, source_target_pairs={{0,1},{1,2},{2,3},{3,0},{4,5},{5,6},{6,7},{7,4},{8,9},{9,10},{10,1... | collective-permute-start | bytes 3145736 | tf_op jit(solution)/shard_map/ppermute | solution.py:190
  26.8 21.0 %copy-start.20 = (f32[256]{0:T(256)S(1)}, f32[256]{0:T(256)}, u32[]{:S(2)}) copy-start(f32[256]{0:T(256)} %param.20) | copy-start | bytes 3076
  26.8 59.4 %collective-permute-start.3 = (bf16[2048,256]{1,0:T(8,128)(2,1)}, bf16[2048,256]{1,0:T(8,128)(2,1)}, u32[]{:S(2)}, u32[]{:S(2)}) collective-permute-start(bf16[2048,256]{1,0:T(8,128)(2,1)} %get-tuple-element.51), channel_id=1, source_target_pairs={{0,3},{1,0},{2,1},{3,2},{4,7},{5,4},{6,5},{7,6},{8,11},{9,8},{10,9... | collective-permute-start | bytes 3145736 | tf_op jit(solution)/shard_map/ppermute | solution.py:190
  30.8 82.4 %collective-permute-start.5 = (bf16[256,2048]{1,0:T(8,128)(2,1)}, bf16[256,2048]{1,0:T(8,128)(2,1)}, u32[]{:S(2)}, u32[]{:S(2)}) collective-permute-start(bf16[256,2048]{1,0:T(8,128)(2,1)} %get-tuple-element.32), channel_id=1, source_target_pairs={{0,3},{1,0},{2,1},{3,2},{4,7},{5,4},{6,5},{7,6},{8,11},{9,8},{10,9... | collective-permute-start | bytes 3145736 | tf_op jit(solution)/shard_map/ppermute | solution.py:190
  46.7 75.6 %collective-permute-start.6 = (bf16[256,2048]{1,0:T(8,128)(2,1)}, bf16[256,2048]{1,0:T(8,128)(2,1)}, u32[]{:S(2)}, u32[]{:S(2)}) collective-permute-start(bf16[256,2048]{1,0:T(8,128)(2,1)} %get-tuple-element.33), channel_id=1, source_target_pairs={{0,1},{1,2},{2,3},{3,0},{4,5},{5,6},{6,7},{7,4},{8,9},{9,10},{10,1... | collective-permute-start | bytes 3145736 | tf_op jit(solution)/shard_map/ppermute | solution.py:190
  71.1 72.7 %all-to-all-start.1 = ((f32[64,4,256]{2,1,0:T(4,128)}), f32[64,4,256]{2,1,0:T(4,128)S(1)}, u32[]{:S(2)}, u32[]{:S(2)}) async-start(f32[64,4,256]{2,1,0:T(4,128)} %reshape.230), calls=%async_computation.1 | async-start | bytes 524288 | tf_op jit(solution)/shard_map/all_to_all | solution.py:307
  76.6 45.7 %copy-start.1 = (bf16[1,2048,512]{2,1,0:T(8,128)(2,1)S(1)}, bf16[1,2048,512]{2,1,0:T(8,128)(2,1)}, u32[]{:S(2)}) copy-start(bf16[1,2048,512]{2,1,0:T(8,128)(2,1)} %param.29) | copy-start | bytes 6291460
  76.6 45.7 %copy-start.4 = (bf16[1,2048,512]{2,1,0:T(8,128)(2,1)S(1)}, bf16[1,2048,512]{2,1,0:T(8,128)(2,1)}, u32[]{:S(2)}) copy-start(bf16[1,2048,512]{2,1,0:T(8,128)(2,1)} %param.30) | copy-start | bytes 6291460
  78.3 43.9 %collective-permute-start.11 = (bf16[128,2048]{1,0:T(8,128)(2,1)S(1)}, bf16[128,2048]{1,0:T(8,128)(2,1)S(1)}, u32[]{:S(2)}, u32[]{:S(2)}) collective-permute-start(bf16[128,2048]{1,0:T(8,128)(2,1)S(1)} %convolution_convert_fusion.2.own_ref), channel_id=1, source_target_pairs={{0,2},{1,3},{2,0},{3,1},{4,6},{5,7},{6,4},{7,5},{8,10},{9,11},{10,... | collective-permute-start | bytes 1572872 | tf_op jit(solution)/shard_map/ppermute | solution.py:190
  83.0 47.8 %collective-permute-start = (bf16[128,2048]{1,0:T(8,128)(2,1)S(1)}, bf16[128,2048]{1,0:T(8,128)(2,1)S(1)}, u32[]{:S(2)}, u32[]{:S(2)}) collective-permute-start(bf16[128,2048]{1,0:T(8,128)(2,1)S(1)} %convolution_convert_fusion.3.own_ref), channel_id=1, source_target_pairs={{0,2},{1,3},{2,0},{3,1},{4,6},{5,7},{6,4},{7,5},{8,10},{9,11},{10,... | collective-permute-start | bytes 1572872 | tf_op jit(solution)/shard_map/ppermute | solution.py:190
  130.7 7.0 %copy-start.11 = (bf16[128,2048]{1,0:T(8,128)(2,1)}, bf16[128,2048]{1,0:T(8,128)(2,1)S(1)}, u32[]{:S(2)}) copy-start(bf16[128,2048]{1,0:T(8,128)(2,1)S(1)} %get-tuple-element.42) | copy-start | bytes 1572868
  130.7 27.7 %collective-permute-start.12 = (bf16[128,2048]{1,0:T(8,128)(2,1)}, bf16[128,2048]{1,0:T(8,128)(2,1)}, u32[]{:S(2)}, u32[]{:S(2)}) collective-permute-start(bf16[128,2048]{1,0:T(8,128)(2,1)} %get-tuple-element.43), channel_id=1, source_target_pairs={{0,2},{1,3},{2,0},{3,1},{4,6},{5,7},{6,4},{7,5},{8,10},{9,11},{10,... | collective-permute-start | bytes 1572872 | tf_op jit(solution)/shard_map/ppermute | solution.py:190
  137.7 22.0 %collective-permute-start.13 = (bf16[128,2048]{1,0:T(8,128)(2,1)}, bf16[128,2048]{1,0:T(8,128)(2,1)}, u32[]{:S(2)}, u32[]{:S(2)}) collective-permute-start(bf16[128,2048]{1,0:T(8,128)(2,1)} %get-tuple-element.45), channel_id=1, source_target_pairs={{0,2},{1,3},{2,0},{3,1},{4,6},{5,7},{6,4},{7,5},{8,10},{9,11},{10,... | collective-permute-start | bytes 1572872 | tf_op jit(solution)/shard_map/ppermute | solution.py:190
  143.7 31.3 %collective-permute-start.14 = (bf16[128,2048]{1,0:T(8,128)(2,1)}, bf16[128,2048]{1,0:T(8,128)(2,1)}, u32[]{:S(2)}, u32[]{:S(2)}) collective-permute-start(bf16[128,2048]{1,0:T(8,128)(2,1)} %convolution_convert_fusion.1.own_ref), channel_id=1, source_target_pairs={{0,2},{1,3},{2,0},{3,1},{4,6},{5,7},{6,4},{7,5},{8,10},{9,11},{10,... | collective-permute-start | bytes 1572872 | tf_op jit(solution)/shard_map/ppermute | solution.py:190
  144.6 19.9 %all-to-all-start.2 = ((bf16[64,4,128]{2,1,0:T(4,128)(2,1)}), bf16[64,4,128]{2,1,0:T(4,128)(2,1)S(1)}, u32[]{:S(2)}, u32[]{:S(2)}) async-start(bf16[64,4,128]{2,1,0:T(4,128)(2,1)} %convert_element_type.108), calls=%async_computation.2 | async-start | bytes 131072 | tf_op jit(solution)/shard_map/all_to_all | solution.py:307
  154.9 34.6 %collective-permute-start.7 = (bf16[128,2048]{1,0:T(8,128)(2,1)}, bf16[128,2048]{1,0:T(8,128)(2,1)}, u32[]{:S(2)}, u32[]{:S(2)}) collective-permute-start(bf16[128,2048]{1,0:T(8,128)(2,1)} %convolution_convert_fusion.4.own_ref), channel_id=1, source_target_pairs={{0,2},{1,3},{2,0},{3,1},{4,6},{5,7},{6,4},{7,5},{8,10},{9,11},{10,... | collective-permute-start | bytes 1572872 | tf_op jit(solution)/shard_map/ppermute | solution.py:190
  164.5 53.0 %all-to-all-start.3 = ((bf16[64,4,2048]{2,1,0:T(4,128)(2,1)}), bf16[64,4,2048]{2,1,0:T(4,128)(2,1)}, u32[]{:S(2)}, u32[]{:S(2)}) async-start(bf16[64,4,2048]{2,1,0:T(4,128)(2,1)} %reshape.235), calls=%async_computation.3 | async-start | bytes 2097152 | tf_op jit(solution)/shard_map/all_to_all | solution.py:307
  179.8 7.6 %copy-start.19 = (bf16[1024,256]{1,0:T(8,128)(2,1)S(1)}, bf16[1024,256]{1,0:T(8,128)(2,1)}, u32[]{:S(2)}) copy-start(bf16[1024,256]{1,0:T(8,128)(2,1)} %gate_ref.1) | copy-start | bytes 1572868
  179.8 7.6 %copy-start.21 = (f32[256]{0:T(256)S(1)}, f32[256]{0:T(256)}, u32[]{:S(2)}) copy-start(f32[256]{0:T(256)} %param.22) | copy-start | bytes 3076
  179.8 7.6 %copy-start.23 = (f32[1024,256]{1,0:T(8,128)S(1)}, f32[1024,256]{1,0:T(8,128)}, u32[]{:S(2)}) copy-start(f32[1024,256]{1,0:T(8,128)} %copy-done.22) | copy-start | bytes 3145732
  179.8 7.6 %copy-start.25 = (bf16[1024,256]{1,0:T(8,128)(2,1)S(1)}, bf16[1024,256]{1,0:T(8,128)(2,1)}, u32[]{:S(2)}) copy-start(bf16[1024,256]{1,0:T(8,128)(2,1)} %copy-done.24) | copy-start | bytes 1572868
  187.2 16.4 %collective-permute-start.15 = (bf16[128,2048]{1,0:T(8,128)(2,1)S(1)}, bf16[128,2048]{1,0:T(8,128)(2,1)S(1)}, u32[]{:S(2)}, u32[]{:S(2)}) collective-permute-start(bf16[128,2048]{1,0:T(8,128)(2,1)S(1)} %get-tuple-element.47), channel_id=1, source_target_pairs={{0,2},{1,3},{2,0},{3,1},{4,6},{5,7},{6,4},{7,5},{8,10},{9,11},{10,... | collective-permute-start | bytes 1572872 | tf_op jit(solution)/shard_map/ppermute | solution.py:190
  197.0 17.0 %collective-permute-start.16 = (bf16[128,2048]{1,0:T(8,128)(2,1)S(1)}, bf16[128,2048]{1,0:T(8,128)(2,1)S(1)}, u32[]{:S(2)}, u32[]{:S(2)}) collective-permute-start(bf16[128,2048]{1,0:T(8,128)(2,1)S(1)} %get-tuple-element.49), channel_id=1, source_target_pairs={{0,2},{1,3},{2,0},{3,1},{4,6},{5,7},{6,4},{7,5},{8,10},{9,11},{10,... | collective-permute-start | bytes 1572872 | tf_op jit(solution)/shard_map/ppermute | solution.py:190
  215.2 13.5 %copy-start.15 = (bf16[1024,256]{1,0:T(8,128)(2,1)S(1)}, bf16[1024,256]{1,0:T(8,128)(2,1)}, u32[]{:S(2)}) copy-start(bf16[1024,256]{1,0:T(8,128)(2,1)} %copy-done.14) | copy-start | bytes 1572868
  217.5 43.6 %all-to-all-start.4 = ((bf16[64,4,2048]{2,1,0:T(4,128)(2,1)}), bf16[64,4,2048]{2,1,0:T(4,128)(2,1)}, u32[]{:S(2)}, u32[]{:S(2)}) async-start(bf16[64,4,2048]{2,1,0:T(4,128)(2,1)} %reshape.236), calls=%async_computation.4 | async-start | bytes 2097152 | tf_op jit(solution)/shard_map/all_to_all | solution.py:307
  228.7 26.5 %collective-permute-start.8 = (bf16[1024,256]{1,0:T(8,128)(2,1)S(1)}, bf16[1024,256]{1,0:T(8,128)(2,1)}, u32[]{:S(2)}, u32[]{:S(2)}) collective-permute-start(bf16[1024,256]{1,0:T(8,128)(2,1)S(1)} %copy-done.15), channel_id=1, source_target_pairs={{0,1},{1,2},{2,3},{3,0},{4,5},{5,6},{6,7},{7,4},{8,9},{9,10},{10,1... | collective-permute-start | bytes 1572872 | tf_op jit(solution)/shard_map/ppermute | solution.py:190
  228.8 26.5 %copy-start.26 = (bf16[1024,512]{1,0:T(8,128)(2,1)S(1)}, bf16[1024,512]{1,0:T(8,128)(2,1)}, u32[]{:S(2)}) copy-start(bf16[1024,512]{1,0:T(8,128)(2,1)} %param.23) | copy-start | bytes 3145732
  228.8 28.4 %collective-permute-start.10 = (bf16[1024,256]{1,0:T(8,128)(2,1)S(1)}, bf16[1024,256]{1,0:T(8,128)(2,1)S(1)}, u32[]{:S(2)}, u32[]{:S(2)}) collective-permute-start(bf16[1024,256]{1,0:T(8,128)(2,1)S(1)} %copy-done.15), channel_id=1, source_target_pairs={{0,2},{1,3},{2,0},{3,1},{4,6},{5,7},{6,4},{7,5},{8,10},{9,11},{10,... | collective-permute-start | bytes 1572872 | tf_op jit(solution)/shard_map/ppermute | solution.py:190
  230.8 25.9 %collective-permute-start.9 = (bf16[1024,256]{1,0:T(8,128)(2,1)S(1)}, bf16[1024,256]{1,0:T(8,128)(2,1)S(1)}, u32[]{:S(2)}, u32[]{:S(2)}) collective-permute-start(bf16[1024,256]{1,0:T(8,128)(2,1)S(1)} %copy-done.15), channel_id=1, source_target_pairs={{0,3},{1,0},{2,1},{3,2},{4,7},{5,4},{6,5},{7,6},{8,11},{9,8},{10,9... | collective-permute-start | bytes 1572872 | tf_op jit(solution)/shard_map/ppermute | solution.py:190
  (20 other events, 45.9 us)

commit v2 on v1

--- a/solution.py
+++ b/solution.py
@@ -14,8 +14,6 @@
 EP = ("ep_0", "ep_1", "ep_2")
 EP_TP = ("ep_0", "ep_1", "ep_2", "tp")
 GROUPS = 2
-EXPERT_VMEM = 24 << 20
-SMALL_VMEM = 12 << 20
 CHUNKS = 2
 
 
@@ -113,7 +111,7 @@
 def prefix_kernel(x_ref, out_ref):
     state = jnp.zeros(out_ref.shape[1:], F32)
     for i in range(x_ref.shape[0]):
-        out_ref[i] = state
+        out_ref[i] = state.astype(BF16)
         state = x_ref[i, :, HEAD:] * state + x_ref[i, :, :HEAD]
 
 
@@ -142,7 +140,6 @@
     return pl.pallas_call(
         kernel,
         out_shape=outs,
-        compiler_params=pltpu.CompilerParams(vmem_limit_bytes=SMALL_VMEM),
         cost_estimate=pl.CostEstimate(
             flops=flops, bytes_accessed=bytes_accessed, transcendentals=transcendentals
         ),
@@ -167,7 +164,7 @@
 def prefix_pass(x):
     return vmem_call(
         prefix_kernel,
-        jax.ShapeDtypeStruct((x.shape[0], x.shape[1], HEAD), F32),
+        jax.ShapeDtypeStruct((x.shape[0], x.shape[1], HEAD), BF16),
         100_000_000,
         1 << 19,
         0,
@@ -191,8 +188,8 @@
 
 
 def expert_kernel(
-    own_ref,
-    far_ref,
+    own,
+    far,
     gate_own,
     gate_right,
     gate_left,
@@ -202,85 +199,118 @@
     down_own,
     down_right,
     down_left,
-    out_own_ref,
-    out_far_ref,
+    out_own,
+    out_far,
     rows,
+    gate_w,
+    up_w,
+    down_w,
     hidden,
-    gate_more,
-    up_more,
-    down_more,
+    out,
     sems,
+    out_sems,
 ):
-    n = own_ref.shape[0]
+    n = own.shape[0]
     tile = gate_right.shape[1]
-    first, second = slice(0, tile), slice(tile, 2 * tile)
+    wide = 512
+    tiles = gate_w.shape[1] // tile
+
+    def columns(owned, right, left):
+        return [owned.at[:, pl.ds(0, tile)], owned.at[:, pl.ds(tile, tile)], right, left]
+
+    gates = columns(gate_own, gate_right, gate_left)
+    ups = columns(up_own, up_right, up_left)
+    downs = [down_own.at[pl.ds(0, tile), :], down_own.at[pl.ds(tile, tile), :]]
+    downs += [down_right, down_left]
+    places = [pl.ds(f * tile, tile) for f in range(tiles)]
     loads = [
-        pltpu.make_async_copy(gate_right, gate_more.at[:, first], sems.at[0]),
-        pltpu.make_async_copy(gate_left, gate_more.at[:, second], sems.at[1]),
-        pltpu.make_async_copy(up_right, up_more.at[:, first], sems.at[2]),
-        pltpu.make_async_copy(up_left, up_more.at[:, second], sems.at[3]),
-        pltpu.make_async_copy(down_right, down_more.at[first, :], sems.at[4]),
-        pltpu.make_async_copy(down_left, down_more.at[second, :], sems.at[5]),
+        pltpu.make_async_copy(own, rows.at[pl.ds(0, n), :], sems.at[0]),
+        pltpu.make_async_copy(far, rows.at[pl.ds(n, n), :], sems.at[1]),
     ]
+    for f in range(tiles):
+        loads.append(pltpu.make_async_copy(gates[f], gate_w.at[:, places[f]], sems.at[2 + 2 * f]))
+        loads.append(pltpu.make_async_copy(ups[f], up_w.at[:, places[f]], sems.at[3 + 2 * f]))
+    for f in range(tiles):
+        to = down_w.at[places[f], :]
+        loads.append(pltpu.make_async_copy(downs[f], to, sems.at[2 + 2 * tiles + f]))
     for load in loads:
         load.start()
-    rows[:n, :] = own_ref[...]
-    rows[n:, :] = far_ref[...]
-
-    def hidden_tiles(gate_w, up_w, offset):
-        def step(f, carry):
-            at = pl.ds(pl.multiple_of(f * tile, tile), tile)
-            to = pl.ds(pl.multiple_of(f * tile + offset, tile), tile)
-            gate = jnp.dot(rows[...], gate_w[:, at], preferred_element_type=F32)
-            upward = jnp.dot(rows[...], up_w[:, at], preferred_element_type=F32)
-            glued = jnp.minimum(gate, CLAMP_LIMIT)
-            linear = jnp.clip(upward, -CLAMP_LIMIT, CLAMP_LIMIT)
-            act = glued / (1.0 + jnp.exp(-SWISH_ALPHA * glued)) * (linear + 1.0)
-            hidden[:, to] = act.astype(BF16)
-            return carry
-
-        lax.fori_loop(0, 2, step, 0)
-
-    hidden_tiles(gate_own, up_own, 0)
-    for load in loads[:4]:
+    loads[0].wait()
+    loads[1].wait()
+
+    def hidden_tile(f, carry):
+        for k in range(tiles):
+
+            @pl.when(f == k)
+            def _():
+                loads[2 + 2 * k].wait()
+                loads[3 + 2 * k].wait()
+
+        at = pl.ds(pl.multiple_of(f * tile, tile), tile)
+        gate = jnp.dot(rows[...], gate_w[:, at], preferred_element_type=F32)
+        upward = jnp.dot(rows[...], up_w[:, at], preferred_element_type=F32)
+        glued = jnp.minimum(gate, CLAMP_LIMIT)
+        linear = jnp.clip(upward, -CLAMP_LIMIT, CLAMP_LIMIT)
+        act = glued / (1.0 + jnp.exp(-SWISH_ALPHA * glued)) * (linear + 1.0)
+        hidden[:, at] = act.astype(BF16)
+        return carry
+
+    lax.fori_loop(0, tiles, hidden_tile, 0)
+    for load in loads[2 + 2 * tiles :]:
         load.wait()
-    hidden_tiles(gate_more, up_more, 2 * tile)
-    for load in loads[4:]:
-        load.wait()
+
+    stores = []
+    for t in range(out.shape[1] // wide):
+        at = pl.ds(t * wide, wide)
+        stores.append(
+            (
+                pltpu.make_async_copy(
+                    out.at[pl.ds(0, n), at], out_own.at[:, at], out_sems.at[2 * t]
+                ),
+                pltpu.make_async_copy(
+                    out.at[pl.ds(n, n), at], out_far.at[:, at], out_sems.at[2 * t + 1]
+                ),
+            )
+        )
 
     def out_tile(t, carry):
-        at = pl.ds(pl.multiple_of(t * 256, 256), 256)
-        part = (
-            jnp.dot(hidden[:, : 2 * tile], down_own[:, at], preferred_element_type=F32)
-            + jnp.dot(hidden[:, 2 * tile :], down_more[:, at], preferred_element_type=F32)
-        ).astype(BF16)
-        out_own_ref[:, at] = part[:n]
-        out_far_ref[:, at] = part[n:]
+        at = pl.ds(pl.multiple_of(t * wide, wide), wide)
+        part = jnp.dot(hidden[...], down_w[:, at], preferred_element_type=F32)
+        out[:, at] = part.astype(BF16)
+        for k, pair in enumerate(stores):
+
+            @pl.when(t == k)
+            def _():
+                for store in pair:
+                    store.start()
+
         return carry
 
-    lax.fori_loop(0, down_own.shape[1] // 256, out_tile, 0)
+    lax.fori_loop(0, len(stores), out_tile, 0)
+    for pair in stores:
+        for store in pair:
+            store.wait()
 
 
 def expert_block(own, far, gates, ups, downs):
     n, features = own.shape
     units = sum(w.shape[1] for w in gates)
-    vmem = pl.BlockSpec(memory_space=pltpu.VMEM)
     hbm = pl.BlockSpec(memory_space=pltpu.HBM)
-    half = units // 2
     return pl.pallas_call(
         expert_kernel,
         out_shape=[jax.ShapeDtypeStruct((n, features), BF16)] * 2,
-        in_specs=[vmem] * 2 + [vmem, hbm, hbm] * 3,
-        out_specs=[vmem] * 2,
+        in_specs=[hbm] * 11,
+        out_specs=[hbm] * 2,
         scratch_shapes=[
             pltpu.VMEM((2 * n, features), BF16),
+            pltpu.VMEM((features, units), BF16),
+            pltpu.VMEM((features, units), BF16),
+            pltpu.VMEM((units, features), BF16),
             pltpu.VMEM((2 * n, units), BF16),
-            pltpu.VMEM((features, half), BF16),
-            pltpu.VMEM((features, half), BF16),
-            pltpu.VMEM((half, features), BF16),
-            pltpu.SemaphoreType.DMA((6,)),
+            pltpu.VMEM((2 * n, features), BF16),
+            pltpu.SemaphoreType.DMA((14,)),
+            pltpu.SemaphoreType.DMA((8,)),
         ],
-        compiler_params=pltpu.CompilerParams(vmem_limit_bytes=EXPERT_VMEM),
         cost_estimate=pl.CostEstimate(
             flops=12 * n * features * units,
             bytes_accessed=6 * features * units + 8 * n * features,
@@ -288,6 +318,26 @@
         ),
         name="expert_block",
     )(own, far, *gates, *ups, *downs)
+
+
+def finish_kernel(flat_ref, coarse_ref, fine_ref, partial_ref, gain_ref, out_ref):
+    total = partial_ref[...]
+    for share in (coarse_ref, fine_ref):
+        total = total + lax.dot_general(
+            share[...], flat_ref[...], (((0,), (0,)), ((), ())), preferred_element_type=F32
+        )
+    out_ref[...] = rms_scale(total, gain_ref[...]).astype(BF16)
+
+
+def finish(flat, coarse, fine, partial, gain):
+    tokens, features = partial.shape
+    return vmem_call(
+        finish_kernel,
+        jax.ShapeDtypeStruct((tokens, features), BF16),
+        4 * flat.shape[0] * tokens * features,
+        4 << 20,
+        tokens,
+    )(flat, coarse, fine, partial, gain.reshape(1, features))
 
 
 def halves(weight, dim):
@@ -335,13 +385,13 @@
     own_share = lax.dynamic_slice_in_dim(selected_specialist_share, place * TOK_DEV, TOK_DEV, 0)
     own_rows = lax.dynamic_slice_in_dim(second_slice_tokens, place * TOK_DEV, TOK_DEV, 0)
 
-    gate_halves = halves(specialist_switch_matrix[0], 1)
-    gate_halves, own_rows = lax.optimization_barrier((gate_halves, own_rows))
-    gates = widened(specialist_switch_matrix[0], gate_halves)
-    ups = widened(specialist_widen_matrix[0], halves(specialist_widen_matrix[0], 1))
     down_halves = halves(specialist_contract_matrix[0], 0)
-    down_halves, retention_logits = lax.optimization_barrier((down_halves, retention_logits))
+    down_halves, own_rows = lax.optimization_barrier((down_halves, own_rows))
     downs = widened(specialist_contract_matrix[0], down_halves)
+    gates = widened(specialist_switch_matrix[0], halves(specialist_switch_matrix[0], 1))
+    up_halves = halves(specialist_widen_matrix[0], 1)
+    up_halves, retention_logits = lax.optimization_barrier((up_halves, retention_logits))
+    ups = widened(specialist_widen_matrix[0], up_halves)
     normed = rms_scale(own_rows.astype(F32), leading_scale_vector).astype(BF16)
     experts = specialist_switch_matrix.shape[0] * members
     capacity = 2 * TOK_DEV * own_route.shape[1] // experts
@@ -391,13 +441,13 @@
         for c in range(CHUNKS):
             i = k * CHUNKS + c
             own = owns[i]
-            if i >= 3:
+            if i >= 2:
                 own, gate = lax.optimization_barrier((own, parts[i - 2][1]))
                 parts[i - 2] = (parts[i - 2][0], gate)
             far = shift(own, 2)
             parts.append(expert_block(own, far, gates, ups, downs))
             if i == 1:
-                entering = exchange(prefix_pass(slices).astype(BF16)).reshape(width, HEAD)
+                entering = exchange(prefix_pass(slices)).reshape(width, HEAD)
     rec = output_pass(raw, qdec, entering, state_result_switch_logits, state_result_scale)
     parts[-1], rec = lax.optimization_barrier((parts[-1], rec))
     for k in range(GROUPS):
@@ -414,11 +464,13 @@
         coarse = share.astype(BF16)
         fine = (share - coarse.astype(F32)).astype(BF16)
         flat = returned.reshape(members * count, features)
-        for piece in (coarse, fine):
-            combined = combined + lax.dot_general(
-                piece, flat, (((0,), (0,)), ((), ())), preferred_element_type=F32
-            )
-    moe_out = rms_scale(combined, trailing_scale_vector).astype(BF16)
+        if k == GROUPS - 1:
+            moe_out = finish(flat, coarse, fine, combined, trailing_scale_vector)
+        else:
+            for piece in (coarse, fine):
+                combined = combined + lax.dot_general(
+                    piece, flat, (((0,), (0,)), ((), ())), preferred_element_type=F32
+                )
 
     own, left, right, far = rec, shift(rec, 1), shift(rec, -1), shift(rec, 2)
     by_block = state_result_matrix.reshape(ring, width, -1)

time: 271 us -> 261 us (0.963)
  Pallas kernels: 35.7 us -> 47.8 us
  local copies, waits for them, and re-layouts: 29.8 us -> 20.8 us
  waiting for transfers between devices: 93 us -> 85 us
  matrix products: 25.5 us -> 19.4 us
    ppermute x17, waiting for transfers between devices: 82.5 us -> 57 us  [shift(): return lax.ppermute(x, 'tp', [(i, (i + by) % n) for i in range(n)])]
    all_to_all x5, waiting for transfers between devices: 10.5 us -> 28.1 us  [exchange(): return lax.all_to_all(x, EP, split_axis=0, concat_axis=0, tiled=True)]
    unnamed x61 -> x27, local copies, waits for them, and re-layouts: 15.1 us -> 3.89 us
    dot_general x4 -> x2, matrix products: 10.4 us -> 3.59 us  [shards(): lax.dot_general(piece, flat, (((0,), (0,)), ((), ())), preferred_element_...]
    pallas_call x0 -> x1, Pallas kernels: none -> 3.01 us  [finish(): vmem_call(finish_kernel, jax.ShapeDtypeStruct((tokens, features), BF16),...]
    pallas_call x4, Pallas kernels: 28.2 us -> 30.9 us  [expert_block(): pl.pallas_call(expert_kernel, out_shape=[jax.ShapeDtypeStruct((n, feature...]
  transfers between devices with their start and end apart: 22 -> 22, of which waited for: 7 -> 8; matrix products, arithmetic and copies ran while one was open for 12% -> 14% of each run, Pallas kernels for 13% -> 17%
where the time goes in v2:
time: 261 us; the launch traced here: 259 us
  waiting for transfers between devices  85 us (33%)
  starting transfers between devices  76.8 us (29%)
  Pallas kernels  47.8 us (18%)
  local copies, waits for them, and re-layouts  20.8 us (8%)
  matrix products  19.4 us (7%)
  other arithmetic  7.81 us (3%)
    ppermute x17, waiting for transfers between devices, shift(): return lax.ppermute(x, 'tp', [(i, (i + by) % n) for i in range(n)])  57 us
    all_to_all x5, starting transfers between devices, exchange(): return lax.all_to_all(x, EP, split_axis=0, concat_axis=0, tiled=True)  47.2 us
    pallas_call x4, Pallas kernels, expert_block(): pl.pallas_call(expert_kernel, out_shape=[jax.ShapeDtypeStruct((n, feature...  30.9 us
    ppermute x17, starting transfers between devices, shift(): return lax.ppermute(x, 'tp', [(i, (i + by) % n) for i in range(n)])  29.6 us
    all_to_all x5, waiting for transfers between devices, exchange(): return lax.all_to_all(x, EP, split_axis=0, concat_axis=0, tiled=True)  28.1 us
    dot_general x4, matrix products, shards(): jnp.dot(chosen.astype(BF16), flat_in[c], preferred_element_type=F32)  8.68 us
    pallas_call x1, Pallas kernels, local_pass(): vmem_call(local_kernel, (jax.ShapeDtypeStruct((rows, width), F32), jax.Sh...  8.58 us
    slice x3, local copies, waits for them, and re-layouts, halves(): lax.slice_in_dim(weight, half, 2 * half, axis=dim)  7.74 us
  transfers between devices with their start and end apart: 22, of which 8 were waited for; matrix products, arithmetic and copies ran while one was open for 14% of the time, Pallas kernels for 17%

profile of v2, /device:TPU:8, one launch (start us, length us, event | category | flops | bytes accessed | tf_op | source)
XLA Modules:
  0.0 258.6 jit_solution(13532279682070309266)
XLA Ops:
  2.3 3.1 %slice_bitcast_fusion = (bf16[256,2048]{1,0:T(8,128)(2,1)}, bf16[256,2048]{1,0:T(8,128)(2,1)}) fusion(bf16[1,512,2048]{2,1,0:T(8,128)(2,1)} %param.31), kind=kLoop, calls=%fused_computation.26 | loop fusion | bytes 4194304 | tf_op jit(solution)/shard_map/slice | solution.py:347
  5.6 2.1 fusion
  7.7 12.3 %all-to-all-start = ((bf16[64,8,2048]{2,1,0:T(8,128)(2,1)}), bf16[64,8,2048]{2,1,0:T(8,128)(2,1)}, u32[]{:S(2)}, u32[]{:S(2)}) async-start(bf16[64,8,2048]{2,1,0:T(8,128)(2,1)} %fusion), calls=%async_computation | async-start | bytes 4194304 | tf_op jit(solution)/shard_map/all_to_all | solution.py:357
  20.1 3.2 %fusion.64 = (bf16[2048,256]{1,0:T(8,128)(2,1)}, bf16[2048,256]{1,0:T(8,128)(2,1)}) fusion(bf16[2048,512]{1,0:T(8,128)(2,1)} %bitcast.69), kind=kLoop, calls=%fused_computation.104 | loop fusion | bytes 4194304 | tf_op jit(solution)/shard_map/slice | solution.py:347
  29.9 2.8 %collective-permute-start.5 = (bf16[256,2048]{1,0:T(8,128)(2,1)}, bf16[256,2048]{1,0:T(8,128)(2,1)}, u32[]{:S(2)}, u32[]{:S(2)}) collective-permute-start(bf16[256,2048]{1,0:T(8,128)(2,1)} %get-tuple-element.34), channel_id=1, source_target_pairs={{0,3},{1,0},{2,1},{3,2},{4,7},{5,4},{6,5},{7,6},{8,11},{9,8},{10,9... | collective-permute-start | bytes 3145736 | tf_op jit(solution)/shard_map/ppermute | solution.py:187
  33.7 8.6 %shard_map.167 = (f32[1024,256]{1,0:T(8,128)}, bf16[1024,256]{1,0:T(8,128)(2,1)}, f32[256,256]{1,0:T(8,128)}) custom-call(bf16[1024,256]{1,0:T(8,128)(2,1)} %q_ref.1, bf16[1024,256]{1,0:T(8,128)(2,1)} %r_ref, bf16[1024,256]{1,0:T(8,128)(2,1)} %v_ref.1, f32[1,256]{1,0:T(1,128)} %bitcast.95, f32[1024,2]{1,0:T(8,128)} %copy.28.fade_ref), custom_call_target="tpu_custom_call" | custom-call | flops 4000000000 | bytes 6291456 | tf_op jit(solution)/shard_map/pallas_call | solution.py:151
  44.7 26.5 %all-to-all-done = bf16[64,8,2048]{2,1,0:T(8,128)(2,1)} async-done(((bf16[64,8,2048]{2,1,0:T(8,128)(2,1)}), bf16[64,8,2048]{2,1,0:T(8,128)(2,1)}, u32[]{:S(2)}, u32[]{:S(2)}) %all-to-all-start) | async-done | bytes 2097184 | tf_op jit(solution)/shard_map/all_to_all | solution.py:357
  71.2 5.4 %all-to-all-start.1 = ((f32[64,4,256]{2,1,0:T(4,128)}), f32[64,4,256]{2,1,0:T(4,128)S(1)}, u32[]{:S(2)}, u32[]{:S(2)}) async-start(f32[64,4,256]{2,1,0:T(4,128)} %reshape.214), calls=%async_computation.1 | async-start | bytes 524288 | tf_op jit(solution)/shard_map/all_to_all | solution.py:357
  78.2 2.4 convolution_convert_fusion.3.own
  82.2 2.8 %collective-permute-start.11 = (bf16[128,2048]{1,0:T(8,128)(2,1)S(1)}, bf16[128,2048]{1,0:T(8,128)(2,1)S(1)}, u32[]{:S(2)}, u32[]{:S(2)}) collective-permute-start(bf16[128,2048]{1,0:T(8,128)(2,1)S(1)} %convolution_convert_fusion.1.own), channel_id=1, source_target_pairs={{0,2},{1,3},{2,0},{3,1},{4,6},{5,7},{6,4},{7,5},{8,10},{9,11},{10,... | collective-permute-start | bytes 1572872 | tf_op jit(solution)/shard_map/ppermute | solution.py:187
  85.0 2.4 convolution_convert_fusion.2.own
  88.3 2.4 convolution_convert_fusion.4.own
  90.6 26.0 %collective-permute-done.5.down_right = bf16[256,2048]{1,0:T(8,128)(2,1)} collective-permute-done((bf16[256,2048]{1,0:T(8,128)(2,1)}, bf16[256,2048]{1,0:T(8,128)(2,1)}, u32[]{:S(2)}, u32[]{:S(2)}) %collective-permute-start.5) | collective-permute-done | bytes 1048608 | tf_op jit(solution)/shard_map/ppermute | solution.py:187
  117.5 7.7 %expert_block.6 = (bf16[128,2048]{1,0:T(8,128)(2,1)}, bf16[128,2048]{1,0:T(8,128)(2,1)}) custom-call(bf16[128,2048]{1,0:T(8,128)(2,1)} %copy-done.3, bf16[128,2048]{1,0:T(8,128)(2,1)} %copy-done.8, bf16[2048,512]{1,0:T(8,128)(2,1)} %bitcast.70, bf16[2048,256]{1,0:T(8,128)(2,1)} %collective-permute-done.1.gate_right, bf16[2048,256]{1,0:T(8,128)(2,1)} %copy-done.2, ...), custom_call_target="tpu_custom_call" | custom-call | flops 3221225472 | bytes 14680064 | tf_op jit(solution)/shard_map/expert_block/pallas_call | solution.py:299
  127.6 7.7 %expert_block.4 = (bf16[128,2048]{1,0:T(8,128)(2,1)}, bf16[128,2048]{1,0:T(8,128)(2,1)}) custom-call(bf16[128,2048]{1,0:T(8,128)(2,1)} %convolution_convert_fusion.3.own, bf16[128,2048]{1,0:T(8,128)(2,1)} %copy-done.7, bf16[2048,512]{1,0:T(8,128)(2,1)} %bitcast.71, bf16[2048,256]{1,0:T(8,128)(2,1)} %collective-permute-done.1.gate_right, ...), custom_call_target="tpu_custom_call" | custom-call | flops 3221225472 | bytes 14680064 | tf_op jit(solution)/shard_map/expert_block/pallas_call | solution.py:299
  135.4 2.3 collective-permute-start.16
  140.1 10.3 %all-to-all-start.2 = ((bf16[64,4,128]{2,1,0:T(4,128)(2,1)}), bf16[64,4,128]{2,1,0:T(4,128)(2,1)S(1)}, u32[]{:S(2)}, u32[]{:S(2)}) async-start(bf16[64,4,128]{2,1,0:T(4,128)(2,1)} %shard_map.168), calls=%async_computation.2 | async-start | bytes 131072 | tf_op jit(solution)/shard_map/all_to_all | solution.py:357
  151.8 2.2 collective-permute-start.7
  159.3 8.7 %all-to-all-start.4 = ((bf16[64,4,2048]{2,1,0:T(4,128)(2,1)}), bf16[64,4,2048]{2,1,0:T(4,128)(2,1)S(1)}, u32[]{:S(2)}, u32[]{:S(2)}) async-start(bf16[64,4,2048]{2,1,0:T(4,128)(2,1)} %reshape.221), calls=%async_computation.4 | async-start | bytes 2097152 | tf_op jit(solution)/shard_map/all_to_all | solution.py:357
  168.0 7.8 %expert_block.7 = (bf16[128,2048]{1,0:T(8,128)(2,1)}, bf16[128,2048]{1,0:T(8,128)(2,1)}) custom-call(bf16[128,2048]{1,0:T(8,128)(2,1)} %convolution_convert_fusion.2.own, bf16[128,2048]{1,0:T(8,128)(2,1)} %collective-permute-done.12.far, bf16[2048,512]{1,0:T(8,128)(2,1)} %bitcast.72, bf16[2048,256]{1,0:T(8,128)(2,1)} %collective-permute-done.1.gate_right, ...), custom_call_target="tpu_custom_call" | custom-call | flops 3221225472 | bytes 14680064 | tf_op jit(solution)/shard_map/expert_block/pallas_call | solution.py:299
  177.2 3.6 %shard_map.169 = bf16[1024,256]{1,0:T(8,128)(2,1)} custom-call(f32[1024,256]{1,0:T(8,128)} %get-tuple-element.40.raw_ref, bf16[1024,256]{1,0:T(8,128)(2,1)} %get-tuple-element.41.qdec_ref, bf16[256,128]{1,0:T(8,128)(2,1)} %bitcast.93, bf16[1024,256]{1,0:T(8,128)(2,1)} %gate_ref.1, f32[1,256]{1,0:T(1,128)} %bitcast.96), custom_call_target="tpu_custom_call" | custom-call | flops 2000000000 | bytes 4194304 | tf_op jit(solution)/shard_map/pallas_call | solution.py:176
  180.8 7.7 %expert_block.5 = (bf16[128,2048]{1,0:T(8,128)(2,1)}, bf16[128,2048]{1,0:T(8,128)(2,1)}) custom-call(bf16[128,2048]{1,0:T(8,128)(2,1)} %convolution_convert_fusion.4.own, bf16[128,2048]{1,0:T(8,128)(2,1)} %collective-permute-done.7.far, bf16[2048,512]{1,0:T(8,128)(2,1)} %bitcast.73, bf16[2048,256]{1,0:T(8,128)(2,1)} %collective-permute-done.1.gate_right, ...), custom_call_target="tpu_custom_call" | custom-call | flops 3221225472 | bytes 14680064 | tf_op jit(solution)/shard_map/expert_block/pallas_call | solution.py:299
  188.5 2.3 collective-permute-start.14
  193.0 11.1 %collective-permute-done.14 = bf16[128,2048]{1,0:T(8,128)(2,1)} collective-permute-done((bf16[128,2048]{1,0:T(8,128)(2,1)}, bf16[128,2048]{1,0:T(8,128)(2,1)}, u32[]{:S(2)}, u32[]{:S(2)}) %collective-permute-start.14) | collective-permute-done | bytes 524320 | tf_op jit(solution)/shard_map/ppermute | solution.py:187
  206.5 2.3 reshape.219
  208.7 10.5 %all-to-all-start.3 = ((bf16[64,4,2048]{2,1,0:T(4,128)(2,1)}), bf16[64,4,2048]{2,1,0:T(4,128)(2,1)}, u32[]{:S(2)}, u32[]{:S(2)}) async-start(bf16[64,4,2048]{2,1,0:T(4,128)(2,1)} %reshape.219), calls=%async_computation.3 | async-start | bytes 2097152 | tf_op jit(solution)/shard_map/all_to_all | solution.py:357
  220.1 3.2 %collective-permute-start.8 = (bf16[1024,256]{1,0:T(8,128)(2,1)}, bf16[1024,256]{1,0:T(8,128)(2,1)}, u32[]{:S(2)}, u32[]{:S(2)}) collective-permute-start(bf16[1024,256]{1,0:T(8,128)(2,1)} %shard_map.169), channel_id=1, source_target_pairs={{0,1},{1,2},{2,3},{3,0},{4,5},{5,6},{6,7},{7,4},{8,9},{9,10},{10,1... | collective-permute-start | bytes 1572872 | tf_op jit(solution)/shard_map/ppermute | solution.py:187
  228.2 7.7 %collective-permute-done.8 = bf16[1024,256]{1,0:T(8,128)(2,1)} collective-permute-done((bf16[1024,256]{1,0:T(8,128)(2,1)}, bf16[1024,256]{1,0:T(8,128)(2,1)}, u32[]{:S(2)}, u32[]{:S(2)}) %collective-permute-start.8) | collective-permute-done | bytes 524320 | tf_op jit(solution)/shard_map/ppermute | solution.py:187
  237.4 10.7 %collective-permute-done.9 = bf16[1024,256]{1,0:T(8,128)(2,1)S(1)} collective-permute-done((bf16[1024,256]{1,0:T(8,128)(2,1)}, bf16[1024,256]{1,0:T(8,128)(2,1)S(1)}, u32[]{:S(2)}, u32[]{:S(2)}) %collective-permute-start.9) | collective-permute-done | bytes 524320 | tf_op jit(solution)/shard_map/ppermute | solution.py:187
  251.2 2.3 fusion.1.partial_ref
  253.5 2.2 reshape.220.flat_ref
  255.6 3.0 %shard_map.170 = bf16[128,2048]{1,0:T(8,128)(2,1)} custom-call(bf16[256,2048]{1,0:T(8,128)(2,1)} %reshape.220.flat_ref, bf16[256,128]{1,0:T(8,128)(2,1)} %fusion.62.coarse_ref, bf16[256,128]{1,0:T(8,128)(2,1)} %subtract_convert_fusion.fine_ref, f32[128,2048]{1,0:T(8,128)} %fusion.1.partial_ref, f32[1,2048]{1,0:T(1,128)} %bitcast.94), custom_call_target="tpu_custom_call" | custom-call | flops 268435456 | bytes 4194304 | tf_op jit(solution)/shard_map/pallas_call | solution.py:334
  (93 shorter events, 44.8 us)
Async XLA Ops:
  0.6 1.6 copy-start
  2.3 3.3 %copy-start.11 = (f32[2048]{0:T(1024)S(1)}, f32[2048]{0:T(1024)}, u32[]{:S(2)}) copy-start(f32[2048]{0:T(1024)} %param.27) | copy-start | bytes 24580
  7.7 63.5 %all-to-all-start = ((bf16[64,8,2048]{2,1,0:T(8,128)(2,1)}), bf16[64,8,2048]{2,1,0:T(8,128)(2,1)}, u32[]{:S(2)}, u32[]{:S(2)}) async-start(bf16[64,8,2048]{2,1,0:T(8,128)(2,1)} %fusion), calls=%async_computation | async-start | bytes 4194304 | tf_op jit(solution)/shard_map/all_to_all | solution.py:357
  20.0 6.4 %copy-start.1 = (bf16[1,2048,512]{2,1,0:T(8,128)(2,1)S(1)}, bf16[1,2048,512]{2,1,0:T(8,128)(2,1)}, u32[]{:S(2)}) copy-start(bf16[1,2048,512]{2,1,0:T(8,128)(2,1)} %param.30) | copy-start | bytes 6291460
  23.2 53.4 %collective-permute-start.2 = (bf16[2048,256]{1,0:T(8,128)(2,1)}, bf16[2048,256]{1,0:T(8,128)(2,1)S(1)}, u32[]{:S(2)}, u32[]{:S(2)}) collective-permute-start(bf16[2048,256]{1,0:T(8,128)(2,1)} %get-tuple-element.54), channel_id=1, source_target_pairs={{0,1},{1,2},{2,3},{3,0},{4,5},{5,6},{6,7},{7,4},{8,9},{9,10},{10,1... | collective-permute-start | bytes 3145736 | tf_op jit(solution)/shard_map/ppermute | solution.py:187
  24.7 57.5 %collective-permute-start.1 = (bf16[2048,256]{1,0:T(8,128)(2,1)}, bf16[2048,256]{1,0:T(8,128)(2,1)}, u32[]{:S(2)}, u32[]{:S(2)}) collective-permute-start(bf16[2048,256]{1,0:T(8,128)(2,1)} %get-tuple-element.55), channel_id=1, source_target_pairs={{0,3},{1,0},{2,1},{3,2},{4,7},{5,4},{6,5},{7,6},{8,11},{9,8},{10,9... | collective-permute-start | bytes 3145736 | tf_op jit(solution)/shard_map/ppermute | solution.py:187
  26.5 6.2 %copy-start.12 = (f32[1024,2]{0,1:T(2,128)S(1)}, f32[1024,2]{0,1:T(2,128)}, u32[]{:S(2)}) copy-start(f32[1024,2]{0,1:T(2,128)} %param.21) | copy-start | bytes 24580
  27.9 59.5 %collective-permute-start.3 = (bf16[2048,256]{1,0:T(8,128)(2,1)}, bf16[2048,256]{1,0:T(8,128)(2,1)}, u32[]{:S(2)}, u32[]{:S(2)}) collective-permute-start(bf16[2048,256]{1,0:T(8,128)(2,1)} %get-tuple-element.32), channel_id=1, source_target_pairs={{0,3},{1,0},{2,1},{3,2},{4,7},{5,4},{6,5},{7,6},{8,11},{9,8},{10,9... | collective-permute-start | bytes 3145736 | tf_op jit(solution)/shard_map/ppermute | solution.py:187
  29.5 61.2 %collective-permute-start.4 = (bf16[2048,256]{1,0:T(8,128)(2,1)}, bf16[2048,256]{1,0:T(8,128)(2,1)}, u32[]{:S(2)}, u32[]{:S(2)}) collective-permute-start(bf16[2048,256]{1,0:T(8,128)(2,1)} %get-tuple-element.33), channel_id=1, source_target_pairs={{0,1},{1,2},{2,3},{3,0},{4,5},{5,6},{6,7},{7,4},{8,9},{9,10},{10,1... | collective-permute-start | bytes 3145736 | tf_op jit(solution)/shard_map/ppermute | solution.py:187
  29.9 86.7 %collective-permute-start.5 = (bf16[256,2048]{1,0:T(8,128)(2,1)}, bf16[256,2048]{1,0:T(8,128)(2,1)}, u32[]{:S(2)}, u32[]{:S(2)}) collective-permute-start(bf16[256,2048]{1,0:T(8,128)(2,1)} %get-tuple-element.34), channel_id=1, source_target_pairs={{0,3},{1,0},{2,1},{3,2},{4,7},{5,4},{6,5},{7,6},{8,11},{9,8},{10,9... | collective-permute-start | bytes 3145736 | tf_op jit(solution)/shard_map/ppermute | solution.py:187
  71.2 66.5 %all-to-all-start.1 = ((f32[64,4,256]{2,1,0:T(4,128)}), f32[64,4,256]{2,1,0:T(4,128)S(1)}, u32[]{:S(2)}, u32[]{:S(2)}) async-start(f32[64,4,256]{2,1,0:T(4,128)} %reshape.214), calls=%async_computation.1 | async-start | bytes 524288 | tf_op jit(solution)/shard_map/all_to_all | solution.py:357
  76.6 10.7 %copy-start.2 = (bf16[2048,256]{1,0:T(8,128)(2,1)}, bf16[2048,256]{1,0:T(8,128)(2,1)S(1)}, u32[]{:S(2)}) copy-start(bf16[2048,256]{1,0:T(8,128)(2,1)S(1)} %collective-permute-done.2.gate_left) | copy-start | bytes 3145732
  76.7 40.0 %collective-permute-start.6 = (bf16[256,2048]{1,0:T(8,128)(2,1)}, bf16[256,2048]{1,0:T(8,128)(2,1)}, u32[]{:S(2)}, u32[]{:S(2)}) collective-permute-start(bf16[256,2048]{1,0:T(8,128)(2,1)} %get-tuple-element.35), channel_id=1, source_target_pairs={{0,1},{1,2},{2,3},{3,0},{4,5},{5,6},{6,7},{7,4},{8,9},{9,10},{10,1... | collective-permute-start | bytes 3145736 | tf_op jit(solution)/shard_map/ppermute | solution.py:187
  82.2 5.2 %copy-start.3 = (bf16[128,2048]{1,0:T(8,128)(2,1)}, bf16[128,2048]{1,0:T(8,128)(2,1)S(1)}, u32[]{:S(2)}) copy-start(bf16[128,2048]{1,0:T(8,128)(2,1)S(1)} %convolution_convert_fusion.1.own) | copy-start | bytes 1572868
  82.2 34.5 %collective-permute-start.11 = (bf16[128,2048]{1,0:T(8,128)(2,1)S(1)}, bf16[128,2048]{1,0:T(8,128)(2,1)S(1)}, u32[]{:S(2)}, u32[]{:S(2)}) collective-permute-start(bf16[128,2048]{1,0:T(8,128)(2,1)S(1)} %convolution_convert_fusion.1.own), channel_id=1, source_target_pairs={{0,2},{1,3},{2,0},{3,1},{4,6},{5,7},{6,4},{7,5},{8,10},{9,11},{10,... | collective-permute-start | bytes 1572872 | tf_op jit(solution)/shard_map/ppermute | solution.py:187
  87.4 39.4 %collective-permute-start = (bf16[128,2048]{1,0:T(8,128)(2,1)}, bf16[128,2048]{1,0:T(8,128)(2,1)S(1)}, u32[]{:S(2)}, u32[]{:S(2)}) collective-permute-start(bf16[128,2048]{1,0:T(8,128)(2,1)} %convolution_convert_fusion.3.own), channel_id=1, source_target_pairs={{0,2},{1,3},{2,0},{3,1},{4,6},{5,7},{6,4},{7,5},{8,10},{9,11},{10,... | collective-permute-start | bytes 1572872 | tf_op jit(solution)/shard_map/ppermute | solution.py:187
  125.2 28.8 %copy-start.5 = (bf16[128,2048]{1,0:T(8,128)(2,1)S(1)}, bf16[128,2048]{1,0:T(8,128)(2,1)}, u32[]{:S(2)}) copy-start(bf16[128,2048]{1,0:T(8,128)(2,1)} %get-tuple-element.50) | copy-start | bytes 1572868
  125.2 28.8 %collective-permute-start.15 = (bf16[128,2048]{1,0:T(8,128)(2,1)}, bf16[128,2048]{1,0:T(8,128)(2,1)}, u32[]{:S(2)}, u32[]{:S(2)}) collective-permute-start(bf16[128,2048]{1,0:T(8,128)(2,1)} %get-tuple-element.51), channel_id=1, source_target_pairs={{0,2},{1,3},{2,0},{3,1},{4,6},{5,7},{6,4},{7,5},{8,10},{9,11},{10,... | collective-permute-start | bytes 1572872 | tf_op jit(solution)/shard_map/ppermute | solution.py:187
  135.4 19.9 %copy-start.6 = (bf16[128,2048]{1,0:T(8,128)(2,1)S(1)}, bf16[128,2048]{1,0:T(8,128)(2,1)}, u32[]{:S(2)}) copy-start(bf16[128,2048]{1,0:T(8,128)(2,1)} %get-tuple-element.52) | copy-start | bytes 1572868
  135.4 19.8 %collective-permute-start.16 = (bf16[128,2048]{1,0:T(8,128)(2,1)}, bf16[128,2048]{1,0:T(8,128)(2,1)}, u32[]{:S(2)}, u32[]{:S(2)}) collective-permute-start(bf16[128,2048]{1,0:T(8,128)(2,1)} %get-tuple-element.53), channel_id=1, source_target_pairs={{0,2},{1,3},{2,0},{3,1},{4,6},{5,7},{6,4},{7,5},{8,10},{9,11},{10,... | collective-permute-start | bytes 1572872 | tf_op jit(solution)/shard_map/ppermute | solution.py:187
  140.1 19.2 %all-to-all-start.2 = ((bf16[64,4,128]{2,1,0:T(4,128)(2,1)}), bf16[64,4,128]{2,1,0:T(4,128)(2,1)S(1)}, u32[]{:S(2)}, u32[]{:S(2)}) async-start(bf16[64,4,128]{2,1,0:T(4,128)(2,1)} %shard_map.168), calls=%async_computation.2 | async-start | bytes 131072 | tf_op jit(solution)/shard_map/all_to_all | solution.py:357
  150.4 17.6 %collective-permute-start.12 = (bf16[128,2048]{1,0:T(8,128)(2,1)}, bf16[128,2048]{1,0:T(8,128)(2,1)}, u32[]{:S(2)}, u32[]{:S(2)}) collective-permute-start(bf16[128,2048]{1,0:T(8,128)(2,1)} %convolution_convert_fusion.2.own), channel_id=1, source_target_pairs={{0,2},{1,3},{2,0},{3,1},{4,6},{5,7},{6,4},{7,5},{8,10},{9,11},{10,... | collective-permute-start | bytes 1572872 | tf_op jit(solution)/shard_map/ppermute | solution.py:187
  151.8 29.0 %collective-permute-start.7 = (bf16[128,2048]{1,0:T(8,128)(2,1)}, bf16[128,2048]{1,0:T(8,128)(2,1)}, u32[]{:S(2)}, u32[]{:S(2)}) collective-permute-start(bf16[128,2048]{1,0:T(8,128)(2,1)} %convolution_convert_fusion.4.own), channel_id=1, source_target_pairs={{0,2},{1,3},{2,0},{3,1},{4,6},{5,7},{6,4},{7,5},{8,10},{9,11},{10,... | collective-permute-start | bytes 1572872 | tf_op jit(solution)/shard_map/ppermute | solution.py:187
  159.3 16.5 %copy-start.10 = (bf16[64,4,128]{2,1,0:T(4,128)(2,1)}, bf16[64,4,128]{2,1,0:T(4,128)(2,1)S(1)}, u32[]{:S(2)}) copy-start(bf16[64,4,128]{2,1,0:T(4,128)(2,1)S(1)} %all-to-all-done.2) | copy-start | bytes 196612
  159.3 49.4 %all-to-all-start.4 = ((bf16[64,4,2048]{2,1,0:T(4,128)(2,1)}), bf16[64,4,2048]{2,1,0:T(4,128)(2,1)S(1)}, u32[]{:S(2)}, u32[]{:S(2)}) async-start(bf16[64,4,2048]{2,1,0:T(4,128)(2,1)} %reshape.221), calls=%async_computation.4 | async-start | bytes 2097152 | tf_op jit(solution)/shard_map/all_to_all | solution.py:357
  175.8 15.9 %collective-permute-start.13 = (bf16[128,2048]{1,0:T(8,128)(2,1)}, bf16[128,2048]{1,0:T(8,128)(2,1)}, u32[]{:S(2)}, u32[]{:S(2)}) collective-permute-start(bf16[128,2048]{1,0:T(8,128)(2,1)} %get-tuple-element.47), channel_id=1, source_target_pairs={{0,2},{1,3},{2,0},{3,1},{4,6},{5,7},{6,4},{7,5},{8,10},{9,11},{10,... | collective-permute-start | bytes 1572872 | tf_op jit(solution)/shard_map/ppermute | solution.py:187
  188.5 15.6 %collective-permute-start.14 = (bf16[128,2048]{1,0:T(8,128)(2,1)}, bf16[128,2048]{1,0:T(8,128)(2,1)}, u32[]{:S(2)}, u32[]{:S(2)}) collective-permute-start(bf16[128,2048]{1,0:T(8,128)(2,1)} %get-tuple-element.49), channel_id=1, source_target_pairs={{0,2},{1,3},{2,0},{3,1},{4,6},{5,7},{6,4},{7,5},{8,10},{9,11},{10,... | collective-permute-start | bytes 1572872 | tf_op jit(solution)/shard_map/ppermute | solution.py:187
  208.7 44.7 %all-to-all-start.3 = ((bf16[64,4,2048]{2,1,0:T(4,128)(2,1)}), bf16[64,4,2048]{2,1,0:T(4,128)(2,1)}, u32[]{:S(2)}, u32[]{:S(2)}) async-start(bf16[64,4,2048]{2,1,0:T(4,128)(2,1)} %reshape.219), calls=%async_computation.3 | async-start | bytes 2097152 | tf_op jit(solution)/shard_map/all_to_all | solution.py:357
  220.1 15.8 %collective-permute-start.8 = (bf16[1024,256]{1,0:T(8,128)(2,1)}, bf16[1024,256]{1,0:T(8,128)(2,1)}, u32[]{:S(2)}, u32[]{:S(2)}) collective-permute-start(bf16[1024,256]{1,0:T(8,128)(2,1)} %shard_map.169), channel_id=1, source_target_pairs={{0,1},{1,2},{2,3},{3,0},{4,5},{5,6},{6,7},{7,4},{8,9},{9,10},{10,1... | collective-permute-start | bytes 1572872 | tf_op jit(solution)/shard_map/ppermute | solution.py:187
  223.3 12.6 %copy-start.4 = (bf16[1024,512]{1,0:T(8,128)(2,1)S(1)}, bf16[1024,512]{1,0:T(8,128)(2,1)}, u32[]{:S(2)}) copy-start(bf16[1024,512]{1,0:T(8,128)(2,1)} %param.23) | copy-start | bytes 3145732
  224.0 24.5 %collective-permute-start.10 = (bf16[1024,256]{1,0:T(8,128)(2,1)}, bf16[1024,256]{1,0:T(8,128)(2,1)S(1)}, u32[]{:S(2)}, u32[]{:S(2)}) collective-permute-start(bf16[1024,256]{1,0:T(8,128)(2,1)} %shard_map.169), channel_id=1, source_target_pairs={{0,2},{1,3},{2,0},{3,1},{4,6},{5,7},{6,4},{7,5},{8,10},{9,11},{10,... | collective-permute-start | bytes 1572872 | tf_op jit(solution)/shard_map/ppermute | solution.py:187
  224.9 23.1 %collective-permute-start.9 = (bf16[1024,256]{1,0:T(8,128)(2,1)}, bf16[1024,256]{1,0:T(8,128)(2,1)S(1)}, u32[]{:S(2)}, u32[]{:S(2)}) collective-permute-start(bf16[1024,256]{1,0:T(8,128)(2,1)} %shard_map.169), channel_id=1, source_target_pairs={{0,3},{1,0},{2,1},{3,2},{4,7},{5,4},{6,5},{7,6},{8,11},{9,8},{10,9... | collective-permute-start | bytes 1572872 | tf_op jit(solution)/shard_map/ppermute | solution.py:187
  (3 other events, 2.3 us)

commit v3 on v2

--- a/solution.py
+++ b/solution.py
@@ -375,7 +375,7 @@
     specialist_widen_matrix,
     specialist_contract_matrix,
 ):
-    _, width = state_probe_logits.shape
+    total_rows, width = state_probe_logits.shape
     members = lax.axis_size(EP)
     place = lax.axis_index("tp")
     ring = lax.axis_size("tp")
@@ -423,6 +423,14 @@
     ends, arrived = lax.optimization_barrier((ends, arrived))
     slices = exchange(ends)
 
+    shares = []
+    for k in range(GROUPS):
+        chosen = slots_of(k * (capacity // GROUPS), capacity // GROUPS)
+        share = jnp.where(chosen, weight[:, None, :], 0.0).reshape(-1, TOK_DEV)
+        coarse = share.astype(BF16)
+        fine = (share - coarse.astype(F32)).astype(BF16)
+        shares.append((coarse, fine))
+
     combined = jnp.zeros((TOK_DEV, features), F32)
     count = capacity // GROUPS
     n = members * count // CHUNKS
@@ -441,28 +449,27 @@
         for c in range(CHUNKS):
             i = k * CHUNKS + c
             own = owns[i]
-            if i >= 2:
-                own, gate = lax.optimization_barrier((own, parts[i - 2][1]))
-                parts[i - 2] = (parts[i - 2][0], gate)
             far = shift(own, 2)
             parts.append(expert_block(own, far, gates, ups, downs))
             if i == 1:
-                entering = exchange(prefix_pass(slices)).reshape(width, HEAD)
-    rec = output_pass(raw, qdec, entering, state_result_switch_logits, state_result_scale)
-    parts[-1], rec = lax.optimization_barrier((parts[-1], rec))
+                leaving = prefix_pass(slices)
     for k in range(GROUPS):
-        first = k * count
         finished = []
         for c in range(CHUNKS):
             mine, other = parts[k * CHUNKS + c]
             back = shift(other, 2)
-            finished.append((mine.astype(F32) + back.astype(F32)).astype(BF16))
-        finished = jnp.concatenate(finished, axis=0)
-        returned = exchange(finished.reshape(members, count, features))
-        share = jnp.where(slots_of(first, count), weight[:, None, :], 0.0)
-        share = share.reshape(experts * count, TOK_DEV)
-        coarse = share.astype(BF16)
-        fine = (share - coarse.astype(F32)).astype(BF16)
+            total = (mine.astype(F32) + back.astype(F32)).astype(BF16)
+            if k == 0:
+                beside = leaving.reshape(CHUNKS, n, HEAD)[c]
+                total = jnp.concatenate([total, beside], axis=1)
+            finished.append(total)
+        finished = jnp.concatenate(finished, axis=0).reshape(members, count, -1)
+        returned = exchange(finished)
+        if k == 0:
+            entering = returned[:, :, features:].reshape(width, HEAD)
+            returned = returned[:, :, :features]
+            rec = output_pass(raw, qdec, entering, state_result_switch_logits, state_result_scale)
+        coarse, fine = shares[k]
         flat = returned.reshape(members * count, features)
         if k == GROUPS - 1:
             moe_out = finish(flat, coarse, fine, combined, trailing_scale_vector)
@@ -472,7 +479,9 @@
                     piece, flat, (((0,), (0,)), ((), ())), preferred_element_type=F32
                 )
 
-    own, left, right, far = rec, shift(rec, 1), shift(rec, -1), shift(rec, 2)
+    half = total_rows // 2
+    own, left, right = rec, shift(rec, 1), shift(rec, -1)
+    far = jnp.concatenate([shift(left[:half], 1), shift(right[half:], -1)], axis=0)
     by_block = state_result_matrix.reshape(ring, width, -1)
 
     def columns(block, at):

time: 261 us -> 279 us (1.069)
  waiting for transfers between devices: 85 us -> 112 us
  starting transfers between devices: 76.8 us -> 69.1 us
    ppermute x17 -> x18, waiting for transfers between devices: 57 us -> 76.3 us  [shift(): return lax.ppermute(x, 'tp', [(i, (i + by) % n) for i in range(n)])]
    all_to_all x5 -> x4, starting transfers between devices: 47.2 us -> 38.5 us  [exchange(): return lax.all_to_all(x, EP, split_axis=0, concat_axis=0, tiled=True)]
    all_to_all x5 -> x4, waiting for transfers between devices: 28.1 us -> 35.4 us  [exchange(): return lax.all_to_all(x, EP, split_axis=0, concat_axis=0, tiled=True)]
    slice x0 -> x5, local copies, waits for them, and re-layouts: none -> 3.18 us  [the longest x1 0.97 us: shards(): left[:half]]
    ppermute x17 -> x18, starting transfers between devices: 29.6 us -> 30.6 us  [shift(): return lax.ppermute(x, 'tp', [(i, (i + by) % n) for i in range(n)])]
  transfers between devices with their start and end apart: 22 -> 22, of which waited for: 8 -> 9; matrix products, arithmetic and copies ran while one was open for 14% -> 13% of each run, Pallas kernels for 17% -> 16%
where the time goes in v3:
time: 279 us; the launch traced here: 277 us
  waiting for transfers between devices  112 us (40%)
  starting transfers between devices  69.1 us (25%)
  Pallas kernels  47.9 us (17%)
  local copies, waits for them, and re-layouts  22.2 us (8%)
  matrix products  19.6 us (7%)
  other arithmetic  5.47 us (2%)
    ppermute x18, waiting for transfers between devices, shift(): return lax.ppermute(x, 'tp', [(i, (i + by) % n) for i in range(n)])  76.3 us
    all_to_all x4, starting transfers between devices, exchange(): return lax.all_to_all(x, EP, split_axis=0, concat_axis=0, tiled=True)  38.5 us
    all_to_all x4, waiting for transfers between devices, exchange(): return lax.all_to_all(x, EP, split_axis=0, concat_axis=0, tiled=True)  35.4 us
    pallas_call x4, Pallas kernels, expert_block(): pl.pallas_call(expert_kernel, out_shape=[jax.ShapeDtypeStruct((n, feature...  30.9 us
    ppermute x18, starting transfers between devices, shift(): return lax.ppermute(x, 'tp', [(i, (i + by) % n) for i in range(n)])  30.6 us
    pallas_call x1, Pallas kernels, local_pass(): vmem_call(local_kernel, (jax.ShapeDtypeStruct((rows, width), F32), jax.Sh...  8.65 us
    dot_general x4, matrix products, shards(): jnp.dot(chosen.astype(BF16), flat_in[c], preferred_element_type=F32)  7.9 us
    slice x3, local copies, waits for them, and re-layouts, halves(): lax.slice_in_dim(weight, half, 2 * half, axis=dim)  7.78 us
  transfers between devices with their start and end apart: 22, of which 9 were waited for; matrix products, arithmetic and copies ran while one was open for 13% of the time, Pallas kernels for 16%

profile of v3, /device:TPU:8, one launch (start us, length us, event | category | flops | bytes accessed | tf_op | source)
XLA Modules:
  0.0 277.0 jit_solution(17557029846288640940)
XLA Ops:
  2.3 3.1 %slice_bitcast_fusion = (bf16[256,2048]{1,0:T(8,128)(2,1)}, bf16[256,2048]{1,0:T(8,128)(2,1)}) fusion(bf16[1,512,2048]{2,1,0:T(8,128)(2,1)} %param.31), kind=kLoop, calls=%fused_computation.26 | loop fusion | bytes 4194304 | tf_op jit(solution)/shard_map/slice | solution.py:347
  7.7 12.3 %all-to-all-start = ((bf16[64,8,2048]{2,1,0:T(8,128)(2,1)}), bf16[64,8,2048]{2,1,0:T(8,128)(2,1)}, u32[]{:S(2)}, u32[]{:S(2)}) async-start(bf16[64,8,2048]{2,1,0:T(8,128)(2,1)} %fusion), calls=%async_computation | async-start | bytes 4194304 | tf_op jit(solution)/shard_map/all_to_all | solution.py:357
  20.0 3.2 %fusion.68 = (bf16[2048,256]{1,0:T(8,128)(2,1)}, bf16[2048,256]{1,0:T(8,128)(2,1)}) fusion(bf16[2048,512]{1,0:T(8,128)(2,1)} %bitcast.68), kind=kLoop, calls=%fused_computation.108 | loop fusion | bytes 4194304 | tf_op jit(solution)/shard_map/slice | solution.py:347
  30.0 2.8 collective-permute-start.5
  33.8 16.9 %collective-permute-done.2.gate_left = bf16[2048,256]{1,0:T(8,128)(2,1)S(1)} collective-permute-done((bf16[2048,256]{1,0:T(8,128)(2,1)}, bf16[2048,256]{1,0:T(8,128)(2,1)S(1)}, u32[]{:S(2)}, u32[]{:S(2)}) %collective-permute-start.2) | collective-permute-done | bytes 1048608 | tf_op jit(solution)/shard_map/ppermute | solution.py:187
  50.9 8.6 %shard_map.167 = (f32[1024,256]{1,0:T(8,128)}, bf16[1024,256]{1,0:T(8,128)(2,1)}, f32[256,256]{1,0:T(8,128)}) custom-call(bf16[1024,256]{1,0:T(8,128)(2,1)} %q_ref.1, bf16[1024,256]{1,0:T(8,128)(2,1)} %r_ref, bf16[1024,256]{1,0:T(8,128)(2,1)} %v_ref.1, f32[1,256]{1,0:T(1,128)} %bitcast.96, f32[1024,2]{1,0:T(8,128)} %copy.30.fade_ref), custom_call_target="tpu_custom_call" | custom-call | flops 4000000000 | bytes 6291456 | tf_op jit(solution)/shard_map/pallas_call | solution.py:151
  61.3 9.8 %all-to-all-done = bf16[64,8,2048]{2,1,0:T(8,128)(2,1)} async-done(((bf16[64,8,2048]{2,1,0:T(8,128)(2,1)}), bf16[64,8,2048]{2,1,0:T(8,128)(2,1)}, u32[]{:S(2)}, u32[]{:S(2)}) %all-to-all-start) | async-done | bytes 2097184 | tf_op jit(solution)/shard_map/all_to_all | solution.py:357
  71.2 5.4 %all-to-all-start.1 = ((f32[64,4,256]{2,1,0:T(4,128)}), f32[64,4,256]{2,1,0:T(4,128)S(1)}, u32[]{:S(2)}, u32[]{:S(2)}) async-start(f32[64,4,256]{2,1,0:T(4,128)} %reshape.220), calls=%async_computation.1 | async-start | bytes 524288 | tf_op jit(solution)/shard_map/all_to_all | solution.py:357
  78.2 3.1 %collective-permute-start.16 = (bf16[128,2048]{1,0:T(8,128)(2,1)S(1)}, bf16[128,2048]{1,0:T(8,128)(2,1)S(1)}, u32[]{:S(2)}, u32[]{:S(2)}) collective-permute-start(bf16[128,2048]{1,0:T(8,128)(2,1)S(1)} %convolution_convert_fusion.1.own), channel_id=1, source_target_pairs={{0,2},{1,3},{2,0},{3,1},{4,6},{5,7},{6,4},{7,5},{8,10},{9,11},{10,... | collective-permute-start | bytes 1572872 | tf_op jit(solution)/shard_map/ppermute | solution.py:187
  83.5 2.4 convolution_convert_fusion.3.own
  85.9 30.7 %collective-permute-done.5.down_right = bf16[256,2048]{1,0:T(8,128)(2,1)} collective-permute-done((bf16[256,2048]{1,0:T(8,128)(2,1)}, bf16[256,2048]{1,0:T(8,128)(2,1)}, u32[]{:S(2)}, u32[]{:S(2)}) %collective-permute-start.5) | collective-permute-done | bytes 1048608 | tf_op jit(solution)/shard_map/ppermute | solution.py:187
  117.4 7.7 %expert_block.7 = (bf16[128,2048]{1,0:T(8,128)(2,1)}, bf16[128,2048]{1,0:T(8,128)(2,1)}) custom-call(bf16[128,2048]{1,0:T(8,128)(2,1)} %copy-done.4, bf16[128,2048]{1,0:T(8,128)(2,1)} %copy-done.9, bf16[2048,512]{1,0:T(8,128)(2,1)} %bitcast.69, bf16[2048,256]{1,0:T(8,128)(2,1)} %collective-permute-done.1.gate_right, bf16[2048,256]{1,0:T(8,128)(2,1)} %copy-done.2, ...), custom_call_target="tpu_custom_call" | custom-call | flops 3221225472 | bytes 14680064 | tf_op jit(solution)/shard_map/expert_block/pallas_call | solution.py:299
  125.5 7.7 %expert_block.6 = (bf16[128,2048]{1,0:T(8,128)(2,1)}, bf16[128,2048]{1,0:T(8,128)(2,1)}) custom-call(bf16[128,2048]{1,0:T(8,128)(2,1)} %copy-done.3, bf16[128,2048]{1,0:T(8,128)(2,1)} %collective-permute-done.14.far, bf16[2048,512]{1,0:T(8,128)(2,1)} %bitcast.70, bf16[2048,256]{1,0:T(8,128)(2,1)} %collective-permute-done.1.gate_right, ...), custom_call_target="tpu_custom_call" | custom-call | flops 3221225472 | bytes 14680064 | tf_op jit(solution)/shard_map/expert_block/pallas_call | solution.py:299
  133.2 3.6 %collective-permute-start.15 = (bf16[128,2048]{1,0:T(8,128)(2,1)}, bf16[128,2048]{1,0:T(8,128)(2,1)}, u32[]{:S(2)}, u32[]{:S(2)}) collective-permute-start(bf16[128,2048]{1,0:T(8,128)(2,1)} %get-tuple-element.37), channel_id=1, source_target_pairs={{0,2},{1,3},{2,0},{3,1},{4,6},{5,7},{6,4},{7,5},{8,10},{9,11},{10,... | collective-permute-start | bytes 1572872 | tf_op jit(solution)/shard_map/ppermute | solution.py:187
  136.8 2.4 convolution_convert_fusion.4.own
  139.3 3.4 %collective-permute-start.8 = (bf16[128,2048]{1,0:T(8,128)(2,1)}, bf16[128,2048]{1,0:T(8,128)(2,1)}, u32[]{:S(2)}, u32[]{:S(2)}) collective-permute-start(bf16[128,2048]{1,0:T(8,128)(2,1)} %convolution_convert_fusion.3.own), channel_id=1, source_target_pairs={{0,2},{1,3},{2,0},{3,1},{4,6},{5,7},{6,4},{7,5},{8,10},{9,11},{10,... | collective-permute-start | bytes 1572872 | tf_op jit(solution)/shard_map/ppermute | solution.py:187
  146.3 7.0 %collective-permute-done.15 = bf16[128,2048]{1,0:T(8,128)(2,1)} collective-permute-done((bf16[128,2048]{1,0:T(8,128)(2,1)}, bf16[128,2048]{1,0:T(8,128)(2,1)}, u32[]{:S(2)}, u32[]{:S(2)}) %collective-permute-start.15) | collective-permute-done | bytes 524320 | tf_op jit(solution)/shard_map/ppermute | solution.py:187
  155.7 10.5 %all-to-all-start.3 = ((bf16[64,4,2048]{2,1,0:T(4,128)(2,1)}), bf16[64,4,2048]{2,1,0:T(4,128)(2,1)}, u32[]{:S(2)}, u32[]{:S(2)}) async-start(bf16[64,4,2048]{2,1,0:T(4,128)(2,1)} %reshape.226), calls=%async_computation.3 | async-start | bytes 2097152 | tf_op jit(solution)/shard_map/all_to_all | solution.py:357
  166.3 7.7 %expert_block.4 = (bf16[128,2048]{1,0:T(8,128)(2,1)}, bf16[128,2048]{1,0:T(8,128)(2,1)}) custom-call(bf16[128,2048]{1,0:T(8,128)(2,1)} %convolution_convert_fusion.4.own, bf16[128,2048]{1,0:T(8,128)(2,1)} %collective-permute-done.far, bf16[2048,512]{1,0:T(8,128)(2,1)} %bitcast.71, bf16[2048,256]{1,0:T(8,128)(2,1)} %collective-permute-done.1.gate_right, ...), custom_call_target="tpu_custom_call" | custom-call | flops 3221225472 | bytes 14680064 | tf_op jit(solution)/shard_map/expert_block/pallas_call | solution.py:299
  174.2 7.7 %expert_block.5 = (bf16[128,2048]{1,0:T(8,128)(2,1)}, bf16[128,2048]{1,0:T(8,128)(2,1)}) custom-call(bf16[128,2048]{1,0:T(8,128)(2,1)} %convolution_convert_fusion.3.own, bf16[128,2048]{1,0:T(8,128)(2,1)} %collective-permute-done.8.far, bf16[2048,512]{1,0:T(8,128)(2,1)} %bitcast.72, bf16[2048,256]{1,0:T(8,128)(2,1)} %collective-permute-done.1.gate_right, ...), custom_call_target="tpu_custom_call" | custom-call | flops 3221225472 | bytes 14680064 | tf_op jit(solution)/shard_map/expert_block/pallas_call | solution.py:299
  182.0 3.5 %collective-permute-start.9 = (bf16[128,2048]{1,0:T(8,128)(2,1)}, bf16[128,2048]{1,0:T(8,128)(2,1)S(1)}, u32[]{:S(2)}, u32[]{:S(2)}) collective-permute-start(bf16[128,2048]{1,0:T(8,128)(2,1)} %get-tuple-element.35), channel_id=1, source_target_pairs={{0,2},{1,3},{2,0},{3,1},{4,6},{5,7},{6,4},{7,5},{8,10},{9,11},{10,... | collective-permute-start | bytes 1572872 | tf_op jit(solution)/shard_map/ppermute | solution.py:187
  185.5 5.1 %collective-permute-done.7 = bf16[128,2048]{1,0:T(8,128)(2,1)S(1)} collective-permute-done((bf16[128,2048]{1,0:T(8,128)(2,1)}, bf16[128,2048]{1,0:T(8,128)(2,1)S(1)}, u32[]{:S(2)}, u32[]{:S(2)}) %collective-permute-start.7) | collective-permute-done | bytes 524320 | tf_op jit(solution)/shard_map/ppermute | solution.py:187
  190.7 10.3 %collective-permute-done.9 = bf16[128,2048]{1,0:T(8,128)(2,1)S(1)} collective-permute-done((bf16[128,2048]{1,0:T(8,128)(2,1)}, bf16[128,2048]{1,0:T(8,128)(2,1)S(1)}, u32[]{:S(2)}, u32[]{:S(2)}) %collective-permute-start.9) | collective-permute-done | bytes 524320 | tf_op jit(solution)/shard_map/ppermute | solution.py:187
  203.4 10.3 %all-to-all-start.2 = ((bf16[64,4,2176]{2,1,0:T(4,128)(2,1)}), bf16[64,4,2176]{2,1,0:T(4,128)(2,1)S(1)}, u32[]{:S(2)}, u32[]{:S(2)}) async-start(bf16[64,4,2176]{2,1,0:T(4,128)(2,1)} %reshape.222), calls=%async_computation.2 | async-start | bytes 2228224 | tf_op jit(solution)/shard_map/all_to_all | solution.py:357
  216.2 2.2 reshape.227.flat_ref
  218.3 25.6 %all-to-all-done.2 = bf16[64,4,2176]{2,1,0:T(4,128)(2,1)S(1)} async-done(((bf16[64,4,2176]{2,1,0:T(4,128)(2,1)}), bf16[64,4,2176]{2,1,0:T(4,128)(2,1)S(1)}, u32[]{:S(2)}, u32[]{:S(2)}) %all-to-all-start.2) | async-done | bytes 1114144 | tf_op jit(solution)/shard_map/all_to_all | solution.py:357
  244.6 3.6 %shard_map.169 = bf16[1024,256]{1,0:T(8,128)(2,1)} custom-call(f32[1024,256]{1,0:T(8,128)} %get-tuple-element.22.raw_ref, bf16[1024,256]{1,0:T(8,128)(2,1)} %get-tuple-element.23.qdec_ref, bf16[256,128]{1,0:T(8,128)(2,1)} %bitcast.94, bf16[1024,256]{1,0:T(8,128)(2,1)} %gate_ref.1, f32[1,256]{1,0:T(1,128)} %bitcast.97), custom_call_target="tpu_custom_call" | custom-call | flops 2000000000 | bytes 4194304 | tf_op jit(solution)/shard_map/pallas_call | solution.py:176
  248.1 3.7 %collective-permute-start.11 = (bf16[1024,256]{1,0:T(8,128)(2,1)}, bf16[1024,256]{1,0:T(8,128)(2,1)}, u32[]{:S(2)}, u32[]{:S(2)}) collective-permute-start(bf16[1024,256]{1,0:T(8,128)(2,1)} %shard_map.169), channel_id=1, source_target_pairs={{0,3},{1,0},{2,1},{3,2},{4,7},{5,4},{6,5},{7,6},{8,11},{9,8},{10,9... | collective-permute-start | bytes 1572872 | tf_op jit(solution)/shard_map/ppermute | solution.py:187
  253.7 2.3 fusion.1.partial_ref
  256.0 3.1 %shard_map.170 = bf16[128,2048]{1,0:T(8,128)(2,1)} custom-call(bf16[256,2048]{1,0:T(8,128)(2,1)} %reshape.227.flat_ref, bf16[256,128]{1,0:T(8,128)(2,1)} %fusion.66.coarse_ref, bf16[256,128]{1,0:T(8,128)(2,1)} %subtract_convert_fusion.fine_ref, f32[128,2048]{1,0:T(8,128)} %fusion.1.partial_ref, f32[1,2048]{1,0:T(1,128)} %bitcast.95), custom_call_target="tpu_custom_call" | custom-call | flops 268435456 | bytes 4194304 | tf_op jit(solution)/shard_map/pallas_call | solution.py:334
  263.2 3.8 %collective-permute-start.13 = (bf16[512,256]{1,0:T(8,128)(2,1)S(1)}, bf16[512,256]{1,0:T(8,128)(2,1)S(1)}, u32[]{:S(2)}, u32[]{:S(2)}) collective-permute-start(bf16[512,256]{1,0:T(8,128)(2,1)S(1)} %slice.94), channel_id=1, source_target_pairs={{0,3},{1,0},{2,1},{3,2},{4,7},{5,4},{6,5},{7,6},{8,11},{9,8},{10,9... | collective-permute-start | bytes 786440 | tf_op jit(solution)/shard_map/ppermute | solution.py:187
  271.0 4.6 %collective-permute-done.12 = bf16[512,256]{1,0:T(8,128)(2,1)S(1)} collective-permute-done((bf16[512,256]{1,0:T(8,128)(2,1)S(1)}, bf16[512,256]{1,0:T(8,128)(2,1)S(1)}, u32[]{:S(2)}, u32[]{:S(2)}) %collective-permute-start.12) | collective-permute-done | bytes 262176 | tf_op jit(solution)/shard_map/ppermute | solution.py:187
  (99 shorter events, 41.9 us)
Async XLA Ops:
  2.3 3.3 %copy-start.12 = (f32[2048]{0:T(1024)S(1)}, f32[2048]{0:T(1024)}, u32[]{:S(2)}) copy-start(f32[2048]{0:T(1024)} %param.27) | copy-start | bytes 24580
  7.7 63.5 %all-to-all-start = ((bf16[64,8,2048]{2,1,0:T(8,128)(2,1)}), bf16[64,8,2048]{2,1,0:T(8,128)(2,1)}, u32[]{:S(2)}, u32[]{:S(2)}) async-start(bf16[64,8,2048]{2,1,0:T(8,128)(2,1)} %fusion), calls=%async_computation | async-start | bytes 4194304 | tf_op jit(solution)/shard_map/all_to_all | solution.py:357
  20.0 6.4 %copy-start.1 = (bf16[1,2048,512]{2,1,0:T(8,128)(2,1)S(1)}, bf16[1,2048,512]{2,1,0:T(8,128)(2,1)}, u32[]{:S(2)}) copy-start(bf16[1,2048,512]{2,1,0:T(8,128)(2,1)} %param.30) | copy-start | bytes 6291460
  23.2 27.5 %collective-permute-start.2 = (bf16[2048,256]{1,0:T(8,128)(2,1)}, bf16[2048,256]{1,0:T(8,128)(2,1)S(1)}, u32[]{:S(2)}, u32[]{:S(2)}) collective-permute-start(bf16[2048,256]{1,0:T(8,128)(2,1)} %get-tuple-element.40), channel_id=1, source_target_pairs={{0,1},{1,2},{2,3},{3,0},{4,5},{5,6},{6,7},{7,4},{8,9},{9,10},{10,1... | collective-permute-start | bytes 3145736 | tf_op jit(solution)/shard_map/ppermute | solution.py:187
  24.7 53.5 %collective-permute-start.1 = (bf16[2048,256]{1,0:T(8,128)(2,1)}, bf16[2048,256]{1,0:T(8,128)(2,1)}, u32[]{:S(2)}, u32[]{:S(2)}) collective-permute-start(bf16[2048,256]{1,0:T(8,128)(2,1)} %get-tuple-element.41), channel_id=1, source_target_pairs={{0,3},{1,0},{2,1},{3,2},{4,7},{5,4},{6,5},{7,6},{8,11},{9,8},{10,9... | collective-permute-start | bytes 3145736 | tf_op jit(solution)/shard_map/ppermute | solution.py:187
  26.4 6.3 %copy-start.13 = (f32[1024,2]{0,1:T(2,128)S(1)}, f32[1024,2]{0,1:T(2,128)}, u32[]{:S(2)}) copy-start(f32[1024,2]{0,1:T(2,128)} %param.21) | copy-start | bytes 24580
  27.9 55.0 %collective-permute-start.3 = (bf16[2048,256]{1,0:T(8,128)(2,1)}, bf16[2048,256]{1,0:T(8,128)(2,1)}, u32[]{:S(2)}, u32[]{:S(2)}) collective-permute-start(bf16[2048,256]{1,0:T(8,128)(2,1)} %get-tuple-element.27), channel_id=1, source_target_pairs={{0,3},{1,0},{2,1},{3,2},{4,7},{5,4},{6,5},{7,6},{8,11},{9,8},{10,9... | collective-permute-start | bytes 3145736 | tf_op jit(solution)/shard_map/ppermute | solution.py:187
  29.5 56.4 %collective-permute-start.4 = (bf16[2048,256]{1,0:T(8,128)(2,1)}, bf16[2048,256]{1,0:T(8,128)(2,1)}, u32[]{:S(2)}, u32[]{:S(2)}) collective-permute-start(bf16[2048,256]{1,0:T(8,128)(2,1)} %get-tuple-element.28), channel_id=1, source_target_pairs={{0,1},{1,2},{2,3},{3,0},{4,5},{5,6},{6,7},{7,4},{8,9},{9,10},{10,1... | collective-permute-start | bytes 3145736 | tf_op jit(solution)/shard_map/ppermute | solution.py:187
  30.0 86.6 %collective-permute-start.5 = (bf16[256,2048]{1,0:T(8,128)(2,1)}, bf16[256,2048]{1,0:T(8,128)(2,1)}, u32[]{:S(2)}, u32[]{:S(2)}) collective-permute-start(bf16[256,2048]{1,0:T(8,128)(2,1)} %get-tuple-element.29), channel_id=1, source_target_pairs={{0,3},{1,0},{2,1},{3,2},{4,7},{5,4},{6,5},{7,6},{8,11},{9,8},{10,9... | collective-permute-start | bytes 3145736 | tf_op jit(solution)/shard_map/ppermute | solution.py:187
  50.7 8.9 %copy-start.2 = (bf16[2048,256]{1,0:T(8,128)(2,1)}, bf16[2048,256]{1,0:T(8,128)(2,1)S(1)}, u32[]{:S(2)}) copy-start(bf16[2048,256]{1,0:T(8,128)(2,1)S(1)} %collective-permute-done.2.gate_left) | copy-start | bytes 3145732
  50.7 66.0 %collective-permute-start.6 = (bf16[256,2048]{1,0:T(8,128)(2,1)}, bf16[256,2048]{1,0:T(8,128)(2,1)}, u32[]{:S(2)}, u32[]{:S(2)}) collective-permute-start(bf16[256,2048]{1,0:T(8,128)(2,1)} %get-tuple-element.30), channel_id=1, source_target_pairs={{0,1},{1,2},{2,3},{3,0},{4,5},{5,6},{6,7},{7,4},{8,9},{9,10},{10,1... | collective-permute-start | bytes 3145736 | tf_op jit(solution)/shard_map/ppermute | solution.py:187
  71.2 71.6 %all-to-all-start.1 = ((f32[64,4,256]{2,1,0:T(4,128)}), f32[64,4,256]{2,1,0:T(4,128)S(1)}, u32[]{:S(2)}, u32[]{:S(2)}) async-start(f32[64,4,256]{2,1,0:T(4,128)} %reshape.220), calls=%async_computation.1 | async-start | bytes 524288 | tf_op jit(solution)/shard_map/all_to_all | solution.py:357
  78.2 39.2 %copy-start.4 = (bf16[128,2048]{1,0:T(8,128)(2,1)}, bf16[128,2048]{1,0:T(8,128)(2,1)S(1)}, u32[]{:S(2)}) copy-start(bf16[128,2048]{1,0:T(8,128)(2,1)S(1)} %convolution_convert_fusion.1.own) | copy-start | bytes 1572868
  78.2 38.4 %collective-permute-start.16 = (bf16[128,2048]{1,0:T(8,128)(2,1)S(1)}, bf16[128,2048]{1,0:T(8,128)(2,1)S(1)}, u32[]{:S(2)}, u32[]{:S(2)}) collective-permute-start(bf16[128,2048]{1,0:T(8,128)(2,1)S(1)} %convolution_convert_fusion.1.own), channel_id=1, source_target_pairs={{0,2},{1,3},{2,0},{3,1},{4,6},{5,7},{6,4},{7,5},{8,10},{9,11},{10,... | collective-permute-start | bytes 1572872 | tf_op jit(solution)/shard_map/ppermute | solution.py:187
  82.9 42.3 %copy-start.3 = (bf16[128,2048]{1,0:T(8,128)(2,1)}, bf16[128,2048]{1,0:T(8,128)(2,1)S(1)}, u32[]{:S(2)}) copy-start(bf16[128,2048]{1,0:T(8,128)(2,1)S(1)} %convolution_convert_fusion.2.own) | copy-start | bytes 1572868
  82.9 42.5 %collective-permute-start.14 = (bf16[128,2048]{1,0:T(8,128)(2,1)S(1)}, bf16[128,2048]{1,0:T(8,128)(2,1)}, u32[]{:S(2)}, u32[]{:S(2)}) collective-permute-start(bf16[128,2048]{1,0:T(8,128)(2,1)S(1)} %convolution_convert_fusion.2.own), channel_id=1, source_target_pairs={{0,2},{1,3},{2,0},{3,1},{4,6},{5,7},{6,4},{7,5},{8,10},{9,11},{10,... | collective-permute-start | bytes 1572872 | tf_op jit(solution)/shard_map/ppermute | solution.py:187
  125.2 20.0 %collective-permute-start.17 = (bf16[128,2048]{1,0:T(8,128)(2,1)}, bf16[128,2048]{1,0:T(8,128)(2,1)}, u32[]{:S(2)}, u32[]{:S(2)}) collective-permute-start(bf16[128,2048]{1,0:T(8,128)(2,1)} %get-tuple-element.39), channel_id=1, source_target_pairs={{0,2},{1,3},{2,0},{3,1},{4,6},{5,7},{6,4},{7,5},{8,10},{9,11},{10,... | collective-permute-start | bytes 1572872 | tf_op jit(solution)/shard_map/ppermute | solution.py:187
  133.2 12.0 %copy-start.6 = (bf16[128,2048]{1,0:T(8,128)(2,1)S(1)}, bf16[128,2048]{1,0:T(8,128)(2,1)}, u32[]{:S(2)}) copy-start(bf16[128,2048]{1,0:T(8,128)(2,1)} %get-tuple-element.38) | copy-start | bytes 1572868
  133.2 20.1 %copy-start.7 = (bf16[128,2048]{1,0:T(8,128)(2,1)S(1)}, bf16[128,2048]{1,0:T(8,128)(2,1)}, u32[]{:S(2)}) copy-start(bf16[128,2048]{1,0:T(8,128)(2,1)} %get-tuple-element.36) | copy-start | bytes 1572868
  133.2 20.1 %collective-permute-start.15 = (bf16[128,2048]{1,0:T(8,128)(2,1)}, bf16[128,2048]{1,0:T(8,128)(2,1)}, u32[]{:S(2)}, u32[]{:S(2)}) collective-permute-start(bf16[128,2048]{1,0:T(8,128)(2,1)} %get-tuple-element.37), channel_id=1, source_target_pairs={{0,2},{1,3},{2,0},{3,1},{4,6},{5,7},{6,4},{7,5},{8,10},{9,11},{10,... | collective-permute-start | bytes 1572872 | tf_op jit(solution)/shard_map/ppermute | solution.py:187
  139.2 27.1 %collective-permute-start = (bf16[128,2048]{1,0:T(8,128)(2,1)}, bf16[128,2048]{1,0:T(8,128)(2,1)}, u32[]{:S(2)}, u32[]{:S(2)}) collective-permute-start(bf16[128,2048]{1,0:T(8,128)(2,1)} %convolution_convert_fusion.4.own), channel_id=1, source_target_pairs={{0,2},{1,3},{2,0},{3,1},{4,6},{5,7},{6,4},{7,5},{8,10},{9,11},{10,... | collective-permute-start | bytes 1572872 | tf_op jit(solution)/shard_map/ppermute | solution.py:187
  139.3 35.0 %collective-permute-start.8 = (bf16[128,2048]{1,0:T(8,128)(2,1)}, bf16[128,2048]{1,0:T(8,128)(2,1)}, u32[]{:S(2)}, u32[]{:S(2)}) collective-permute-start(bf16[128,2048]{1,0:T(8,128)(2,1)} %convolution_convert_fusion.3.own), channel_id=1, source_target_pairs={{0,2},{1,3},{2,0},{3,1},{4,6},{5,7},{6,4},{7,5},{8,10},{9,11},{10,... | collective-permute-start | bytes 1572872 | tf_op jit(solution)/shard_map/ppermute | solution.py:187
  155.7 47.7 %all-to-all-start.3 = ((bf16[64,4,2048]{2,1,0:T(4,128)(2,1)}), bf16[64,4,2048]{2,1,0:T(4,128)(2,1)}, u32[]{:S(2)}, u32[]{:S(2)}) async-start(bf16[64,4,2048]{2,1,0:T(4,128)(2,1)} %reshape.226), calls=%async_computation.3 | async-start | bytes 2097152 | tf_op jit(solution)/shard_map/all_to_all | solution.py:357
  174.0 11.4 %copy-start.11 = (bf16[64,4,128]{2,1,0:T(4,128)(2,1)S(1)}, bf16[64,4,128]{2,1,0:T(4,128)(2,1)}, u32[]{:S(2)}) copy-start(bf16[64,4,128]{2,1,0:T(4,128)(2,1)} %shard_map.168) | copy-start | bytes 196612
  174.0 16.6 %copy-start.8 = (bf16[128,2048]{1,0:T(8,128)(2,1)S(1)}, bf16[128,2048]{1,0:T(8,128)(2,1)}, u32[]{:S(2)}) copy-start(bf16[128,2048]{1,0:T(8,128)(2,1)} %get-tuple-element.31) | copy-start | bytes 1572868
  174.0 16.6 %collective-permute-start.7 = (bf16[128,2048]{1,0:T(8,128)(2,1)}, bf16[128,2048]{1,0:T(8,128)(2,1)S(1)}, u32[]{:S(2)}, u32[]{:S(2)}) collective-permute-start(bf16[128,2048]{1,0:T(8,128)(2,1)} %get-tuple-element.32), channel_id=1, source_target_pairs={{0,2},{1,3},{2,0},{3,1},{4,6},{5,7},{6,4},{7,5},{8,10},{9,11},{10,... | collective-permute-start | bytes 1572872 | tf_op jit(solution)/shard_map/ppermute | solution.py:187
  182.0 19.0 %collective-permute-start.9 = (bf16[128,2048]{1,0:T(8,128)(2,1)}, bf16[128,2048]{1,0:T(8,128)(2,1)S(1)}, u32[]{:S(2)}, u32[]{:S(2)}) collective-permute-start(bf16[128,2048]{1,0:T(8,128)(2,1)} %get-tuple-element.35), channel_id=1, source_target_pairs={{0,2},{1,3},{2,0},{3,1},{4,6},{5,7},{6,4},{7,5},{8,10},{9,11},{10,... | collective-permute-start | bytes 1572872 | tf_op jit(solution)/shard_map/ppermute | solution.py:187
  203.4 40.5 %all-to-all-start.2 = ((bf16[64,4,2176]{2,1,0:T(4,128)(2,1)}), bf16[64,4,2176]{2,1,0:T(4,128)(2,1)S(1)}, u32[]{:S(2)}, u32[]{:S(2)}) async-start(bf16[64,4,2176]{2,1,0:T(4,128)(2,1)} %reshape.222), calls=%async_computation.2 | async-start | bytes 2228224 | tf_op jit(solution)/shard_map/all_to_all | solution.py:357
  248.1 14.1 %collective-permute-start.11 = (bf16[1024,256]{1,0:T(8,128)(2,1)}, bf16[1024,256]{1,0:T(8,128)(2,1)}, u32[]{:S(2)}, u32[]{:S(2)}) collective-permute-start(bf16[1024,256]{1,0:T(8,128)(2,1)} %shard_map.169), channel_id=1, source_target_pairs={{0,3},{1,0},{2,1},{3,2},{4,7},{5,4},{6,5},{7,6},{8,11},{9,8},{10,9... | collective-permute-start | bytes 1572872 | tf_op jit(solution)/shard_map/ppermute | solution.py:187
  251.8 15.2 %collective-permute-start.10 = (bf16[1024,256]{1,0:T(8,128)(2,1)}, bf16[1024,256]{1,0:T(8,128)(2,1)}, u32[]{:S(2)}, u32[]{:S(2)}) collective-permute-start(bf16[1024,256]{1,0:T(8,128)(2,1)} %shard_map.169), channel_id=1, source_target_pairs={{0,1},{1,2},{2,3},{3,0},{4,5},{5,6},{6,7},{7,4},{8,9},{9,10},{10,1... | collective-permute-start | bytes 1572872 | tf_op jit(solution)/shard_map/ppermute | solution.py:187
  263.2 7.8 %collective-permute-start.13 = (bf16[512,256]{1,0:T(8,128)(2,1)S(1)}, bf16[512,256]{1,0:T(8,128)(2,1)S(1)}, u32[]{:S(2)}, u32[]{:S(2)}) collective-permute-start(bf16[512,256]{1,0:T(8,128)(2,1)S(1)} %slice.94), channel_id=1, source_target_pairs={{0,3},{1,0},{2,1},{3,2},{4,7},{5,4},{6,5},{7,6},{8,11},{9,8},{10,9... | collective-permute-start | bytes 786440 | tf_op jit(solution)/shard_map/ppermute | solution.py:187
  267.9 7.7 %collective-permute-start.12 = (bf16[512,256]{1,0:T(8,128)(2,1)S(1)}, bf16[512,256]{1,0:T(8,128)(2,1)S(1)}, u32[]{:S(2)}, u32[]{:S(2)}) collective-permute-start(bf16[512,256]{1,0:T(8,128)(2,1)S(1)} %slice.93), channel_id=1, source_target_pairs={{0,1},{1,2},{2,3},{3,0},{4,5},{5,6},{6,7},{7,4},{8,9},{9,10},{10,1... | collective-permute-start | bytes 786440 | tf_op jit(solution)/shard_map/ppermute | solution.py:187
  (4 other events, 6.2 us)

commit v4 on v3

--- a/solution.py
+++ b/solution.py
@@ -233,18 +233,21 @@
     for f in range(tiles):
         to = down_w.at[places[f], :]
         loads.append(pltpu.make_async_copy(downs[f], to, sems.at[2 + 2 * tiles + f]))
-    for load in loads:
+    batches = [loads[:4], loads[4:6]]
+    batches += [loads[2 + 2 * f : 4 + 2 * f] for f in range(2, tiles)]
+    batches += [loads[2 + 2 * tiles : 4 + 2 * tiles], loads[4 + 2 * tiles :]]
+    for load in batches[0] + batches[1]:
         load.start()
-    loads[0].wait()
-    loads[1].wait()
 
     def hidden_tile(f, carry):
         for k in range(tiles):
 
             @pl.when(f == k)
             def _():
-                loads[2 + 2 * k].wait()
-                loads[3 + 2 * k].wait()
+                for load in batches[k]:
+                    load.wait()
+                for load in batches[k + 2]:
+                    load.start()
 
         at = pl.ds(pl.multiple_of(f * tile, tile), tile)
         gate = jnp.dot(rows[...], gate_w[:, at], preferred_element_type=F32)

time: 279 us -> 281 us (level)
  Pallas kernels: 47.9 us -> 52 us
    pallas_call x4, Pallas kernels: 30.9 us -> 35 us  [expert_block(): pl.pallas_call(expert_kernel, out_shape=[jax.ShapeDtypeStruct((n, feature...]
  transfers between devices with their start and end apart: 22 -> 22, of which waited for: 9 -> 9; matrix products, arithmetic and copies ran while one was open for 13% -> 13% of each run, Pallas kernels for 16% -> 17%
where the time goes in v4:
time: 281 us; the launch traced here: 279 us
  waiting for transfers between devices  110 us (39%)
  starting transfers between devices  69.1 us (25%)
  Pallas kernels  52 us (19%)
  local copies, waits for them, and re-layouts  22.2 us (8%)
  matrix products  19.6 us (7%)
  other arithmetic  5.47 us (2%)
    ppermute x18, waiting for transfers between devices, shift(): return lax.ppermute(x, 'tp', [(i, (i + by) % n) for i in range(n)])  74.2 us
    all_to_all x4, starting transfers between devices, exchange(): return lax.all_to_all(x, EP, split_axis=0, concat_axis=0, tiled=True)  38.5 us
    all_to_all x4, waiting for transfers between devices, exchange(): return lax.all_to_all(x, EP, split_axis=0, concat_axis=0, tiled=True)  35.4 us
    pallas_call x4, Pallas kernels, expert_block(): pl.pallas_call(expert_kernel, out_shape=[jax.ShapeDtypeStruct((n, feature...  35 us
    ppermute x18, starting transfers between devices, shift(): return lax.ppermute(x, 'tp', [(i, (i + by) % n) for i in range(n)])  30.6 us
    pallas_call x1, Pallas kernels, local_pass(): vmem_call(local_kernel, (jax.ShapeDtypeStruct((rows, width), F32), jax.Sh...  8.65 us
    dot_general x4, matrix products, shards(): jnp.dot(chosen.astype(BF16), flat_in[c], preferred_element_type=F32)  7.91 us
    slice x3, local copies, waits for them, and re-layouts, halves(): lax.slice_in_dim(weight, half, 2 * half, axis=dim)  7.78 us
  transfers between devices with their start and end apart: 22, of which 9 were waited for; matrix products, arithmetic and copies ran while one was open for 13% of the time, Pallas kernels for 17%

profile of v4, /device:TPU:8, one launch (start us, length us, event | category | flops | bytes accessed | tf_op | source)
XLA Modules:
  0.0 279.1 jit_solution(4561923652336977056)
XLA Ops:
  2.3 3.1 %slice_bitcast_fusion = (bf16[256,2048]{1,0:T(8,128)(2,1)}, bf16[256,2048]{1,0:T(8,128)(2,1)}) fusion(bf16[1,512,2048]{2,1,0:T(8,128)(2,1)} %param.31), kind=kLoop, calls=%fused_computation.26 | loop fusion | bytes 4194304 | tf_op jit(solution)/shard_map/slice | solution.py:350
  7.7 12.3 %all-to-all-start = ((bf16[64,8,2048]{2,1,0:T(8,128)(2,1)}), bf16[64,8,2048]{2,1,0:T(8,128)(2,1)}, u32[]{:S(2)}, u32[]{:S(2)}) async-start(bf16[64,8,2048]{2,1,0:T(8,128)(2,1)} %fusion), calls=%async_computation | async-start | bytes 4194304 | tf_op jit(solution)/shard_map/all_to_all | solution.py:360
  20.0 3.2 %fusion.68 = (bf16[2048,256]{1,0:T(8,128)(2,1)}, bf16[2048,256]{1,0:T(8,128)(2,1)}) fusion(bf16[2048,512]{1,0:T(8,128)(2,1)} %bitcast.68), kind=kLoop, calls=%fused_computation.108 | loop fusion | bytes 4194304 | tf_op jit(solution)/shard_map/slice | solution.py:350
  30.0 2.8 collective-permute-start.5
  33.8 16.9 %collective-permute-done.2.gate_left = bf16[2048,256]{1,0:T(8,128)(2,1)S(1)} collective-permute-done((bf16[2048,256]{1,0:T(8,128)(2,1)}, bf16[2048,256]{1,0:T(8,128)(2,1)S(1)}, u32[]{:S(2)}, u32[]{:S(2)}) %collective-permute-start.2) | collective-permute-done | bytes 1048608 | tf_op jit(solution)/shard_map/ppermute | solution.py:187
  50.9 8.6 %shard_map.167 = (f32[1024,256]{1,0:T(8,128)}, bf16[1024,256]{1,0:T(8,128)(2,1)}, f32[256,256]{1,0:T(8,128)}) custom-call(bf16[1024,256]{1,0:T(8,128)(2,1)} %q_ref.1, bf16[1024,256]{1,0:T(8,128)(2,1)} %r_ref, bf16[1024,256]{1,0:T(8,128)(2,1)} %v_ref.1, f32[1,256]{1,0:T(1,128)} %bitcast.96, f32[1024,2]{1,0:T(8,128)} %copy.30.fade_ref), custom_call_target="tpu_custom_call" | custom-call | flops 4000000000 | bytes 6291456 | tf_op jit(solution)/shard_map/pallas_call | solution.py:151
  61.3 9.8 %all-to-all-done = bf16[64,8,2048]{2,1,0:T(8,128)(2,1)} async-done(((bf16[64,8,2048]{2,1,0:T(8,128)(2,1)}), bf16[64,8,2048]{2,1,0:T(8,128)(2,1)}, u32[]{:S(2)}, u32[]{:S(2)}) %all-to-all-start) | async-done | bytes 2097184 | tf_op jit(solution)/shard_map/all_to_all | solution.py:360
  71.2 5.4 %all-to-all-start.1 = ((f32[64,4,256]{2,1,0:T(4,128)}), f32[64,4,256]{2,1,0:T(4,128)S(1)}, u32[]{:S(2)}, u32[]{:S(2)}) async-start(f32[64,4,256]{2,1,0:T(4,128)} %reshape.220), calls=%async_computation.1 | async-start | bytes 524288 | tf_op jit(solution)/shard_map/all_to_all | solution.py:360
  78.2 3.1 %collective-permute-start.16 = (bf16[128,2048]{1,0:T(8,128)(2,1)S(1)}, bf16[128,2048]{1,0:T(8,128)(2,1)S(1)}, u32[]{:S(2)}, u32[]{:S(2)}) collective-permute-start(bf16[128,2048]{1,0:T(8,128)(2,1)S(1)} %convolution_convert_fusion.1.own), channel_id=1, source_target_pairs={{0,2},{1,3},{2,0},{3,1},{4,6},{5,7},{6,4},{7,5},{8,10},{9,11},{10,... | collective-permute-start | bytes 1572872 | tf_op jit(solution)/shard_map/ppermute | solution.py:187
  83.5 2.4 convolution_convert_fusion.3.own
  85.9 30.7 %collective-permute-done.5.down_right = bf16[256,2048]{1,0:T(8,128)(2,1)} collective-permute-done((bf16[256,2048]{1,0:T(8,128)(2,1)}, bf16[256,2048]{1,0:T(8,128)(2,1)}, u32[]{:S(2)}, u32[]{:S(2)}) %collective-permute-start.5) | collective-permute-done | bytes 1048608 | tf_op jit(solution)/shard_map/ppermute | solution.py:187
  117.4 8.8 %expert_block.7 = (bf16[128,2048]{1,0:T(8,128)(2,1)}, bf16[128,2048]{1,0:T(8,128)(2,1)}) custom-call(bf16[128,2048]{1,0:T(8,128)(2,1)} %copy-done.4, bf16[128,2048]{1,0:T(8,128)(2,1)} %copy-done.9, bf16[2048,512]{1,0:T(8,128)(2,1)} %bitcast.69, bf16[2048,256]{1,0:T(8,128)(2,1)} %collective-permute-done.1.gate_right, bf16[2048,256]{1,0:T(8,128)(2,1)} %copy-done.2, ...), custom_call_target="tpu_custom_call" | custom-call | flops 3221225472 | bytes 14680064 | tf_op jit(solution)/shard_map/expert_block/pallas_call | solution.py:302
  126.5 8.8 %expert_block.6 = (bf16[128,2048]{1,0:T(8,128)(2,1)}, bf16[128,2048]{1,0:T(8,128)(2,1)}) custom-call(bf16[128,2048]{1,0:T(8,128)(2,1)} %copy-done.3, bf16[128,2048]{1,0:T(8,128)(2,1)} %collective-permute-done.14.far, bf16[2048,512]{1,0:T(8,128)(2,1)} %bitcast.70, bf16[2048,256]{1,0:T(8,128)(2,1)} %collective-permute-done.1.gate_right, ...), custom_call_target="tpu_custom_call" | custom-call | flops 3221225472 | bytes 14680064 | tf_op jit(solution)/shard_map/expert_block/pallas_call | solution.py:302
  135.3 3.6 %collective-permute-start.15 = (bf16[128,2048]{1,0:T(8,128)(2,1)}, bf16[128,2048]{1,0:T(8,128)(2,1)}, u32[]{:S(2)}, u32[]{:S(2)}) collective-permute-start(bf16[128,2048]{1,0:T(8,128)(2,1)} %get-tuple-element.37), channel_id=1, source_target_pairs={{0,2},{1,3},{2,0},{3,1},{4,6},{5,7},{6,4},{7,5},{8,10},{9,11},{10,... | collective-permute-start | bytes 1572872 | tf_op jit(solution)/shard_map/ppermute | solution.py:187
  138.9 2.4 convolution_convert_fusion.4.own
  141.4 3.4 %collective-permute-start.8 = (bf16[128,2048]{1,0:T(8,128)(2,1)}, bf16[128,2048]{1,0:T(8,128)(2,1)}, u32[]{:S(2)}, u32[]{:S(2)}) collective-permute-start(bf16[128,2048]{1,0:T(8,128)(2,1)} %convolution_convert_fusion.3.own), channel_id=1, source_target_pairs={{0,2},{1,3},{2,0},{3,1},{4,6},{5,7},{6,4},{7,5},{8,10},{9,11},{10,... | collective-permute-start | bytes 1572872 | tf_op jit(solution)/shard_map/ppermute | solution.py:187
  148.4 5.9 %collective-permute-done.15 = bf16[128,2048]{1,0:T(8,128)(2,1)} collective-permute-done((bf16[128,2048]{1,0:T(8,128)(2,1)}, bf16[128,2048]{1,0:T(8,128)(2,1)}, u32[]{:S(2)}, u32[]{:S(2)}) %collective-permute-start.15) | collective-permute-done | bytes 524320 | tf_op jit(solution)/shard_map/ppermute | solution.py:187
  156.8 10.5 %all-to-all-start.3 = ((bf16[64,4,2048]{2,1,0:T(4,128)(2,1)}), bf16[64,4,2048]{2,1,0:T(4,128)(2,1)}, u32[]{:S(2)}, u32[]{:S(2)}) async-start(bf16[64,4,2048]{2,1,0:T(4,128)(2,1)} %reshape.226), calls=%async_computation.3 | async-start | bytes 2097152 | tf_op jit(solution)/shard_map/all_to_all | solution.py:360
  167.3 8.8 %expert_block.4 = (bf16[128,2048]{1,0:T(8,128)(2,1)}, bf16[128,2048]{1,0:T(8,128)(2,1)}) custom-call(bf16[128,2048]{1,0:T(8,128)(2,1)} %convolution_convert_fusion.4.own, bf16[128,2048]{1,0:T(8,128)(2,1)} %collective-permute-done.far, bf16[2048,512]{1,0:T(8,128)(2,1)} %bitcast.71, bf16[2048,256]{1,0:T(8,128)(2,1)} %collective-permute-done.1.gate_right, ...), custom_call_target="tpu_custom_call" | custom-call | flops 3221225472 | bytes 14680064 | tf_op jit(solution)/shard_map/expert_block/pallas_call | solution.py:302
  177.3 8.7 %expert_block.5 = (bf16[128,2048]{1,0:T(8,128)(2,1)}, bf16[128,2048]{1,0:T(8,128)(2,1)}) custom-call(bf16[128,2048]{1,0:T(8,128)(2,1)} %convolution_convert_fusion.3.own, bf16[128,2048]{1,0:T(8,128)(2,1)} %collective-permute-done.8.far, bf16[2048,512]{1,0:T(8,128)(2,1)} %bitcast.72, bf16[2048,256]{1,0:T(8,128)(2,1)} %collective-permute-done.1.gate_right, ...), custom_call_target="tpu_custom_call" | custom-call | flops 3221225472 | bytes 14680064 | tf_op jit(solution)/shard_map/expert_block/pallas_call | solution.py:302
  186.1 2.5 collective-permute-start.9
  188.6 4.1 %collective-permute-done.7 = bf16[128,2048]{1,0:T(8,128)(2,1)S(1)} collective-permute-done((bf16[128,2048]{1,0:T(8,128)(2,1)}, bf16[128,2048]{1,0:T(8,128)(2,1)S(1)}, u32[]{:S(2)}, u32[]{:S(2)}) %collective-permute-start.7) | collective-permute-done | bytes 524320 | tf_op jit(solution)/shard_map/ppermute | solution.py:187
  192.8 10.2 %collective-permute-done.9 = bf16[128,2048]{1,0:T(8,128)(2,1)S(1)} collective-permute-done((bf16[128,2048]{1,0:T(8,128)(2,1)}, bf16[128,2048]{1,0:T(8,128)(2,1)S(1)}, u32[]{:S(2)}, u32[]{:S(2)}) %collective-permute-start.9) | collective-permute-done | bytes 524320 | tf_op jit(solution)/shard_map/ppermute | solution.py:187
  205.5 10.3 %all-to-all-start.2 = ((bf16[64,4,2176]{2,1,0:T(4,128)(2,1)}), bf16[64,4,2176]{2,1,0:T(4,128)(2,1)S(1)}, u32[]{:S(2)}, u32[]{:S(2)}) async-start(bf16[64,4,2176]{2,1,0:T(4,128)(2,1)} %reshape.222), calls=%async_computation.2 | async-start | bytes 2228224 | tf_op jit(solution)/shard_map/all_to_all | solution.py:360
  218.2 2.2 reshape.227.flat_ref
  220.4 25.6 %all-to-all-done.2 = bf16[64,4,2176]{2,1,0:T(4,128)(2,1)S(1)} async-done(((bf16[64,4,2176]{2,1,0:T(4,128)(2,1)}), bf16[64,4,2176]{2,1,0:T(4,128)(2,1)S(1)}, u32[]{:S(2)}, u32[]{:S(2)}) %all-to-all-start.2) | async-done | bytes 1114144 | tf_op jit(solution)/shard_map/all_to_all | solution.py:360
  246.6 3.6 %shard_map.169 = bf16[1024,256]{1,0:T(8,128)(2,1)} custom-call(f32[1024,256]{1,0:T(8,128)} %get-tuple-element.22.raw_ref, bf16[1024,256]{1,0:T(8,128)(2,1)} %get-tuple-element.23.qdec_ref, bf16[256,128]{1,0:T(8,128)(2,1)} %bitcast.94, bf16[1024,256]{1,0:T(8,128)(2,1)} %gate_ref.1, f32[1,256]{1,0:T(1,128)} %bitcast.97), custom_call_target="tpu_custom_call" | custom-call | flops 2000000000 | bytes 4194304 | tf_op jit(solution)/shard_map/pallas_call | solution.py:176
  250.2 3.7 %collective-permute-start.11 = (bf16[1024,256]{1,0:T(8,128)(2,1)}, bf16[1024,256]{1,0:T(8,128)(2,1)}, u32[]{:S(2)}, u32[]{:S(2)}) collective-permute-start(bf16[1024,256]{1,0:T(8,128)(2,1)} %shard_map.169), channel_id=1, source_target_pairs={{0,3},{1,0},{2,1},{3,2},{4,7},{5,4},{6,5},{7,6},{8,11},{9,8},{10,9... | collective-permute-start | bytes 1572872 | tf_op jit(solution)/shard_map/ppermute | solution.py:187
  255.8 2.3 fusion.1.partial_ref
  258.0 3.1 %shard_map.170 = bf16[128,2048]{1,0:T(8,128)(2,1)} custom-call(bf16[256,2048]{1,0:T(8,128)(2,1)} %reshape.227.flat_ref, bf16[256,128]{1,0:T(8,128)(2,1)} %fusion.66.coarse_ref, bf16[256,128]{1,0:T(8,128)(2,1)} %subtract_convert_fusion.fine_ref, f32[128,2048]{1,0:T(8,128)} %fusion.1.partial_ref, f32[1,2048]{1,0:T(1,128)} %bitcast.95), custom_call_target="tpu_custom_call" | custom-call | flops 268435456 | bytes 4194304 | tf_op jit(solution)/shard_map/pallas_call | solution.py:337
  265.3 3.8 %collective-permute-start.13 = (bf16[512,256]{1,0:T(8,128)(2,1)S(1)}, bf16[512,256]{1,0:T(8,128)(2,1)S(1)}, u32[]{:S(2)}, u32[]{:S(2)}) collective-permute-start(bf16[512,256]{1,0:T(8,128)(2,1)S(1)} %slice.94), channel_id=1, source_target_pairs={{0,3},{1,0},{2,1},{3,2},{4,7},{5,4},{6,5},{7,6},{8,11},{9,8},{10,9... | collective-permute-start | bytes 786440 | tf_op jit(solution)/shard_map/ppermute | solution.py:187
  273.1 4.6 %collective-permute-done.12 = bf16[512,256]{1,0:T(8,128)(2,1)S(1)} collective-permute-done((bf16[512,256]{1,0:T(8,128)(2,1)S(1)}, bf16[512,256]{1,0:T(8,128)(2,1)S(1)}, u32[]{:S(2)}, u32[]{:S(2)}) %collective-permute-start.12) | collective-permute-done | bytes 262176 | tf_op jit(solution)/shard_map/ppermute | solution.py:187
  (99 shorter events, 43.0 us)
Async XLA Ops:
  2.3 3.3 %copy-start.12 = (f32[2048]{0:T(1024)S(1)}, f32[2048]{0:T(1024)}, u32[]{:S(2)}) copy-start(f32[2048]{0:T(1024)} %param.27) | copy-start | bytes 24580
  7.7 63.5 %all-to-all-start = ((bf16[64,8,2048]{2,1,0:T(8,128)(2,1)}), bf16[64,8,2048]{2,1,0:T(8,128)(2,1)}, u32[]{:S(2)}, u32[]{:S(2)}) async-start(bf16[64,8,2048]{2,1,0:T(8,128)(2,1)} %fusion), calls=%async_computation | async-start | bytes 4194304 | tf_op jit(solution)/shard_map/all_to_all | solution.py:360
  20.0 6.4 %copy-start.1 = (bf16[1,2048,512]{2,1,0:T(8,128)(2,1)S(1)}, bf16[1,2048,512]{2,1,0:T(8,128)(2,1)}, u32[]{:S(2)}) copy-start(bf16[1,2048,512]{2,1,0:T(8,128)(2,1)} %param.30) | copy-start | bytes 6291460
  23.2 27.5 %collective-permute-start.2 = (bf16[2048,256]{1,0:T(8,128)(2,1)}, bf16[2048,256]{1,0:T(8,128)(2,1)S(1)}, u32[]{:S(2)}, u32[]{:S(2)}) collective-permute-start(bf16[2048,256]{1,0:T(8,128)(2,1)} %get-tuple-element.40), channel_id=1, source_target_pairs={{0,1},{1,2},{2,3},{3,0},{4,5},{5,6},{6,7},{7,4},{8,9},{9,10},{10,1... | collective-permute-start | bytes 3145736 | tf_op jit(solution)/shard_map/ppermute | solution.py:187
  24.7 53.5 %collective-permute-start.1 = (bf16[2048,256]{1,0:T(8,128)(2,1)}, bf16[2048,256]{1,0:T(8,128)(2,1)}, u32[]{:S(2)}, u32[]{:S(2)}) collective-permute-start(bf16[2048,256]{1,0:T(8,128)(2,1)} %get-tuple-element.41), channel_id=1, source_target_pairs={{0,3},{1,0},{2,1},{3,2},{4,7},{5,4},{6,5},{7,6},{8,11},{9,8},{10,9... | collective-permute-start | bytes 3145736 | tf_op jit(solution)/shard_map/ppermute | solution.py:187
  26.4 6.3 %copy-start.13 = (f32[1024,2]{0,1:T(2,128)S(1)}, f32[1024,2]{0,1:T(2,128)}, u32[]{:S(2)}) copy-start(f32[1024,2]{0,1:T(2,128)} %param.21) | copy-start | bytes 24580
  27.9 55.0 %collective-permute-start.3 = (bf16[2048,256]{1,0:T(8,128)(2,1)}, bf16[2048,256]{1,0:T(8,128)(2,1)}, u32[]{:S(2)}, u32[]{:S(2)}) collective-permute-start(bf16[2048,256]{1,0:T(8,128)(2,1)} %get-tuple-element.27), channel_id=1, source_target_pairs={{0,3},{1,0},{2,1},{3,2},{4,7},{5,4},{6,5},{7,6},{8,11},{9,8},{10,9... | collective-permute-start | bytes 3145736 | tf_op jit(solution)/shard_map/ppermute | solution.py:187
  29.5 56.4 %collective-permute-start.4 = (bf16[2048,256]{1,0:T(8,128)(2,1)}, bf16[2048,256]{1,0:T(8,128)(2,1)}, u32[]{:S(2)}, u32[]{:S(2)}) collective-permute-start(bf16[2048,256]{1,0:T(8,128)(2,1)} %get-tuple-element.28), channel_id=1, source_target_pairs={{0,1},{1,2},{2,3},{3,0},{4,5},{5,6},{6,7},{7,4},{8,9},{9,10},{10,1... | collective-permute-start | bytes 3145736 | tf_op jit(solution)/shard_map/ppermute | solution.py:187
  30.0 86.6 %collective-permute-start.5 = (bf16[256,2048]{1,0:T(8,128)(2,1)}, bf16[256,2048]{1,0:T(8,128)(2,1)}, u32[]{:S(2)}, u32[]{:S(2)}) collective-permute-start(bf16[256,2048]{1,0:T(8,128)(2,1)} %get-tuple-element.29), channel_id=1, source_target_pairs={{0,3},{1,0},{2,1},{3,2},{4,7},{5,4},{6,5},{7,6},{8,11},{9,8},{10,9... | collective-permute-start | bytes 3145736 | tf_op jit(solution)/shard_map/ppermute | solution.py:187
  50.7 8.9 %copy-start.2 = (bf16[2048,256]{1,0:T(8,128)(2,1)}, bf16[2048,256]{1,0:T(8,128)(2,1)S(1)}, u32[]{:S(2)}) copy-start(bf16[2048,256]{1,0:T(8,128)(2,1)S(1)} %collective-permute-done.2.gate_left) | copy-start | bytes 3145732
  50.7 66.0 %collective-permute-start.6 = (bf16[256,2048]{1,0:T(8,128)(2,1)}, bf16[256,2048]{1,0:T(8,128)(2,1)}, u32[]{:S(2)}, u32[]{:S(2)}) collective-permute-start(bf16[256,2048]{1,0:T(8,128)(2,1)} %get-tuple-element.30), channel_id=1, source_target_pairs={{0,1},{1,2},{2,3},{3,0},{4,5},{5,6},{6,7},{7,4},{8,9},{9,10},{10,1... | collective-permute-start | bytes 3145736 | tf_op jit(solution)/shard_map/ppermute | solution.py:187
  71.2 73.6 %all-to-all-start.1 = ((f32[64,4,256]{2,1,0:T(4,128)}), f32[64,4,256]{2,1,0:T(4,128)S(1)}, u32[]{:S(2)}, u32[]{:S(2)}) async-start(f32[64,4,256]{2,1,0:T(4,128)} %reshape.220), calls=%async_computation.1 | async-start | bytes 524288 | tf_op jit(solution)/shard_map/all_to_all | solution.py:360
  78.2 39.2 %copy-start.4 = (bf16[128,2048]{1,0:T(8,128)(2,1)}, bf16[128,2048]{1,0:T(8,128)(2,1)S(1)}, u32[]{:S(2)}) copy-start(bf16[128,2048]{1,0:T(8,128)(2,1)S(1)} %convolution_convert_fusion.1.own) | copy-start | bytes 1572868
  78.2 38.4 %collective-permute-start.16 = (bf16[128,2048]{1,0:T(8,128)(2,1)S(1)}, bf16[128,2048]{1,0:T(8,128)(2,1)S(1)}, u32[]{:S(2)}, u32[]{:S(2)}) collective-permute-start(bf16[128,2048]{1,0:T(8,128)(2,1)S(1)} %convolution_convert_fusion.1.own), channel_id=1, source_target_pairs={{0,2},{1,3},{2,0},{3,1},{4,6},{5,7},{6,4},{7,5},{8,10},{9,11},{10,... | collective-permute-start | bytes 1572872 | tf_op jit(solution)/shard_map/ppermute | solution.py:187
  82.9 43.3 %copy-start.3 = (bf16[128,2048]{1,0:T(8,128)(2,1)}, bf16[128,2048]{1,0:T(8,128)(2,1)S(1)}, u32[]{:S(2)}) copy-start(bf16[128,2048]{1,0:T(8,128)(2,1)S(1)} %convolution_convert_fusion.2.own) | copy-start | bytes 1572868
  82.9 43.6 %collective-permute-start.14 = (bf16[128,2048]{1,0:T(8,128)(2,1)S(1)}, bf16[128,2048]{1,0:T(8,128)(2,1)}, u32[]{:S(2)}, u32[]{:S(2)}) collective-permute-start(bf16[128,2048]{1,0:T(8,128)(2,1)S(1)} %convolution_convert_fusion.2.own), channel_id=1, source_target_pairs={{0,2},{1,3},{2,0},{3,1},{4,6},{5,7},{6,4},{7,5},{8,10},{9,11},{10,... | collective-permute-start | bytes 1572872 | tf_op jit(solution)/shard_map/ppermute | solution.py:187
  126.2 21.0 %collective-permute-start.17 = (bf16[128,2048]{1,0:T(8,128)(2,1)}, bf16[128,2048]{1,0:T(8,128)(2,1)}, u32[]{:S(2)}, u32[]{:S(2)}) collective-permute-start(bf16[128,2048]{1,0:T(8,128)(2,1)} %get-tuple-element.39), channel_id=1, source_target_pairs={{0,2},{1,3},{2,0},{3,1},{4,6},{5,7},{6,4},{7,5},{8,10},{9,11},{10,... | collective-permute-start | bytes 1572872 | tf_op jit(solution)/shard_map/ppermute | solution.py:187
  135.3 12.0 %copy-start.6 = (bf16[128,2048]{1,0:T(8,128)(2,1)S(1)}, bf16[128,2048]{1,0:T(8,128)(2,1)}, u32[]{:S(2)}) copy-start(bf16[128,2048]{1,0:T(8,128)(2,1)} %get-tuple-element.38) | copy-start | bytes 1572868
  135.3 19.0 %copy-start.7 = (bf16[128,2048]{1,0:T(8,128)(2,1)S(1)}, bf16[128,2048]{1,0:T(8,128)(2,1)}, u32[]{:S(2)}) copy-start(bf16[128,2048]{1,0:T(8,128)(2,1)} %get-tuple-element.36) | copy-start | bytes 1572868
  135.3 19.0 %collective-permute-start.15 = (bf16[128,2048]{1,0:T(8,128)(2,1)}, bf16[128,2048]{1,0:T(8,128)(2,1)}, u32[]{:S(2)}, u32[]{:S(2)}) collective-permute-start(bf16[128,2048]{1,0:T(8,128)(2,1)} %get-tuple-element.37), channel_id=1, source_target_pairs={{0,2},{1,3},{2,0},{3,1},{4,6},{5,7},{6,4},{7,5},{8,10},{9,11},{10,... | collective-permute-start | bytes 1572872 | tf_op jit(solution)/shard_map/ppermute | solution.py:187
  141.3 26.0 %collective-permute-start = (bf16[128,2048]{1,0:T(8,128)(2,1)}, bf16[128,2048]{1,0:T(8,128)(2,1)}, u32[]{:S(2)}, u32[]{:S(2)}) collective-permute-start(bf16[128,2048]{1,0:T(8,128)(2,1)} %convolution_convert_fusion.4.own), channel_id=1, source_target_pairs={{0,2},{1,3},{2,0},{3,1},{4,6},{5,7},{6,4},{7,5},{8,10},{9,11},{10,... | collective-permute-start | bytes 1572872 | tf_op jit(solution)/shard_map/ppermute | solution.py:187
  141.4 36.0 %collective-permute-start.8 = (bf16[128,2048]{1,0:T(8,128)(2,1)}, bf16[128,2048]{1,0:T(8,128)(2,1)}, u32[]{:S(2)}, u32[]{:S(2)}) collective-permute-start(bf16[128,2048]{1,0:T(8,128)(2,1)} %convolution_convert_fusion.3.own), channel_id=1, source_target_pairs={{0,2},{1,3},{2,0},{3,1},{4,6},{5,7},{6,4},{7,5},{8,10},{9,11},{10,... | collective-permute-start | bytes 1572872 | tf_op jit(solution)/shard_map/ppermute | solution.py:187
  156.8 48.7 %all-to-all-start.3 = ((bf16[64,4,2048]{2,1,0:T(4,128)(2,1)}), bf16[64,4,2048]{2,1,0:T(4,128)(2,1)}, u32[]{:S(2)}, u32[]{:S(2)}) async-start(bf16[64,4,2048]{2,1,0:T(4,128)(2,1)} %reshape.226), calls=%async_computation.3 | async-start | bytes 2097152 | tf_op jit(solution)/shard_map/all_to_all | solution.py:360
  176.1 12.5 %copy-start.11 = (bf16[64,4,128]{2,1,0:T(4,128)(2,1)S(1)}, bf16[64,4,128]{2,1,0:T(4,128)(2,1)}, u32[]{:S(2)}) copy-start(bf16[64,4,128]{2,1,0:T(4,128)(2,1)} %shard_map.168) | copy-start | bytes 196612
  176.1 16.6 %copy-start.8 = (bf16[128,2048]{1,0:T(8,128)(2,1)S(1)}, bf16[128,2048]{1,0:T(8,128)(2,1)}, u32[]{:S(2)}) copy-start(bf16[128,2048]{1,0:T(8,128)(2,1)} %get-tuple-element.31) | copy-start | bytes 1572868
  176.1 16.6 %collective-permute-start.7 = (bf16[128,2048]{1,0:T(8,128)(2,1)}, bf16[128,2048]{1,0:T(8,128)(2,1)S(1)}, u32[]{:S(2)}, u32[]{:S(2)}) collective-permute-start(bf16[128,2048]{1,0:T(8,128)(2,1)} %get-tuple-element.32), channel_id=1, source_target_pairs={{0,2},{1,3},{2,0},{3,1},{4,6},{5,7},{6,4},{7,5},{8,10},{9,11},{10,... | collective-permute-start | bytes 1572872 | tf_op jit(solution)/shard_map/ppermute | solution.py:187
  186.1 17.0 %collective-permute-start.9 = (bf16[128,2048]{1,0:T(8,128)(2,1)}, bf16[128,2048]{1,0:T(8,128)(2,1)S(1)}, u32[]{:S(2)}, u32[]{:S(2)}) collective-permute-start(bf16[128,2048]{1,0:T(8,128)(2,1)} %get-tuple-element.35), channel_id=1, source_target_pairs={{0,2},{1,3},{2,0},{3,1},{4,6},{5,7},{6,4},{7,5},{8,10},{9,11},{10,... | collective-permute-start | bytes 1572872 | tf_op jit(solution)/shard_map/ppermute | solution.py:187
  205.5 40.5 %all-to-all-start.2 = ((bf16[64,4,2176]{2,1,0:T(4,128)(2,1)}), bf16[64,4,2176]{2,1,0:T(4,128)(2,1)S(1)}, u32[]{:S(2)}, u32[]{:S(2)}) async-start(bf16[64,4,2176]{2,1,0:T(4,128)(2,1)} %reshape.222), calls=%async_computation.2 | async-start | bytes 2228224 | tf_op jit(solution)/shard_map/all_to_all | solution.py:360
  250.2 14.1 %collective-permute-start.11 = (bf16[1024,256]{1,0:T(8,128)(2,1)}, bf16[1024,256]{1,0:T(8,128)(2,1)}, u32[]{:S(2)}, u32[]{:S(2)}) collective-permute-start(bf16[1024,256]{1,0:T(8,128)(2,1)} %shard_map.169), channel_id=1, source_target_pairs={{0,3},{1,0},{2,1},{3,2},{4,7},{5,4},{6,5},{7,6},{8,11},{9,8},{10,9... | collective-permute-start | bytes 1572872 | tf_op jit(solution)/shard_map/ppermute | solution.py:187
  253.9 15.2 %collective-permute-start.10 = (bf16[1024,256]{1,0:T(8,128)(2,1)}, bf16[1024,256]{1,0:T(8,128)(2,1)}, u32[]{:S(2)}, u32[]{:S(2)}) collective-permute-start(bf16[1024,256]{1,0:T(8,128)(2,1)} %shard_map.169), channel_id=1, source_target_pairs={{0,1},{1,2},{2,3},{3,0},{4,5},{5,6},{6,7},{7,4},{8,9},{9,10},{10,1... | collective-permute-start | bytes 1572872 | tf_op jit(solution)/shard_map/ppermute | solution.py:187
  265.3 7.8 %collective-permute-start.13 = (bf16[512,256]{1,0:T(8,128)(2,1)S(1)}, bf16[512,256]{1,0:T(8,128)(2,1)S(1)}, u32[]{:S(2)}, u32[]{:S(2)}) collective-permute-start(bf16[512,256]{1,0:T(8,128)(2,1)S(1)} %slice.94), channel_id=1, source_target_pairs={{0,3},{1,0},{2,1},{3,2},{4,7},{5,4},{6,5},{7,6},{8,11},{9,8},{10,9... | collective-permute-start | bytes 786440 | tf_op jit(solution)/shard_map/ppermute | solution.py:187
  270.0 7.7 %collective-permute-start.12 = (bf16[512,256]{1,0:T(8,128)(2,1)S(1)}, bf16[512,256]{1,0:T(8,128)(2,1)S(1)}, u32[]{:S(2)}, u32[]{:S(2)}) collective-permute-start(bf16[512,256]{1,0:T(8,128)(2,1)S(1)} %slice.93), channel_id=1, source_target_pairs={{0,1},{1,2},{2,3},{3,0},{4,5},{5,6},{6,7},{7,4},{8,9},{9,10},{10,1... | collective-permute-start | bytes 786440 | tf_op jit(solution)/shard_map/ppermute | solution.py:187
  (4 other events, 6.2 us)

commit v5 on v3

--- a/solution.py
+++ b/solution.py
@@ -375,7 +375,7 @@
     specialist_widen_matrix,
     specialist_contract_matrix,
 ):
-    total_rows, width = state_probe_logits.shape
+    _, width = state_probe_logits.shape
     members = lax.axis_size(EP)
     place = lax.axis_index("tp")
     ring = lax.axis_size("tp")
@@ -479,9 +479,7 @@
                     piece, flat, (((0,), (0,)), ((), ())), preferred_element_type=F32
                 )
 
-    half = total_rows // 2
-    own, left, right = rec, shift(rec, 1), shift(rec, -1)
-    far = jnp.concatenate([shift(left[:half], 1), shift(right[half:], -1)], axis=0)
+    own, far, left, right = rec, shift(rec, 2), shift(rec, 1), shift(rec, -1)
     by_block = state_result_matrix.reshape(ring, width, -1)
 
     def columns(block, at):

time: 279 us -> 282 us (1.011)
  waiting for transfers between devices: 112 us -> 118 us
  starting transfers between devices: 69.1 us -> 66.1 us
    ppermute x18 -> x17, waiting for transfers between devices: 76.3 us -> 82.4 us  [shift(): return lax.ppermute(x, 'tp', [(i, (i + by) % n) for i in range(n)])]
    ppermute x18 -> x17, starting transfers between devices: 30.6 us -> 27.6 us  [shift(): return lax.ppermute(x, 'tp', [(i, (i + by) % n) for i in range(n)])]
  transfers between devices with their start and end apart: 22 -> 21, of which waited for: 9 -> 8; matrix products, arithmetic and copies ran while one was open for 13% -> 12% of each run, Pallas kernels for 16% -> 16%
where the time goes in v5:
time: 282 us; the launch traced here: 279 us
  waiting for transfers between devices  118 us (42%)
  starting transfers between devices  66.1 us (23%)
  Pallas kernels  48 us (17%)
  matrix products  20.7 us (7%)
  local copies, waits for them, and re-layouts  20.2 us (7%)
  other arithmetic  5.46 us (2%)
    ppermute x17, waiting for transfers between devices, shift(): return lax.ppermute(x, 'tp', [(i, (i + by) % n) for i in range(n)])  82.4 us
    all_to_all x4, starting transfers between devices, exchange(): return lax.all_to_all(x, EP, split_axis=0, concat_axis=0, tiled=True)  38.5 us
    all_to_all x4, waiting for transfers between devices, exchange(): return lax.all_to_all(x, EP, split_axis=0, concat_axis=0, tiled=True)  35.4 us
    pallas_call x4, Pallas kernels, expert_block(): pl.pallas_call(expert_kernel, out_shape=[jax.ShapeDtypeStruct((n, feature...  30.9 us
    ppermute x17, starting transfers between devices, shift(): return lax.ppermute(x, 'tp', [(i, (i + by) % n) for i in range(n)])  27.6 us
    pallas_call x1, Pallas kernels, local_pass(): vmem_call(local_kernel, (jax.ShapeDtypeStruct((rows, width), F32), jax.Sh...  8.65 us
    dot_general x4, matrix products, shards(): jnp.dot(chosen.astype(BF16), flat_in[c], preferred_element_type=F32)  7.91 us
    slice x3, local copies, waits for them, and re-layouts, halves(): lax.slice_in_dim(weight, half, 2 * half, axis=dim)  7.8 us
  transfers between devices with their start and end apart: 21, of which 8 were waited for; matrix products, arithmetic and copies ran while one was open for 12% of the time, Pallas kernels for 16%

profile of v5, /device:TPU:8, one launch (start us, length us, event | category | flops | bytes accessed | tf_op | source)
XLA Modules:
  0.0 279.3 jit_solution(3277139281247519487)
XLA Ops:
  2.3 3.1 %slice_bitcast_fusion = (bf16[256,2048]{1,0:T(8,128)(2,1)}, bf16[256,2048]{1,0:T(8,128)(2,1)}) fusion(bf16[1,512,2048]{2,1,0:T(8,128)(2,1)} %param.31), kind=kLoop, calls=%fused_computation.26 | loop fusion | bytes 4194304 | tf_op jit(solution)/shard_map/slice | solution.py:347
  7.7 12.3 %all-to-all-start = ((bf16[64,8,2048]{2,1,0:T(8,128)(2,1)}), bf16[64,8,2048]{2,1,0:T(8,128)(2,1)}, u32[]{:S(2)}, u32[]{:S(2)}) async-start(bf16[64,8,2048]{2,1,0:T(8,128)(2,1)} %fusion), calls=%async_computation | async-start | bytes 4194304 | tf_op jit(solution)/shard_map/all_to_all | solution.py:357
  20.0 3.2 %fusion.64 = (bf16[2048,256]{1,0:T(8,128)(2,1)}, bf16[2048,256]{1,0:T(8,128)(2,1)}) fusion(bf16[2048,512]{1,0:T(8,128)(2,1)} %bitcast.71), kind=kLoop, calls=%fused_computation.104 | loop fusion | bytes 4194304 | tf_op jit(solution)/shard_map/slice | solution.py:347
  30.0 2.8 collective-permute-start.5
  33.8 16.9 %collective-permute-done.2.gate_left = bf16[2048,256]{1,0:T(8,128)(2,1)S(1)} collective-permute-done((bf16[2048,256]{1,0:T(8,128)(2,1)}, bf16[2048,256]{1,0:T(8,128)(2,1)S(1)}, u32[]{:S(2)}, u32[]{:S(2)}) %collective-permute-start.2) | collective-permute-done | bytes 1048608 | tf_op jit(solution)/shard_map/ppermute | solution.py:187
  50.9 8.7 %shard_map.167 = (f32[1024,256]{1,0:T(8,128)}, bf16[1024,256]{1,0:T(8,128)(2,1)}, f32[256,256]{1,0:T(8,128)}) custom-call(bf16[1024,256]{1,0:T(8,128)(2,1)} %q_ref.1, bf16[1024,256]{1,0:T(8,128)(2,1)} %r_ref, bf16[1024,256]{1,0:T(8,128)(2,1)} %v_ref.1, f32[1,256]{1,0:T(1,128)} %bitcast.99, f32[1024,2]{1,0:T(8,128)} %copy.30.fade_ref), custom_call_target="tpu_custom_call" | custom-call | flops 4000000000 | bytes 6291456 | tf_op jit(solution)/shard_map/pallas_call | solution.py:151
  61.3 9.8 %all-to-all-done = bf16[64,8,2048]{2,1,0:T(8,128)(2,1)} async-done(((bf16[64,8,2048]{2,1,0:T(8,128)(2,1)}), bf16[64,8,2048]{2,1,0:T(8,128)(2,1)}, u32[]{:S(2)}, u32[]{:S(2)}) %all-to-all-start) | async-done | bytes 2097184 | tf_op jit(solution)/shard_map/all_to_all | solution.py:357
  71.2 5.4 %all-to-all-start.1 = ((f32[64,4,256]{2,1,0:T(4,128)}), f32[64,4,256]{2,1,0:T(4,128)S(1)}, u32[]{:S(2)}, u32[]{:S(2)}) async-start(f32[64,4,256]{2,1,0:T(4,128)} %reshape.220), calls=%async_computation.1 | async-start | bytes 524288 | tf_op jit(solution)/shard_map/all_to_all | solution.py:357
  78.2 3.1 %collective-permute-start.15 = (bf16[128,2048]{1,0:T(8,128)(2,1)S(1)}, bf16[128,2048]{1,0:T(8,128)(2,1)S(1)}, u32[]{:S(2)}, u32[]{:S(2)}) collective-permute-start(bf16[128,2048]{1,0:T(8,128)(2,1)S(1)} %convolution_convert_fusion.1.own), channel_id=1, source_target_pairs={{0,2},{1,3},{2,0},{3,1},{4,6},{5,7},{6,4},{7,5},{8,10},{9,11},{10,... | collective-permute-start | bytes 1572872 | tf_op jit(solution)/shard_map/ppermute | solution.py:187
  83.5 2.4 convolution_convert_fusion.3.own
  85.9 30.7 %collective-permute-done.5.down_right = bf16[256,2048]{1,0:T(8,128)(2,1)} collective-permute-done((bf16[256,2048]{1,0:T(8,128)(2,1)}, bf16[256,2048]{1,0:T(8,128)(2,1)}, u32[]{:S(2)}, u32[]{:S(2)}) %collective-permute-start.5) | collective-permute-done | bytes 1048608 | tf_op jit(solution)/shard_map/ppermute | solution.py:187
  117.4 7.7 %expert_block.7 = (bf16[128,2048]{1,0:T(8,128)(2,1)}, bf16[128,2048]{1,0:T(8,128)(2,1)}) custom-call(bf16[128,2048]{1,0:T(8,128)(2,1)} %copy-done.4, bf16[128,2048]{1,0:T(8,128)(2,1)} %copy-done.9, bf16[2048,512]{1,0:T(8,128)(2,1)} %bitcast.72, bf16[2048,256]{1,0:T(8,128)(2,1)} %collective-permute-done.1.gate_right, bf16[2048,256]{1,0:T(8,128)(2,1)} %copy-done.2, ...), custom_call_target="tpu_custom_call" | custom-call | flops 3221225472 | bytes 14680064 | tf_op jit(solution)/shard_map/expert_block/pallas_call | solution.py:299
  125.5 7.7 %expert_block.6 = (bf16[128,2048]{1,0:T(8,128)(2,1)}, bf16[128,2048]{1,0:T(8,128)(2,1)}) custom-call(bf16[128,2048]{1,0:T(8,128)(2,1)} %copy-done.3, bf16[128,2048]{1,0:T(8,128)(2,1)} %collective-permute-done.13.far, bf16[2048,512]{1,0:T(8,128)(2,1)} %bitcast.73, bf16[2048,256]{1,0:T(8,128)(2,1)} %collective-permute-done.1.gate_right, ...), custom_call_target="tpu_custom_call" | custom-call | flops 3221225472 | bytes 14680064 | tf_op jit(solution)/shard_map/expert_block/pallas_call | solution.py:299
  133.2 3.6 %collective-permute-start.14 = (bf16[128,2048]{1,0:T(8,128)(2,1)}, bf16[128,2048]{1,0:T(8,128)(2,1)}, u32[]{:S(2)}, u32[]{:S(2)}) collective-permute-start(bf16[128,2048]{1,0:T(8,128)(2,1)} %get-tuple-element.37), channel_id=1, source_target_pairs={{0,2},{1,3},{2,0},{3,1},{4,6},{5,7},{6,4},{7,5},{8,10},{9,11},{10,... | collective-permute-start | bytes 1572872 | tf_op jit(solution)/shard_map/ppermute | solution.py:187
  136.8 2.4 convolution_convert_fusion.4.own
  139.3 3.4 %collective-permute-start.8 = (bf16[128,2048]{1,0:T(8,128)(2,1)}, bf16[128,2048]{1,0:T(8,128)(2,1)}, u32[]{:S(2)}, u32[]{:S(2)}) collective-permute-start(bf16[128,2048]{1,0:T(8,128)(2,1)} %convolution_convert_fusion.3.own), channel_id=1, source_target_pairs={{0,2},{1,3},{2,0},{3,1},{4,6},{5,7},{6,4},{7,5},{8,10},{9,11},{10,... | collective-permute-start | bytes 1572872 | tf_op jit(solution)/shard_map/ppermute | solution.py:187
  146.4 6.9 %collective-permute-done.14 = bf16[128,2048]{1,0:T(8,128)(2,1)} collective-permute-done((bf16[128,2048]{1,0:T(8,128)(2,1)}, bf16[128,2048]{1,0:T(8,128)(2,1)}, u32[]{:S(2)}, u32[]{:S(2)}) %collective-permute-start.14) | collective-permute-done | bytes 524320 | tf_op jit(solution)/shard_map/ppermute | solution.py:187
  155.8 10.5 %all-to-all-start.3 = ((bf16[64,4,2048]{2,1,0:T(4,128)(2,1)}), bf16[64,4,2048]{2,1,0:T(4,128)(2,1)}, u32[]{:S(2)}, u32[]{:S(2)}) async-start(bf16[64,4,2048]{2,1,0:T(4,128)(2,1)} %reshape.226), calls=%async_computation.3 | async-start | bytes 2097152 | tf_op jit(solution)/shard_map/all_to_all | solution.py:357
  166.3 7.7 %expert_block.4 = (bf16[128,2048]{1,0:T(8,128)(2,1)}, bf16[128,2048]{1,0:T(8,128)(2,1)}) custom-call(bf16[128,2048]{1,0:T(8,128)(2,1)} %convolution_convert_fusion.4.own, bf16[128,2048]{1,0:T(8,128)(2,1)} %collective-permute-done.far, bf16[2048,512]{1,0:T(8,128)(2,1)} %bitcast.74, bf16[2048,256]{1,0:T(8,128)(2,1)} %collective-permute-done.1.gate_right, ...), custom_call_target="tpu_custom_call" | custom-call | flops 3221225472 | bytes 14680064 | tf_op jit(solution)/shard_map/expert_block/pallas_call | solution.py:299
  174.2 7.7 %expert_block.5 = (bf16[128,2048]{1,0:T(8,128)(2,1)}, bf16[128,2048]{1,0:T(8,128)(2,1)}) custom-call(bf16[128,2048]{1,0:T(8,128)(2,1)} %convolution_convert_fusion.3.own, bf16[128,2048]{1,0:T(8,128)(2,1)} %collective-permute-done.8.far, bf16[2048,512]{1,0:T(8,128)(2,1)} %bitcast.75, bf16[2048,256]{1,0:T(8,128)(2,1)} %collective-permute-done.1.gate_right, ...), custom_call_target="tpu_custom_call" | custom-call | flops 3221225472 | bytes 14680064 | tf_op jit(solution)/shard_map/expert_block/pallas_call | solution.py:299
  182.0 3.5 %collective-permute-start.9 = (bf16[128,2048]{1,0:T(8,128)(2,1)}, bf16[128,2048]{1,0:T(8,128)(2,1)S(1)}, u32[]{:S(2)}, u32[]{:S(2)}) collective-permute-start(bf16[128,2048]{1,0:T(8,128)(2,1)} %get-tuple-element.35), channel_id=1, source_target_pairs={{0,2},{1,3},{2,0},{3,1},{4,6},{5,7},{6,4},{7,5},{8,10},{9,11},{10,... | collective-permute-start | bytes 1572872 | tf_op jit(solution)/shard_map/ppermute | solution.py:187
  185.5 5.1 %collective-permute-done.7 = bf16[128,2048]{1,0:T(8,128)(2,1)S(1)} collective-permute-done((bf16[128,2048]{1,0:T(8,128)(2,1)}, bf16[128,2048]{1,0:T(8,128)(2,1)S(1)}, u32[]{:S(2)}, u32[]{:S(2)}) %collective-permute-start.7) | collective-permute-done | bytes 524320 | tf_op jit(solution)/shard_map/ppermute | solution.py:187
  190.8 10.2 %collective-permute-done.9 = bf16[128,2048]{1,0:T(8,128)(2,1)S(1)} collective-permute-done((bf16[128,2048]{1,0:T(8,128)(2,1)}, bf16[128,2048]{1,0:T(8,128)(2,1)S(1)}, u32[]{:S(2)}, u32[]{:S(2)}) %collective-permute-start.9) | collective-permute-done | bytes 524320 | tf_op jit(solution)/shard_map/ppermute | solution.py:187
  203.4 10.3 %all-to-all-start.2 = ((bf16[64,4,2176]{2,1,0:T(4,128)(2,1)}), bf16[64,4,2176]{2,1,0:T(4,128)(2,1)S(1)}, u32[]{:S(2)}, u32[]{:S(2)}) async-start(bf16[64,4,2176]{2,1,0:T(4,128)(2,1)} %reshape.222), calls=%async_computation.2 | async-start | bytes 2228224 | tf_op jit(solution)/shard_map/all_to_all | solution.py:357
  216.2 2.1 reshape.227.flat_ref
  218.3 25.6 %all-to-all-done.2 = bf16[64,4,2176]{2,1,0:T(4,128)(2,1)S(1)} async-done(((bf16[64,4,2176]{2,1,0:T(4,128)(2,1)}), bf16[64,4,2176]{2,1,0:T(4,128)(2,1)S(1)}, u32[]{:S(2)}, u32[]{:S(2)}) %all-to-all-start.2) | async-done | bytes 1114144 | tf_op jit(solution)/shard_map/all_to_all | solution.py:357
  244.6 3.6 %shard_map.169 = bf16[1024,256]{1,0:T(8,128)(2,1)} custom-call(f32[1024,256]{1,0:T(8,128)} %get-tuple-element.22.raw_ref, bf16[1024,256]{1,0:T(8,128)(2,1)} %get-tuple-element.23.qdec_ref, bf16[256,128]{1,0:T(8,128)(2,1)} %bitcast.97, bf16[1024,256]{1,0:T(8,128)(2,1)} %gate_ref.1, f32[1,256]{1,0:T(1,128)} %bitcast.100), custom_call_target="tpu_custom_call" | custom-call | flops 2000000000 | bytes 4194304 | tf_op jit(solution)/shard_map/pallas_call | solution.py:176
  248.4 3.7 %collective-permute-start.11 = (bf16[1024,256]{1,0:T(8,128)(2,1)}, bf16[1024,256]{1,0:T(8,128)(2,1)}, u32[]{:S(2)}, u32[]{:S(2)}) collective-permute-start(bf16[1024,256]{1,0:T(8,128)(2,1)} %shard_map.169), channel_id=1, source_target_pairs={{0,3},{1,0},{2,1},{3,2},{4,7},{5,4},{6,5},{7,6},{8,11},{9,8},{10,9... | collective-permute-start | bytes 1572872 | tf_op jit(solution)/shard_map/ppermute | solution.py:187
  254.6 2.3 fusion.1.partial_ref
  256.9 3.1 %shard_map.170 = bf16[128,2048]{1,0:T(8,128)(2,1)} custom-call(bf16[256,2048]{1,0:T(8,128)(2,1)} %reshape.227.flat_ref, bf16[256,128]{1,0:T(8,128)(2,1)} %fusion.62.coarse_ref, bf16[256,128]{1,0:T(8,128)(2,1)} %subtract_convert_fusion.fine_ref, f32[128,2048]{1,0:T(8,128)} %fusion.1.partial_ref, f32[1,2048]{1,0:T(1,128)} %bitcast.98), custom_call_target="tpu_custom_call" | custom-call | flops 268435456 | bytes 4194304 | tf_op jit(solution)/shard_map/pallas_call | solution.py:334
  261.4 12.4 %collective-permute-done.10 = bf16[1024,256]{1,0:T(8,128)(2,1)} collective-permute-done((bf16[1024,256]{1,0:T(8,128)(2,1)}, bf16[1024,256]{1,0:T(8,128)(2,1)}, u32[]{:S(2)}, u32[]{:S(2)}) %collective-permute-start.10) | collective-permute-done | bytes 524320 | tf_op jit(solution)/shard_map/ppermute | solution.py:187
  276.8 2.5 add_convert_fusion
  (95 shorter events, 37.7 us)
Async XLA Ops:
  2.3 3.3 %copy-start.12 = (f32[2048]{0:T(1024)S(1)}, f32[2048]{0:T(1024)}, u32[]{:S(2)}) copy-start(f32[2048]{0:T(1024)} %param.27) | copy-start | bytes 24580
  7.7 63.5 %all-to-all-start = ((bf16[64,8,2048]{2,1,0:T(8,128)(2,1)}), bf16[64,8,2048]{2,1,0:T(8,128)(2,1)}, u32[]{:S(2)}, u32[]{:S(2)}) async-start(bf16[64,8,2048]{2,1,0:T(8,128)(2,1)} %fusion), calls=%async_computation | async-start | bytes 4194304 | tf_op jit(solution)/shard_map/all_to_all | solution.py:357
  20.0 6.4 %copy-start.1 = (bf16[1,2048,512]{2,1,0:T(8,128)(2,1)S(1)}, bf16[1,2048,512]{2,1,0:T(8,128)(2,1)}, u32[]{:S(2)}) copy-start(bf16[1,2048,512]{2,1,0:T(8,128)(2,1)} %param.30) | copy-start | bytes 6291460
  23.2 27.5 %collective-permute-start.2 = (bf16[2048,256]{1,0:T(8,128)(2,1)}, bf16[2048,256]{1,0:T(8,128)(2,1)S(1)}, u32[]{:S(2)}, u32[]{:S(2)}) collective-permute-start(bf16[2048,256]{1,0:T(8,128)(2,1)} %get-tuple-element.40), channel_id=1, source_target_pairs={{0,1},{1,2},{2,3},{3,0},{4,5},{5,6},{6,7},{7,4},{8,9},{9,10},{10,1... | collective-permute-start | bytes 3145736 | tf_op jit(solution)/shard_map/ppermute | solution.py:187
  24.7 53.5 %collective-permute-start.1 = (bf16[2048,256]{1,0:T(8,128)(2,1)}, bf16[2048,256]{1,0:T(8,128)(2,1)}, u32[]{:S(2)}, u32[]{:S(2)}) collective-permute-start(bf16[2048,256]{1,0:T(8,128)(2,1)} %get-tuple-element.41), channel_id=1, source_target_pairs={{0,3},{1,0},{2,1},{3,2},{4,7},{5,4},{6,5},{7,6},{8,11},{9,8},{10,9... | collective-permute-start | bytes 3145736 | tf_op jit(solution)/shard_map/ppermute | solution.py:187
  26.4 6.3 %copy-start.13 = (f32[1024,2]{0,1:T(2,128)S(1)}, f32[1024,2]{0,1:T(2,128)}, u32[]{:S(2)}) copy-start(f32[1024,2]{0,1:T(2,128)} %param.21) | copy-start | bytes 24580
  28.0 55.0 %collective-permute-start.3 = (bf16[2048,256]{1,0:T(8,128)(2,1)}, bf16[2048,256]{1,0:T(8,128)(2,1)}, u32[]{:S(2)}, u32[]{:S(2)}) collective-permute-start(bf16[2048,256]{1,0:T(8,128)(2,1)} %get-tuple-element.27), channel_id=1, source_target_pairs={{0,3},{1,0},{2,1},{3,2},{4,7},{5,4},{6,5},{7,6},{8,11},{9,8},{10,9... | collective-permute-start | bytes 3145736 | tf_op jit(solution)/shard_map/ppermute | solution.py:187
  29.5 56.4 %collective-permute-start.4 = (bf16[2048,256]{1,0:T(8,128)(2,1)}, bf16[2048,256]{1,0:T(8,128)(2,1)}, u32[]{:S(2)}, u32[]{:S(2)}) collective-permute-start(bf16[2048,256]{1,0:T(8,128)(2,1)} %get-tuple-element.28), channel_id=1, source_target_pairs={{0,1},{1,2},{2,3},{3,0},{4,5},{5,6},{6,7},{7,4},{8,9},{9,10},{10,1... | collective-permute-start | bytes 3145736 | tf_op jit(solution)/shard_map/ppermute | solution.py:187
  30.0 86.6 %collective-permute-start.5 = (bf16[256,2048]{1,0:T(8,128)(2,1)}, bf16[256,2048]{1,0:T(8,128)(2,1)}, u32[]{:S(2)}, u32[]{:S(2)}) collective-permute-start(bf16[256,2048]{1,0:T(8,128)(2,1)} %get-tuple-element.29), channel_id=1, source_target_pairs={{0,3},{1,0},{2,1},{3,2},{4,7},{5,4},{6,5},{7,6},{8,11},{9,8},{10,9... | collective-permute-start | bytes 3145736 | tf_op jit(solution)/shard_map/ppermute | solution.py:187
  50.7 8.9 %copy-start.2 = (bf16[2048,256]{1,0:T(8,128)(2,1)}, bf16[2048,256]{1,0:T(8,128)(2,1)S(1)}, u32[]{:S(2)}) copy-start(bf16[2048,256]{1,0:T(8,128)(2,1)S(1)} %collective-permute-done.2.gate_left) | copy-start | bytes 3145732
  50.7 66.0 %collective-permute-start.6 = (bf16[256,2048]{1,0:T(8,128)(2,1)}, bf16[256,2048]{1,0:T(8,128)(2,1)}, u32[]{:S(2)}, u32[]{:S(2)}) collective-permute-start(bf16[256,2048]{1,0:T(8,128)(2,1)} %get-tuple-element.30), channel_id=1, source_target_pairs={{0,1},{1,2},{2,3},{3,0},{4,5},{5,6},{6,7},{7,4},{8,9},{9,10},{10,1... | collective-permute-start | bytes 3145736 | tf_op jit(solution)/shard_map/ppermute | solution.py:187
  71.2 71.6 %all-to-all-start.1 = ((f32[64,4,256]{2,1,0:T(4,128)}), f32[64,4,256]{2,1,0:T(4,128)S(1)}, u32[]{:S(2)}, u32[]{:S(2)}) async-start(f32[64,4,256]{2,1,0:T(4,128)} %reshape.220), calls=%async_computation.1 | async-start | bytes 524288 | tf_op jit(solution)/shard_map/all_to_all | solution.py:357
  78.2 39.2 %copy-start.4 = (bf16[128,2048]{1,0:T(8,128)(2,1)}, bf16[128,2048]{1,0:T(8,128)(2,1)S(1)}, u32[]{:S(2)}) copy-start(bf16[128,2048]{1,0:T(8,128)(2,1)S(1)} %convolution_convert_fusion.1.own) | copy-start | bytes 1572868
  78.2 38.4 %collective-permute-start.15 = (bf16[128,2048]{1,0:T(8,128)(2,1)S(1)}, bf16[128,2048]{1,0:T(8,128)(2,1)S(1)}, u32[]{:S(2)}, u32[]{:S(2)}) collective-permute-start(bf16[128,2048]{1,0:T(8,128)(2,1)S(1)} %convolution_convert_fusion.1.own), channel_id=1, source_target_pairs={{0,2},{1,3},{2,0},{3,1},{4,6},{5,7},{6,4},{7,5},{8,10},{9,11},{10,... | collective-permute-start | bytes 1572872 | tf_op jit(solution)/shard_map/ppermute | solution.py:187
  82.9 42.3 %copy-start.3 = (bf16[128,2048]{1,0:T(8,128)(2,1)}, bf16[128,2048]{1,0:T(8,128)(2,1)S(1)}, u32[]{:S(2)}) copy-start(bf16[128,2048]{1,0:T(8,128)(2,1)S(1)} %convolution_convert_fusion.2.own) | copy-start | bytes 1572868
  82.9 42.5 %collective-permute-start.13 = (bf16[128,2048]{1,0:T(8,128)(2,1)S(1)}, bf16[128,2048]{1,0:T(8,128)(2,1)}, u32[]{:S(2)}, u32[]{:S(2)}) collective-permute-start(bf16[128,2048]{1,0:T(8,128)(2,1)S(1)} %convolution_convert_fusion.2.own), channel_id=1, source_target_pairs={{0,2},{1,3},{2,0},{3,1},{4,6},{5,7},{6,4},{7,5},{8,10},{9,11},{10,... | collective-permute-start | bytes 1572872 | tf_op jit(solution)/shard_map/ppermute | solution.py:187
  125.2 20.0 %collective-permute-start.16 = (bf16[128,2048]{1,0:T(8,128)(2,1)}, bf16[128,2048]{1,0:T(8,128)(2,1)}, u32[]{:S(2)}, u32[]{:S(2)}) collective-permute-start(bf16[128,2048]{1,0:T(8,128)(2,1)} %get-tuple-element.39), channel_id=1, source_target_pairs={{0,2},{1,3},{2,0},{3,1},{4,6},{5,7},{6,4},{7,5},{8,10},{9,11},{10,... | collective-permute-start | bytes 1572872 | tf_op jit(solution)/shard_map/ppermute | solution.py:187
  133.2 12.0 %copy-start.6 = (bf16[128,2048]{1,0:T(8,128)(2,1)S(1)}, bf16[128,2048]{1,0:T(8,128)(2,1)}, u32[]{:S(2)}) copy-start(bf16[128,2048]{1,0:T(8,128)(2,1)} %get-tuple-element.38) | copy-start | bytes 1572868
  133.2 20.1 %copy-start.7 = (bf16[128,2048]{1,0:T(8,128)(2,1)S(1)}, bf16[128,2048]{1,0:T(8,128)(2,1)}, u32[]{:S(2)}) copy-start(bf16[128,2048]{1,0:T(8,128)(2,1)} %get-tuple-element.36) | copy-start | bytes 1572868
  133.2 20.1 %collective-permute-start.14 = (bf16[128,2048]{1,0:T(8,128)(2,1)}, bf16[128,2048]{1,0:T(8,128)(2,1)}, u32[]{:S(2)}, u32[]{:S(2)}) collective-permute-start(bf16[128,2048]{1,0:T(8,128)(2,1)} %get-tuple-element.37), channel_id=1, source_target_pairs={{0,2},{1,3},{2,0},{3,1},{4,6},{5,7},{6,4},{7,5},{8,10},{9,11},{10,... | collective-permute-start | bytes 1572872 | tf_op jit(solution)/shard_map/ppermute | solution.py:187
  139.2 27.1 %collective-permute-start = (bf16[128,2048]{1,0:T(8,128)(2,1)}, bf16[128,2048]{1,0:T(8,128)(2,1)}, u32[]{:S(2)}, u32[]{:S(2)}) collective-permute-start(bf16[128,2048]{1,0:T(8,128)(2,1)} %convolution_convert_fusion.4.own), channel_id=1, source_target_pairs={{0,2},{1,3},{2,0},{3,1},{4,6},{5,7},{6,4},{7,5},{8,10},{9,11},{10,... | collective-permute-start | bytes 1572872 | tf_op jit(solution)/shard_map/ppermute | solution.py:187
  139.3 35.0 %collective-permute-start.8 = (bf16[128,2048]{1,0:T(8,128)(2,1)}, bf16[128,2048]{1,0:T(8,128)(2,1)}, u32[]{:S(2)}, u32[]{:S(2)}) collective-permute-start(bf16[128,2048]{1,0:T(8,128)(2,1)} %convolution_convert_fusion.3.own), channel_id=1, source_target_pairs={{0,2},{1,3},{2,0},{3,1},{4,6},{5,7},{6,4},{7,5},{8,10},{9,11},{10,... | collective-permute-start | bytes 1572872 | tf_op jit(solution)/shard_map/ppermute | solution.py:187
  155.8 47.7 %all-to-all-start.3 = ((bf16[64,4,2048]{2,1,0:T(4,128)(2,1)}), bf16[64,4,2048]{2,1,0:T(4,128)(2,1)}, u32[]{:S(2)}, u32[]{:S(2)}) async-start(bf16[64,4,2048]{2,1,0:T(4,128)(2,1)} %reshape.226), calls=%async_computation.3 | async-start | bytes 2097152 | tf_op jit(solution)/shard_map/all_to_all | solution.py:357
  174.0 11.5 %copy-start.11 = (bf16[64,4,128]{2,1,0:T(4,128)(2,1)S(1)}, bf16[64,4,128]{2,1,0:T(4,128)(2,1)}, u32[]{:S(2)}) copy-start(bf16[64,4,128]{2,1,0:T(4,128)(2,1)} %shard_map.168) | copy-start | bytes 196612
  174.0 16.6 %copy-start.8 = (bf16[128,2048]{1,0:T(8,128)(2,1)S(1)}, bf16[128,2048]{1,0:T(8,128)(2,1)}, u32[]{:S(2)}) copy-start(bf16[128,2048]{1,0:T(8,128)(2,1)} %get-tuple-element.31) | copy-start | bytes 1572868
  174.0 16.6 %collective-permute-start.7 = (bf16[128,2048]{1,0:T(8,128)(2,1)}, bf16[128,2048]{1,0:T(8,128)(2,1)S(1)}, u32[]{:S(2)}, u32[]{:S(2)}) collective-permute-start(bf16[128,2048]{1,0:T(8,128)(2,1)} %get-tuple-element.32), channel_id=1, source_target_pairs={{0,2},{1,3},{2,0},{3,1},{4,6},{5,7},{6,4},{7,5},{8,10},{9,11},{10,... | collective-permute-start | bytes 1572872 | tf_op jit(solution)/shard_map/ppermute | solution.py:187
  182.0 19.0 %collective-permute-start.9 = (bf16[128,2048]{1,0:T(8,128)(2,1)}, bf16[128,2048]{1,0:T(8,128)(2,1)S(1)}, u32[]{:S(2)}, u32[]{:S(2)}) collective-permute-start(bf16[128,2048]{1,0:T(8,128)(2,1)} %get-tuple-element.35), channel_id=1, source_target_pairs={{0,2},{1,3},{2,0},{3,1},{4,6},{5,7},{6,4},{7,5},{8,10},{9,11},{10,... | collective-permute-start | bytes 1572872 | tf_op jit(solution)/shard_map/ppermute | solution.py:187
  203.4 40.5 %all-to-all-start.2 = ((bf16[64,4,2176]{2,1,0:T(4,128)(2,1)}), bf16[64,4,2176]{2,1,0:T(4,128)(2,1)S(1)}, u32[]{:S(2)}, u32[]{:S(2)}) async-start(bf16[64,4,2176]{2,1,0:T(4,128)(2,1)} %reshape.222), calls=%async_computation.2 | async-start | bytes 2228224 | tf_op jit(solution)/shard_map/all_to_all | solution.py:357
  248.2 28.6 %collective-permute-start.12 = (bf16[1024,256]{1,0:T(8,128)(2,1)}, bf16[1024,256]{1,0:T(8,128)(2,1)}, u32[]{:S(2)}, u32[]{:S(2)}) collective-permute-start(bf16[1024,256]{1,0:T(8,128)(2,1)} %shard_map.169), channel_id=1, source_target_pairs={{0,2},{1,3},{2,0},{3,1},{4,6},{5,7},{6,4},{7,5},{8,10},{9,11},{10,... | collective-permute-start | bytes 1572872 | tf_op jit(solution)/shard_map/ppermute | solution.py:187
  248.4 26.9 %collective-permute-start.11 = (bf16[1024,256]{1,0:T(8,128)(2,1)}, bf16[1024,256]{1,0:T(8,128)(2,1)}, u32[]{:S(2)}, u32[]{:S(2)}) collective-permute-start(bf16[1024,256]{1,0:T(8,128)(2,1)} %shard_map.169), channel_id=1, source_target_pairs={{0,3},{1,0},{2,1},{3,2},{4,7},{5,4},{6,5},{7,6},{8,11},{9,8},{10,9... | collective-permute-start | bytes 1572872 | tf_op jit(solution)/shard_map/ppermute | solution.py:187
  252.1 21.7 %collective-permute-start.10 = (bf16[1024,256]{1,0:T(8,128)(2,1)}, bf16[1024,256]{1,0:T(8,128)(2,1)}, u32[]{:S(2)}, u32[]{:S(2)}) collective-permute-start(bf16[1024,256]{1,0:T(8,128)(2,1)} %shard_map.169), channel_id=1, source_target_pairs={{0,1},{1,2},{2,3},{3,0},{4,5},{5,6},{6,7},{7,4},{8,9},{9,10},{10,1... | collective-permute-start | bytes 1572872 | tf_op jit(solution)/shard_map/ppermute | solution.py:187
  256.9 3.1 %copy-start.5 = (bf16[1024,512]{1,0:T(8,128)(2,1)S(1)}, bf16[1024,512]{1,0:T(8,128)(2,1)}, u32[]{:S(2)}) copy-start(bf16[1024,512]{1,0:T(8,128)(2,1)} %param.23) | copy-start | bytes 3145732
  (3 other events, 3.1 us)
